TPU v7x, 128 devices: a whole 4x4x4 slice. The times are simulated.
128 devices in a mesh: kv: 16 (over z, y), tp: 8 (over x, core).
Axes of the slice: x: 4, y: 4, z: 4, core: 2. Of those that a mesh axis runs over, the one named last changes fastest.
Arguments:
- tokens: bfloat16 [256, 4, 2048], P(None, None, ('kv', 'tp')), may hold values from -520 to 520
- input_norm_gain: bfloat16 [2048], replicated, may hold values from 0.099609375 to 1.8984375
- query_weight: bfloat16 [2048, 2048], P(None, 'kv'), may hold values from -0.125 to 0.125
- key_weight: bfloat16 [2048, 2048], P(None, 'kv'), may hold values from -0.125 to 0.125
- value_weight: bfloat16 [2048, 16, 128], P(None, 'kv', 'tp'), may hold values from -1.14904852 to 1.14904852
- output_gate_weight: bfloat16 [2048, 16, 128], P(None, 'kv', 'tp'), may hold values from -0.125 to 0.125
- strength_weight: bfloat16 [2048, 16], P(None, 'kv'), may hold values from -0.125 to 0.125
- decay_weight: bfloat16 [2048, 16], P(None, 'kv'), may hold values from -0.125 to 0.125
- head_decay_rate: float32 [16], P('kv'), may hold values from 0.005 to 1.5
- proposal_log_decay: float32 [256, 4, 16], P(None, None, 'kv'), may hold values from -0.69 to 0
- head_norm_gain: bfloat16 [128], P('tp'), may hold values from 0.099609375 to 1.8984375
- output_weight: bfloat16 [16, 128, 2048], P('kv', 'tp'), may hold values from -1.14904852 to 1.14904852
- output_norm_gain: bfloat16 [2048], P(('kv', 'tp')), may hold values from 0.099609375 to 1.8984375
- state: float32 [256, 16, 128, 128], P(None, 'kv', 'tp'), may hold values from -4.5961941 to 4.5961941
- previous_keys: bfloat16 [256, 4, 2048], P(None, None, 'kv'), may hold values from -6 to 6
- previous_values: bfloat16 [256, 4, 16, 128], P(None, None, 'kv', 'tp'), may hold values from -52 to 52
- previous_log_decay: float32 [256, 4, 16], P(None, None, 'kv'), may hold values from -0.7 to -0.02
- previous_strengths: float32 [256, 4, 16], P(None, None, 'kv'), may hold values from 0.1 to 0.9
- accepted: int32 [256], replicated, may hold values from 0 to 4
- parent: int32 [256, 4], replicated, may hold values from -1 to 2, as said below
Outputs:
- layer_out: bfloat16 [256, 4, 2048], P(None, None, ('kv', 'tp'))
- accepted_state: float32 [256, 16, 128, 128], P(None, 'kv', 'tp')
Inputs may be any that keep to these rules, and one draw needn't show every extreme that they name: parent[b, i] is -1 or a proposal index below i; -1 means that proposal i follows the accepted old proposals directly.
All inputs are finite; a program needn't handle non-finite values.
Results may differ from a plain program's by a relative error of at most 0.019.
Values may be sent and summed in bfloat16 or wider, within the bound.
No kernel may reach another device: no remote copies, remote signals or barrier semaphores. Data moves between devices by JAX's collectives and lax.ppermute only.
A program may use at most 128 MiB of HBM per device.

v0:
```python
import jax
import jax.numpy as jnp
from jax import lax
from jax.experimental import pallas as pl
from jax.experimental.pallas import tpu as pltpu
from jax.sharding import PartitionSpec as P


epsilon = 1e-06
f32 = jnp.float32
bf16 = jnp.bfloat16
BOTH = ("kv", "tp")
GROUPS = 2
VMEM_LIMIT = 16 << 20


def dot(a, b, ca, cb):
    return lax.dot_general(a, b, (((ca,), (cb,)), ((), ())), preferred_element_type=f32)


def iota(shape, dim):
    return lax.broadcasted_iota(jnp.int32, shape, dim)


def roll(x, shift):
    return pltpu.roll(x, shift, 1)


def split(x):
    hi = x.astype(bf16)
    return hi, (x - hi.astype(f32)).astype(bf16)


def cost(flops, size):
    return pl.CostEstimate(flops=flops, bytes_accessed=size, transcendentals=0)


def chunk_lanes(rows, group):
    lane = iota((1, 128), 1)
    packed = None
    for j in range(4):
        if isinstance(group, int):
            half = rows[j][:, 128 * (group // 4) : 128 * (group // 4) + 128]
            shift = (32 * j - 32 * (group % 4)) % 128
            moved = roll(half, shift) if shift else half
        else:
            half = jnp.where(group >= 4, rows[j][:, 128:], rows[j][:, :128])
            moved = roll(half, lax.rem(32 * j + 128 - 32 * lax.rem(group, 4), 128))
        packed = moved if packed is None else jnp.where(lane // 32 == j, moved, packed)
    return packed


def solve(rhs, coupling):
    x = rhs
    for _ in range(3):
        x = rhs - sum(coupling[d] * roll(x, 32 * d) for d in (1, 2, 3))
    return x


def send_tokens_kernel(x_ref, out_ref):
    rows = [x_ref[i].astype(f32) for i in range(4)]
    for t in range(8):
        block = chunk_lanes(rows, t).astype(bf16)
        for k in range(16):
            out_ref[k, t] = block


def send_tokens(tokens):
    return pl.pallas_call(
        send_tokens_kernel,
        out_shape=jax.ShapeDtypeStruct((16, 8, 16, 128), bf16),
        cost_estimate=cost(1000000, 1 << 19),
        compiler_params=pltpu.CompilerParams(vmem_limit_bytes=VMEM_LIMIT),
        name="send_tokens",
    )(tokens)


def state_kernel(state_ref, key_ref, value_ref, strength_ref, decay_ref, accepted_ref, out_ref, low_ref):
    for part in range(GROUPS):
        rows = pl.ds(32 * part, 32)
        new = state_of_group(
            GROUPS * pl.program_id(0) + part,
            state_ref[rows],
            key_ref[pl.ds(128 * part, 128), :],
            value_ref,
            strength_ref,
            decay_ref,
            accepted_ref,
        )
        out_ref[rows] = new
        low_ref[pl.ds(512 * part, 512), :] = new.reshape(512, 128).astype(bf16)


def state_of_group(group, state, key_rows, value_ref, strength_ref, decay_ref, accepted_ref):
    lane = iota((1, 128), 1)
    place = lane // 32
    values = chunk_lanes([value_ref[j].astype(f32) for j in range(4)], group)
    strength = chunk_lanes([strength_ref[j] for j in range(4)], group)
    decay = chunk_lanes([decay_ref[j] for j in range(4)], group)
    accepted = chunk_lanes([accepted_ref[...].astype(f32)] * 4, group)
    live = jnp.where(place < accepted, 1.0, 0.0)
    beta = strength * live
    g = decay * live
    gam = g + sum(jnp.where(place >= d, roll(g, 32 * d), 0.0) for d in (1, 2, 3))
    last = g + sum(roll(g, 32 * d) for d in (1, 2, 3))
    row = iota((128, 128), 0)
    column = iota((128, 128), 1)
    order = jnp.where(column == (row % 32) * 4 + row // 32, 1.0, 0.0).astype(bf16)
    keys = dot(order, key_rows, 1, 0).astype(bf16)
    gram = dot(keys, keys, 1, 1)

    def diagonal(d):
        return jnp.sum(jnp.where(row == column - 32 * d, gram, 0.0), axis=0, keepdims=True)

    unit = lax.rsqrt(diagonal(0) + epsilon)
    coupling = {
        d: jnp.where(
            place >= d,
            beta * diagonal(d) * unit * roll(unit, 32 * d) * jnp.exp(jnp.minimum(gam - roll(gam, 32 * d), 0.0)),
            0.0,
        )
        for d in (1, 2, 3)
    }
    flat = state.reshape(512, 128)
    high, low = split(flat)
    seen = dot(high, keys, 1, 1) + dot(low, keys, 1, 1)
    own = iota((32, 16, 128), 0) == iota((32, 16, 128), 2) % 32
    seen = jnp.sum(jnp.where(own, seen.reshape(32, 16, 128), 0.0), axis=0)
    update = solve(beta * (values - jnp.exp(gam) * unit * seen), coupling)
    update = update * (jnp.exp(last - gam) * unit)
    spread = jnp.where(own, jnp.broadcast_to(update[None], (32, 16, 128)), 0.0).reshape(512, 128)
    high, low = split(spread)
    change = dot(high, keys, 1, 0) + dot(low, keys, 1, 0)
    keep = jnp.where(iota((32, 128), 0) == iota((32, 128), 1), jnp.exp(last), 0.0)
    keep = jnp.sum(keep, axis=1, keepdims=True)
    keep = jnp.broadcast_to(jnp.broadcast_to(keep, (32, 128))[:, None, :], (32, 16, 128))
    return keep * state + change.reshape(32, 16, 128)


def new_state(state, keys, values, strengths, decays, accepted):
    return pl.pallas_call(
        state_kernel,
        grid=(8 // GROUPS,),
        in_specs=[
            pl.BlockSpec((32 * GROUPS, 16, 128), lambda i: (i, 0, 0)),
            pl.BlockSpec((128 * GROUPS, 128), lambda i: (i, 0)),
            pl.BlockSpec((4, 16, 256), lambda i: (0, 0, 0)),
            pl.BlockSpec((4, 1, 256), lambda i: (0, 0, 0)),
            pl.BlockSpec((4, 1, 256), lambda i: (0, 0, 0)),
            pl.BlockSpec((1, 256), lambda i: (0, 0)),
        ],
        out_specs=[
            pl.BlockSpec((32 * GROUPS, 16, 128), lambda i: (i, 0, 0)),
            pl.BlockSpec((512 * GROUPS, 128), lambda i: (i, 0)),
        ],
        out_shape=[
            jax.ShapeDtypeStruct((256, 16, 128), f32),
            jax.ShapeDtypeStruct((4096, 128), bf16),
        ],
        cost_estimate=cost(2000000000, 5 << 20),
        compiler_params=pltpu.CompilerParams(vmem_limit_bytes=VMEM_LIMIT),
        name="new_state",
    )(state, keys, values, strengths, decays, accepted)


def rows_kernel(
    x_ref, gain_ref, wq_ref, wk_ref, scalars_ref, *rest
):
    packs, (log_decay_ref, parent_ref, rate_ref, index_ref, high_ref, low_ref, pv_ref, gate_ref) = rest[:8], rest[8:]
    group = index_ref[0, 0]
    x = x_ref[...].astype(f32)
    scale = lax.rsqrt(jnp.mean(x * x, axis=0, keepdims=True) + epsilon)
    normed = (x * scale * gain_ref[...].astype(f32)).astype(bf16)

    def project(weight, dim):
        return dot(weight, normed, dim, 0)

    def rounded(x):
        return x.astype(bf16).astype(f32)

    queries = rounded(project(wq_ref[...], 0))
    keys = rounded(project(wk_ref[...], 0))
    logits = project(scalars_ref[...], 1)
    both = jnp.concatenate(
        [pack[0:16, :2048] for pack in packs] + [pack[16:32, :2048] for pack in packs], axis=0
    )
    both = rounded(project(both, 1))
    values, zgate = both[:128], both[128:]
    gain = jnp.concatenate([pack[16:32, 2048:] for pack in packs], axis=0).astype(f32)

    def unit(x):
        return x * lax.rsqrt(jnp.sum(x * x, axis=0, keepdims=True) + epsilon)

    queries = unit(queries) * 128**-0.5
    keys = unit(keys)
    beta = jax.nn.sigmoid(logits[0:1, :])
    pre = logits[1:2, :]
    softplus = jnp.maximum(pre, 0.0) + jnp.log1p(jnp.exp(-jnp.abs(pre)))
    log_decay = chunk_lanes([log_decay_ref[i] for i in range(4)], group)
    parent = chunk_lanes([parent_ref[i : i + 1, :].astype(f32) for i in range(4)], group)
    g = log_decay - rate_ref[0, 0] * softplus
    place = (iota((1, 128), 1) // 32).astype(f32)
    hit = {d: jnp.where((parent == place - d) & (place >= d), 1.0, 0.0) for d in (1, 2, 3)}
    seen = {1: hit[1]}
    seen[2] = hit[2] + hit[1] * roll(seen[1], 32)
    seen[3] = hit[3] + hit[1] * roll(seen[2], 32) + hit[2] * roll(seen[1], 64)
    gam = g + sum(seen[d] * roll(g, 32 * d) for d in (1, 2, 3))
    coupling, reach = {}, {0: jnp.sum(queries * keys, axis=0, keepdims=True)}
    for d in (1, 2, 3):
        earlier = roll(keys, 32 * d)
        weight = jnp.exp(jnp.minimum(gam - roll(gam, 32 * d), 0.0)) * seen[d]
        coupling[d] = beta * weight * jnp.sum(keys * earlier, axis=0, keepdims=True)
        reach[d] = weight * jnp.sum(queries * earlier, axis=0, keepdims=True)
    solved_values = solve(beta * values, coupling)
    solved_keys = solve((beta * jnp.exp(gam)) * keys, coupling)

    def reached(x):
        return reach[0] * x + sum(reach[d] * roll(x, 32 * d) for d in (1, 2, 3))

    probe = jnp.exp(gam) * queries - reached(solved_keys)
    high_ref[...], low_ref[...] = split(probe)
    pv_ref[...] = reached(solved_values)
    gate_ref[...] = gain * (zgate * jax.nn.sigmoid(zgate))


def vmem_specs(count):
    return [pl.BlockSpec(memory_space=pltpu.VMEM)] * count


def row_side(x, gain, wq, wk, scalars, packs, log_decay, parent, rate, index):
    return pl.pallas_call(
        rows_kernel,
        in_specs=vmem_specs(15) + [pl.BlockSpec(memory_space=pltpu.SMEM)] * 2,
        out_specs=vmem_specs(4),
        out_shape=[
            jax.ShapeDtypeStruct((128, 128), bf16),
            jax.ShapeDtypeStruct((128, 128), bf16),
            jax.ShapeDtypeStruct((128, 128), f32),
            jax.ShapeDtypeStruct((128, 128), f32),
        ],
        cost_estimate=cost(2000000000, 4 << 20),
        compiler_params=pltpu.CompilerParams(vmem_limit_bytes=VMEM_LIMIT),
        name="row_side",
    )(x, gain, wq, wk, scalars, *packs, log_decay, parent, rate, index)


def readout_kernel(state_ref, high_ref, low_ref, pv_ref, gate_ref, *rest):
    packs, (index_ref, out_ref) = rest[:8], rest[8:]
    index = index_ref[0, 0]
    own = iota((32, 16, 128), 0) == iota((32, 16, 128), 2) % 32
    pieces = []
    chip, core = index // 2, lax.rem(index, 2)
    for d in range(8):
        block = state_ref[2 * lax.rem(chip + d % 4, 4) + (core if d < 4 else 1 - core)]
        read = dot(block, high_ref[...], 1, 0) + dot(block, low_ref[...], 1, 0)
        pieces.append(jnp.sum(jnp.where(own, read.reshape(32, 16, 128), 0.0), axis=0))
    o = jnp.concatenate(pieces, axis=0) + pv_ref[...]
    o = o * lax.rsqrt(jnp.mean(o * o, axis=0, keepdims=True) + epsilon)
    o = (o * gate_ref[...]).astype(bf16)
    weight = jnp.concatenate([pack[32:48, :2048] for pack in packs], axis=0)
    out_ref[...] = dot(o, weight, 0, 0).astype(bf16)


def readout(state, high, low, pv, gate, packs, index):
    return pl.pallas_call(
        readout_kernel,
        in_specs=vmem_specs(13) + [pl.BlockSpec(memory_space=pltpu.SMEM)],
        out_specs=pl.BlockSpec(memory_space=pltpu.VMEM),
        out_shape=jax.ShapeDtypeStruct((128, 2048), bf16),
        cost_estimate=cost(500000000, 3 << 20),
        compiler_params=pltpu.CompilerParams(vmem_limit_bytes=VMEM_LIMIT),
        name="readout",
    )(state, high, low, pv, gate, *packs, index)


def total_kernel(part_ref, out_ref):
    total = jnp.sum(part_ref[...].astype(f32), axis=0)
    total = total * lax.rsqrt(jnp.mean(total * total, axis=1, keepdims=True) + epsilon)
    stacked = jnp.concatenate([total[:, 128 * c : 128 * c + 128] for c in range(16)], axis=0)
    out_ref[...] = stacked.T


def sum_heads(parts):
    return pl.pallas_call(
        total_kernel,
        in_specs=vmem_specs(1),
        out_specs=pl.BlockSpec(memory_space=pltpu.VMEM),
        out_shape=jax.ShapeDtypeStruct((128, 128), f32),
        cost_estimate=cost(1000000, 1 << 19),
        compiler_params=pltpu.CompilerParams(vmem_limit_bytes=VMEM_LIMIT),
        name="sum_heads",
    )(parts)


def final_kernel(x_ref, gain_ref, out_ref, scratch):
    scratch[...] = x_ref[...].T * gain_ref[...]
    lane = iota((1, 128), 1)
    rows = [scratch[pl.ds(r, 16, 8), :] for r in range(8)]
    blocks = []
    for i in range(4):
        halves = []
        for h in range(2):
            packed = None
            for q in range(4):
                shift = (32 * q - 32 * i) % 128
                moved = roll(rows[4 * h + q], shift) if shift else rows[4 * h + q]
                packed = moved if packed is None else jnp.where(lane // 32 == q, moved, packed)
            halves.append(packed)
        blocks.append(jnp.concatenate(halves, axis=1))
    full = jnp.concatenate(blocks, axis=0).astype(bf16)
    source = iota((256, 256), 0)
    target = iota((256, 256), 1)
    wanted = (source % 8) * 32 + ((source // 8) % 4) * 8 + source // 32
    order = jnp.where(wanted == target, 1.0, 0.0).astype(bf16)
    out_ref[...] = dot(full, order, 1, 0).astype(bf16).reshape(4, 16, 256)


def final_rows(x, gain):
    return pl.pallas_call(
        final_kernel,
        in_specs=vmem_specs(2),
        out_specs=pl.BlockSpec(memory_space=pltpu.VMEM),
        out_shape=jax.ShapeDtypeStruct((4, 16, 256), bf16),
        scratch_shapes=[pltpu.VMEM((128, 128), f32)],
        cost_estimate=cost(10000000, 1 << 18),
        compiler_params=pltpu.CompilerParams(vmem_limit_bytes=VMEM_LIMIT),
        name="final_rows",
    )(x, gain)


def chips(x):
    return [lax.ppermute(x, "tp", [((i + 2 * d) % 8, i) for i in range(8)]) for d in range(1, 4)]


def cores(arrays):
    return [lax.ppermute(x, "tp", [(i ^ 1, i) for i in range(8)]) for x in arrays]


def whole_step(
    tokens,
    input_norm_gain,
    query_weight,
    key_weight,
    value_weight,
    output_gate_weight,
    strength_weight,
    decay_weight,
    head_decay_rate,
    proposal_log_decay,
    head_norm_gain,
    output_weight,
    output_norm_gain,
    state,
    previous_keys,
    previous_values,
    previous_log_decay,
    previous_strengths,
    accepted,
    parent,
):
    tp = lax.axis_index("tp").astype(jnp.int32)
    index = tp.reshape(1, 1)

    sent = send_tokens(jnp.transpose(tokens, (1, 2, 0))).reshape(128, 16, 128)
    x = lax.all_to_all(sent, BOTH, 0, 0, tiled=True).reshape(2048, 128)

    value_rows = jnp.transpose(value_weight[:, 0, :], (1, 0))
    gate_rows = jnp.transpose(output_gate_weight[:, 0, :], (1, 0))
    gain_lanes = jnp.broadcast_to(head_norm_gain[:, None], (16, 128))
    output_rows = output_weight[0].reshape(16, 128, 16).transpose(0, 2, 1).reshape(16, 2048)
    pack = jnp.concatenate(
        [
            jnp.concatenate([value_rows, gate_rows, output_rows], axis=0),
            jnp.concatenate([gain_lanes] * 3, axis=0),
        ],
        axis=1,
    )
    near = [pack] + chips(pack)
    packs = near + cores(near)

    old_values = jnp.transpose(previous_values[:, :, 0, :], (1, 2, 0))
    accepted_state, low_state = new_state(
        state.reshape(256, 16, 128),
        previous_keys.reshape(1024, 128),
        old_values,
        jnp.transpose(previous_strengths, (1, 2, 0)),
        jnp.transpose(previous_log_decay, (1, 2, 0)),
        accepted.reshape(1, 256),
    )
    moved_state = lax.all_to_all(low_state.reshape(8, 512, 128), "tp", 0, 0, tiled=True)

    scalars = jnp.concatenate(
        [jnp.transpose(strength_weight, (1, 0)), jnp.transpose(decay_weight, (1, 0)), jnp.zeros((14, 2048), bf16)], axis=0
    )
    high, low, pv, gate = row_side(
        x,
        jnp.broadcast_to(input_norm_gain[:, None], (2048, 128)),
        query_weight,
        key_weight,
        scalars,
        packs,
        jnp.transpose(proposal_log_decay, (1, 2, 0)),
        jnp.transpose(parent, (1, 0)),
        head_decay_rate.reshape(1, 1),
        index,
    )
    part = readout(moved_state, high, low, pv, gate, packs, index)
    parts = lax.all_to_all(part.reshape(16, 8, 2048), "kv", 0, 0, tiled=True)
    blocks = lax.all_to_all(sum_heads(parts), BOTH, 0, 0, tiled=True)
    gain_rows = jnp.broadcast_to(jnp.repeat(output_norm_gain.astype(f32), 8)[:, None], (128, 128))
    out = final_rows(blocks, gain_rows)
    return jnp.transpose(out, (2, 0, 1)), accepted_state.reshape(state.shape)


def solution(mesh):
    placed = (
        P(None, None, ("kv", "tp")),
        P(),
        P(None, "kv"),
        P(None, "kv"),
        P(None, "kv", "tp"),
        P(None, "kv", "tp"),
        P(None, "kv"),
        P(None, "kv"),
        P("kv"),
        P(None, None, "kv"),
        P("tp"),
        P("kv", "tp", None),
        P(("kv", "tp")),
        P(None, "kv", "tp", None),
        P(None, None, "kv"),
        P(None, None, "kv", "tp"),
        P(None, None, "kv"),
        P(None, None, "kv"),
        P(),
        P(),
    )
    return jax.shard_map(
        whole_step,
        mesh=mesh,
        in_specs=placed,
        out_specs=(P(None, None, ("kv", "tp")), P(None, "kv", "tp", None)),
        check_vma=False,
    )
```

profile of v0, /device:TPU:1, one launch (start us, length us, event | category | flops | bytes accessed | tf_op | source)
XLA Modules:
  0.0 94.4 jit_solution(12318985193773901903)
XLA Ops:
  0.6 0.0 copy-start.10
  0.7 0.8 copy-done
  1.4 0.9 %send_tokens.1 = bf16[16,8,16,128]{3,2,1,0:T(8,128)(2,1)} custom-call(bf16[4,16,256]{2,1,0:T(8,128)(2,1)S(1)} %bitcast.42), custom_call_target="tpu_custom_call" | custom-call | flops 1000000 | bytes 524288 | tf_op jit(solution)/shard_map/send_tokens/pallas_call | solution.py:69
  2.4 11.5 %all-to-all-start.1 = ((bf16[128,16,128]{2,1,0:T(8,128)(2,1)}), bf16[128,16,128]{2,1,0:T(8,128)(2,1)S(1)}, u32[]{:S(2)}, u32[]{:S(2)}) async-start(bf16[128,16,128]{2,1,0:T(8,128)(2,1)} %bitcast.9), calls=%async_computation.1 | async-start | bytes 1048576 | tf_op jit(solution)/shard_map/all_to_all | solution.py:365
  13.9 1.2 %reshape_squeeze.3 = bf16[16,128,16]{2,1,0:T(8,128)(2,1)S(1)} reshape(bf16[1,16,2048]{2,1,0:T(8,128)(2,1)} %param.31) | data formatting | bytes 131072 | tf_op jit(solution)/shard_map/reshape;squeeze | solution.py:370
  15.1 0.2 copy.26
  15.4 0.0 copy-start.1
  15.4 1.6 %copy-done.1 = f32[256,1,16,128]{3,2,1,0:T(8,128)S(1)} copy-done((f32[256,1,16,128]{3,2,1,0:T(8,128)S(1)}, f32[256,1,16,128]{3,2,1,0:T(8,128)}, u32[]{:S(2)}) %copy-start.1) | copy-done | bytes 2097176
  17.0 6.8 %new_state.1 = (f32[256,16,128]{2,1,0:T(8,128)}, bf16[4096,128]{1,0:T(8,128)(2,1)}) custom-call(f32[256,16,128]{2,1,0:T(8,128)S(1)} %bitcast.43, bf16[1024,128]{1,0:T(8,128)(2,1)S(1)} %bitcast.44, bf16[4,16,256]{2,1,0:T(8,128)(2,1)S(1)} %bitcast.45, f32[4,1,256]{2,1,0:T(1,128)S(1)} %bitcast.46, f32[4,1,256]{2,1,0:T(1,128)S(1)} %bitcast.47, s32[1,256]{1,0:T(1,128)S(1)} %bitcast.50), custom_call_target="tpu_custom_call" | custom-call | flops 2000000000 | bytes 5242880 | tf_op jit(solution)/shard_map/new_state/pallas_call | solution.py:141
  23.8 0.0 copy-start.14
  23.8 0.0 copy-start.15
  23.8 0.0 copy-start.8
  23.8 0.0 copy-start.9
  23.8 3.7 %all-to-all-done.1 = bf16[128,16,128]{2,1,0:T(8,128)(2,1)S(1)} async-done(((bf16[128,16,128]{2,1,0:T(8,128)(2,1)}), bf16[128,16,128]{2,1,0:T(8,128)(2,1)S(1)}, u32[]{:S(2)}, u32[]{:S(2)}) %all-to-all-start.1) | async-done | bytes 524320 | tf_op jit(solution)/shard_map/all_to_all | solution.py:365
  27.5 4.4 %all-to-all-start = ((bf16[8,512,128]{2,1,0:T(8,128)(2,1)}), bf16[8,512,128]{2,1,0:T(8,128)(2,1)S(1)}, u32[]{:S(2)}, u32[]{:S(2)}) async-start(bf16[8,512,128]{2,1,0:T(8,128)(2,1)} %bitcast.7), calls=%async_computation | async-start | bytes 2097152 | tf_op jit(solution)/shard_map/all_to_all | solution.py:390
  31.9 0.1 broadcast_in_dim.27
  32.0 2.7 %collective-permute-start = (bf16[48,2176]{1,0:T(8,128)(2,1)S(1)}, bf16[48,2176]{1,0:T(8,128)(2,1)S(1)}, u32[]{:S(2)}, u32[]{:S(2)}) collective-permute-start(bf16[48,2176]{1,0:T(8,128)(2,1)S(1)} %maximum_maximum_fusion.rest_0_), channel_id=1, source_target_pairs={{2,0},{3,1},{4,2},{5,3},{6,4},{7,5},{0,6},{1,7},{10,8},{11,9},{12,... | collective-permute-start | bytes 626696 | tf_op jit(solution)/shard_map/ppermute | solution.py:332
  34.7 0.5 collective-permute-start.1
  35.2 0.6 collective-permute-start.2
  35.8 1.2 %collective-permute-start.3 = (bf16[48,2176]{1,0:T(8,128)(2,1)S(1)}, bf16[48,2176]{1,0:T(8,128)(2,1)S(1)}, u32[]{:S(2)}, u32[]{:S(2)}) collective-permute-start(bf16[48,2176]{1,0:T(8,128)(2,1)S(1)} %maximum_maximum_fusion.rest_0_), channel_id=1, source_target_pairs={{1,0},{0,1},{3,2},{2,3},{5,4},{4,5},{7,6},{6,7},{9,8},{8,9},{11,10... | collective-permute-start | bytes 626696 | tf_op jit(solution)/shard_map/ppermute | solution.py:336
  37.0 0.1 pad.8.clone
  37.1 12.8 %collective-permute-done.rest_1_ = bf16[48,2176]{1,0:T(8,128)(2,1)S(1)} collective-permute-done((bf16[48,2176]{1,0:T(8,128)(2,1)S(1)}, bf16[48,2176]{1,0:T(8,128)(2,1)S(1)}, u32[]{:S(2)}, u32[]{:S(2)}) %collective-permute-start) | collective-permute-done | bytes 208928 | tf_op jit(solution)/shard_map/ppermute | solution.py:332
  49.9 1.5 %collective-permute-start.4 = (bf16[48,2176]{1,0:T(8,128)(2,1)S(1)}, bf16[48,2176]{1,0:T(8,128)(2,1)S(1)}, u32[]{:S(2)}, u32[]{:S(2)}) collective-permute-start(bf16[48,2176]{1,0:T(8,128)(2,1)S(1)} %collective-permute-done.rest_1_), channel_id=1, source_target_pairs={{1,0},{0,1},{3,2},{2,3},{5,4},{4,5},{7,6},{6,7},{9,8},{8,9},{11,10... | collective-permute-start | bytes 626696 | tf_op jit(solution)/shard_map/ppermute | solution.py:336
  51.4 0.0 collective-permute-done.1.rest_2_
  51.4 1.5 %collective-permute-start.5 = (bf16[48,2176]{1,0:T(8,128)(2,1)S(1)}, bf16[48,2176]{1,0:T(8,128)(2,1)S(1)}, u32[]{:S(2)}, u32[]{:S(2)}) collective-permute-start(bf16[48,2176]{1,0:T(8,128)(2,1)S(1)} %collective-permute-done.1.rest_2_), channel_id=1, source_target_pairs={{1,0},{0,1},{3,2},{2,3},{5,4},{4,5},{7,6},{6,7},{9,8},{8,9},{11,10... | collective-permute-start | bytes 626696 | tf_op jit(solution)/shard_map/ppermute | solution.py:336
  52.9 2.8 %collective-permute-done.2.rest_3_ = bf16[48,2176]{1,0:T(8,128)(2,1)S(1)} collective-permute-done((bf16[48,2176]{1,0:T(8,128)(2,1)S(1)}, bf16[48,2176]{1,0:T(8,128)(2,1)S(1)}, u32[]{:S(2)}, u32[]{:S(2)}) %collective-permute-start.2) | collective-permute-done | bytes 208928 | tf_op jit(solution)/shard_map/ppermute | solution.py:332
  55.8 0.8 collective-permute-start.6
  56.5 0.1 maximum_maximum_fusion.1.scalars_ref
  57.3 0.0 collective-permute-done.3.rest_4_
  57.3 0.0 collective-permute-done.4.rest_5_
  57.3 0.0 collective-permute-done.5.rest_6_
  57.3 0.3 collective-permute-done.6.rest_7_
  57.6 0.3 broadcast_in_dim.12.gain_ref
  58.0 0.0 copy-start.2
  58.0 1.0 %copy-done.2 = bf16[2048,128]{1,0:T(8,128)(2,1)S(1)} copy-done((bf16[2048,128]{1,0:T(8,128)(2,1)S(1)}, bf16[2048,128]{1,0:T(8,128)(2,1)}, u32[]{:S(2)}) %copy-start.2) | copy-done | bytes 524312
  59.0 1.0 %copy-done.3 = bf16[2048,128]{1,0:T(8,128)(2,1)S(1)} copy-done((bf16[2048,128]{1,0:T(8,128)(2,1)S(1)}, bf16[2048,128]{1,0:T(8,128)(2,1)}, u32[]{:S(2)}) %copy-start.3) | copy-done | bytes 524312
  60.1 1.6 %row_side.1 = (bf16[128,128]{1,0:T(8,128)(2,1)S(1)}, bf16[128,128]{1,0:T(8,128)(2,1)S(1)}, f32[128,128]{1,0:T(8,128)S(1)}, f32[128,128]{1,0:T(8,128)S(1)}) custom-call(bf16[2048,128]{1,0:T(8,128)(2,1)S(1)} %bitcast.40, bf16[2048,128]{1,0:T(8,128)(2,1)S(1)} %broadcast_in_dim.12.gain_ref, bf16[2048,128]{1,0:T(8,128)(2,1)S(1)} %copy-done.2, ...), custom_call_target="tpu_custom_call" | custom-call | flops 2000000000 | bytes 4194304 | tf_op jit(solution)/shard_map/row_side/pallas_call | solution.py:231
  61.7 0.0 all-to-all-done.state_ref
  61.7 0.0 copy-start.17
  61.7 1.0 %readout.1 = bf16[128,2048]{1,0:T(8,128)(2,1)S(1)} custom-call(bf16[8,512,128]{2,1,0:T(8,128)(2,1)S(1)} %all-to-all-done.state_ref, bf16[128,128]{1,0:T(8,128)(2,1)S(1)} %get-tuple-element.9.high_ref, bf16[128,128]{1,0:T(8,128)(2,1)S(1)} %get-tuple-element.10.low_ref, f32[128,128]{1,0:T(8,128)S(1)} %get-tuple-element.11.pv_ref, ...), custom_call_target="tpu_custom_call" | custom-call | flops 500000000 | bytes 3145728 | tf_op jit(solution)/shard_map/readout/pallas_call | solution.py:265
  62.8 14.4 %all_to_all.26.part_ref = bf16[16,8,2048]{2,1,0:T(8,128)(2,1)S(1)} all-to-all(bf16[16,8,2048]{2,1,0:T(8,128)(2,1)S(1)} %bitcast.39), channel_id=1, replica_groups=mesh['kv'=16,'tp'=8] {'kv'}, dimensions={0} | all-to-all | bytes 1048576 | tf_op jit(solution)/shard_map/all_to_all | solution.py:408
  77.2 0.9 sum_heads.1
  78.1 5.6 %all-to-all-start.3 = ((f32[128,1,128]{2,1,0:T(1,128)}), f32[128,1,128]{2,1,0:T(1,128)S(1)}, u32[]{:S(2)}, u32[]{:S(2)}) async-start(f32[128,1,128]{2,1,0:T(1,128)} %bitcast.24), calls=%async_computation.3 | async-start | bytes 131072 | tf_op jit(solution)/shard_map/all_to_all | solution.py:409
  83.7 0.1 broadcast_in_dim.28
  83.8 0.1 broadcast_in_dim.29
  83.9 9.4 %all-to-all-done.3 = f32[128,1,128]{2,1,0:T(1,128)S(1)} async-done(((f32[128,1,128]{2,1,0:T(1,128)}), f32[128,1,128]{2,1,0:T(1,128)S(1)}, u32[]{:S(2)}, u32[]{:S(2)}) %all-to-all-start.3) | async-done | bytes 65568 | tf_op jit(solution)/shard_map/all_to_all | solution.py:409
  93.3 0.1 broadcast_in_dim.30.gain_ref
  93.4 1.0 %final_rows.1 = bf16[4,16,256]{2,1,0:T(8,128)(2,1)} custom-call(f32[128,128]{1,0:T(8,128)S(1)} %bitcast.41, f32[128,128]{1,0:T(8,128)S(1)} %broadcast_in_dim.30.gain_ref), custom_call_target="tpu_custom_call" | custom-call | flops 10000000 | bytes 262144 | tf_op jit(solution)/shard_map/final_rows/pallas_call | solution.py:319
  (27 shorter events, 0.1 us)
Async XLA Ops:
  0.6 14.7 %copy-start.10 = (s32[256]{0:T(256)S(1)}, s32[256]{0:T(256)}, u32[]{:S(2)}) copy-start(s32[256]{0:T(256)} %param.38) | copy-start | bytes 3076
  0.6 0.8 copy-start
  1.4 13.9 %copy-start.4 = (bf16[256,4,128]{2,1,0:T(4,128)(2,1)S(1)}, bf16[256,4,128]{2,1,0:T(4,128)(2,1)}, u32[]{:S(2)}) copy-start(bf16[256,4,128]{2,1,0:T(4,128)(2,1)} %param.34) | copy-start | bytes 786436
  1.4 14.0 %copy-start.5 = (bf16[256,4,1,16]{0,3,2,1:T(8,128)(2,1)S(1)}, bf16[256,4,1,16]{0,3,2,1:T(8,128)(2,1)}, u32[]{:S(2)}) copy-start(bf16[256,4,1,16]{0,3,2,1:T(8,128)(2,1)} %param.35) | copy-start | bytes 98308
  1.4 14.0 %copy-start.6 = (f32[256,4,1]{0,2,1:T(1,128)S(1)}, f32[256,4,1]{0,2,1:T(1,128)}, u32[]{:S(2)}) copy-start(f32[256,4,1]{0,2,1:T(1,128)} %param.37) | copy-start | bytes 12292
  1.4 14.0 %copy-start.7 = (f32[256,4,1]{0,2,1:T(1,128)S(1)}, f32[256,4,1]{0,2,1:T(1,128)}, u32[]{:S(2)}) copy-start(f32[256,4,1]{0,2,1:T(1,128)} %param.36) | copy-start | bytes 12292
  2.4 25.1 %all-to-all-start.1 = ((bf16[128,16,128]{2,1,0:T(8,128)(2,1)}), bf16[128,16,128]{2,1,0:T(8,128)(2,1)S(1)}, u32[]{:S(2)}, u32[]{:S(2)}) async-start(bf16[128,16,128]{2,1,0:T(8,128)(2,1)} %bitcast.9), calls=%async_computation.1 | async-start | bytes 1048576 | tf_op jit(solution)/shard_map/all_to_all | solution.py:365
  15.4 1.6 %copy-start.1 = (f32[256,1,16,128]{3,2,1,0:T(8,128)S(1)}, f32[256,1,16,128]{3,2,1,0:T(8,128)}, u32[]{:S(2)}) copy-start(f32[256,1,16,128]{3,2,1,0:T(8,128)} %param.33) | copy-start | bytes 6291460
  23.7 8.2 %copy-start.16 = (bf16[16]{0:T(256)(128)(2,1)S(1)}, bf16[16]{0:T(256)(128)(2,1)}, u32[]{:S(2)}) copy-start(bf16[16]{0:T(256)(128)(2,1)} %param.30) | copy-start | bytes 100
  23.7 8.2 %copy-start.11 = (bf16[2048,1,16]{0,2,1:T(8,128)(2,1)S(1)}, bf16[2048,1,16]{0,2,1:T(8,128)(2,1)}, u32[]{:S(2)}) copy-start(bf16[2048,1,16]{0,2,1:T(8,128)(2,1)} %param.25) | copy-start | bytes 196612
  23.7 8.2 %copy-start.12 = (bf16[2048,1,16]{0,2,1:T(8,128)(2,1)S(1)}, bf16[2048,1,16]{0,2,1:T(8,128)(2,1)}, u32[]{:S(2)}) copy-start(bf16[2048,1,16]{0,2,1:T(8,128)(2,1)} %param.24) | copy-start | bytes 196612
  23.7 32.8 %copy-start.13 = (bf16[2048,1]{0,1:T(2,128)(2,1)S(1)}, bf16[2048,1]{0,1:T(2,128)(2,1)}, u32[]{:S(2)}) copy-start(bf16[2048,1]{0,1:T(2,128)(2,1)} %param.27) | copy-start | bytes 12292
  23.8 32.8 %copy-start.14 = (bf16[2048,1]{0,1:T(2,128)(2,1)S(1)}, bf16[2048,1]{0,1:T(2,128)(2,1)}, u32[]{:S(2)}) copy-start(bf16[2048,1]{0,1:T(2,128)(2,1)} %param.26) | copy-start | bytes 12292
  23.8 33.9 %copy-start.15 = (bf16[2048]{0:T(1024)(128)(2,1)S(1)}, bf16[2048]{0:T(1024)(128)(2,1)}, u32[]{:S(2)}) copy-start(bf16[2048]{0:T(1024)(128)(2,1)} %param.21) | copy-start | bytes 12292
  23.8 34.2 %copy-start.8 = (f32[256,4,1]{0,2,1:T(1,128)S(1)}, f32[256,4,1]{0,2,1:T(1,128)}, u32[]{:S(2)}) copy-start(f32[256,4,1]{0,2,1:T(1,128)} %param.29) | copy-start | bytes 12292
  23.8 34.2 %copy-start.9 = (s32[256,4]{0,1:T(4,128)S(1)}, s32[256,4]{0,1:T(4,128)}, u32[]{:S(2)}) copy-start(s32[256,4]{0,1:T(4,128)} %param.39) | copy-start | bytes 12292
  27.5 34.2 %all-to-all-start = ((bf16[8,512,128]{2,1,0:T(8,128)(2,1)}), bf16[8,512,128]{2,1,0:T(8,128)(2,1)S(1)}, u32[]{:S(2)}, u32[]{:S(2)}) async-start(bf16[8,512,128]{2,1,0:T(8,128)(2,1)} %bitcast.7), calls=%async_computation | async-start | bytes 2097152 | tf_op jit(solution)/shard_map/all_to_all | solution.py:390
  32.0 17.9 %collective-permute-start = (bf16[48,2176]{1,0:T(8,128)(2,1)S(1)}, bf16[48,2176]{1,0:T(8,128)(2,1)S(1)}, u32[]{:S(2)}, u32[]{:S(2)}) collective-permute-start(bf16[48,2176]{1,0:T(8,128)(2,1)S(1)} %maximum_maximum_fusion.rest_0_), channel_id=1, source_target_pairs={{2,0},{3,1},{4,2},{5,3},{6,4},{7,5},{0,6},{1,7},{10,8},{11,9},{12,... | collective-permute-start | bytes 626696 | tf_op jit(solution)/shard_map/ppermute | solution.py:332
  34.7 16.8 %collective-permute-start.1 = (bf16[48,2176]{1,0:T(8,128)(2,1)S(1)}, bf16[48,2176]{1,0:T(8,128)(2,1)S(1)}, u32[]{:S(2)}, u32[]{:S(2)}) collective-permute-start(bf16[48,2176]{1,0:T(8,128)(2,1)S(1)} %maximum_maximum_fusion.rest_0_), channel_id=1, source_target_pairs={{4,0},{5,1},{6,2},{7,3},{0,4},{1,5},{2,6},{3,7},{12,8},{13,9},{14,... | collective-permute-start | bytes 626696 | tf_op jit(solution)/shard_map/ppermute | solution.py:332
  35.2 20.5 %collective-permute-start.2 = (bf16[48,2176]{1,0:T(8,128)(2,1)S(1)}, bf16[48,2176]{1,0:T(8,128)(2,1)S(1)}, u32[]{:S(2)}, u32[]{:S(2)}) collective-permute-start(bf16[48,2176]{1,0:T(8,128)(2,1)S(1)} %maximum_maximum_fusion.rest_0_), channel_id=1, source_target_pairs={{6,0},{7,1},{0,2},{1,3},{2,4},{3,5},{4,6},{5,7},{14,8},{15,9},{8,1... | collective-permute-start | bytes 626696 | tf_op jit(solution)/shard_map/ppermute | solution.py:332
  35.8 21.5 %collective-permute-start.3 = (bf16[48,2176]{1,0:T(8,128)(2,1)S(1)}, bf16[48,2176]{1,0:T(8,128)(2,1)S(1)}, u32[]{:S(2)}, u32[]{:S(2)}) collective-permute-start(bf16[48,2176]{1,0:T(8,128)(2,1)S(1)} %maximum_maximum_fusion.rest_0_), channel_id=1, source_target_pairs={{1,0},{0,1},{3,2},{2,3},{5,4},{4,5},{7,6},{6,7},{9,8},{8,9},{11,10... | collective-permute-start | bytes 626696 | tf_op jit(solution)/shard_map/ppermute | solution.py:336
  49.9 7.4 %collective-permute-start.4 = (bf16[48,2176]{1,0:T(8,128)(2,1)S(1)}, bf16[48,2176]{1,0:T(8,128)(2,1)S(1)}, u32[]{:S(2)}, u32[]{:S(2)}) collective-permute-start(bf16[48,2176]{1,0:T(8,128)(2,1)S(1)} %collective-permute-done.rest_1_), channel_id=1, source_target_pairs={{1,0},{0,1},{3,2},{2,3},{5,4},{4,5},{7,6},{6,7},{9,8},{8,9},{11,10... | collective-permute-start | bytes 626696 | tf_op jit(solution)/shard_map/ppermute | solution.py:336
  51.4 5.9 %collective-permute-start.5 = (bf16[48,2176]{1,0:T(8,128)(2,1)S(1)}, bf16[48,2176]{1,0:T(8,128)(2,1)S(1)}, u32[]{:S(2)}, u32[]{:S(2)}) collective-permute-start(bf16[48,2176]{1,0:T(8,128)(2,1)S(1)} %collective-permute-done.1.rest_2_), channel_id=1, source_target_pairs={{1,0},{0,1},{3,2},{2,3},{5,4},{4,5},{7,6},{6,7},{9,8},{8,9},{11,10... | collective-permute-start | bytes 626696 | tf_op jit(solution)/shard_map/ppermute | solution.py:336
  55.8 1.9 %collective-permute-start.6 = (bf16[48,2176]{1,0:T(8,128)(2,1)S(1)}, bf16[48,2176]{1,0:T(8,128)(2,1)S(1)}, u32[]{:S(2)}, u32[]{:S(2)}) collective-permute-start(bf16[48,2176]{1,0:T(8,128)(2,1)S(1)} %collective-permute-done.2.rest_3_), channel_id=1, source_target_pairs={{1,0},{0,1},{3,2},{2,3},{5,4},{4,5},{7,6},{6,7},{9,8},{8,9},{11,10... | collective-permute-start | bytes 626696 | tf_op jit(solution)/shard_map/ppermute | solution.py:336
  58.0 1.0 %copy-start.2 = (bf16[2048,128]{1,0:T(8,128)(2,1)S(1)}, bf16[2048,128]{1,0:T(8,128)(2,1)}, u32[]{:S(2)}) copy-start(bf16[2048,128]{1,0:T(8,128)(2,1)} %wq_ref.1) | copy-start | bytes 1572868
  59.0 1.0 %copy-start.3 = (bf16[2048,128]{1,0:T(8,128)(2,1)S(1)}, bf16[2048,128]{1,0:T(8,128)(2,1)}, u32[]{:S(2)}) copy-start(bf16[2048,128]{1,0:T(8,128)(2,1)} %wk_ref.1) | copy-start | bytes 1572868
  61.7 22.0 %copy-start.17 = (bf16[16]{0:T(256)(128)(2,1)S(1)}, bf16[16]{0:T(256)(128)(2,1)}, u32[]{:S(2)}) copy-start(bf16[16]{0:T(256)(128)(2,1)} %param.32) | copy-start | bytes 100
  78.1 15.3 %all-to-all-start.3 = ((f32[128,1,128]{2,1,0:T(1,128)}), f32[128,1,128]{2,1,0:T(1,128)S(1)}, u32[]{:S(2)}, u32[]{:S(2)}) async-start(f32[128,1,128]{2,1,0:T(1,128)} %bitcast.24), calls=%async_computation.3 | async-start | bytes 131072 | tf_op jit(solution)/shard_map/all_to_all | solution.py:409
where the time goes:
time: 94.9 us; the launch traced here: 94.4 us
  starting transfers between devices  30.4 us (32%)
  waiting for transfers between devices  29 us (31%)
  blocking collectives  14.4 us (15%)
  Pallas kernels  12.3 us (13%)
  local copies, waits for them, and re-layouts  6.67 us (7%)
  between operations  1.54 us (2%)
    ppermute x3, waiting for transfers between devices, chips(): lax.ppermute(x, 'tp', [((i + 2 * d) % 8, i) for i in range(8)])  15.6 us
    all_to_all x1, blocking collectives, whole_step(): parts = lax.all_to_all(part.reshape(16, 8, 2048), 'kv', 0, 0, tiled=True)  14.4 us
    all_to_all x1, starting transfers between devices, whole_step(): x = lax.all_to_all(sent, BOTH, 0, 0, tiled=True).reshape(2048, 128)  11.5 us
    all_to_all x1, waiting for transfers between devices, whole_step(): blocks = lax.all_to_all(sum_heads(parts), BOTH, 0, 0, tiled=True)  9.43 us
    pallas_call x1, Pallas kernels, new_state(): pl.pallas_call(state_kernel, grid=(8 // GROUPS,), in_specs=[pl.BlockSpec(...  6.75 us
    all_to_all x1, starting transfers between devices, whole_step(): blocks = lax.all_to_all(sum_heads(parts), BOTH, 0, 0, tiled=True)  5.64 us
    ppermute x4, starting transfers between devices, cores(): lax.ppermute(x, 'tp', [(i ^ 1, i) for i in range(8)])  5.05 us
    unnamed x37, local copies, waits for them, and re-layouts  4.51 us
  transfers between devices with their start and end apart: 10, of which 5 were waited for; matrix products, arithmetic and copies ran while one was open for 2% of the time, Pallas kernels for 9%

commit v1 on v0

v1 whole, which is shorter than its diff:
```python
import jax
import jax.numpy as jnp
from jax import lax
from jax.experimental import pallas as pl
from jax.experimental.pallas import tpu as pltpu
from jax.sharding import PartitionSpec as P


epsilon = 1e-06
f32 = jnp.float32
bf16 = jnp.bfloat16
BOTH = ("kv", "tp")
VMEM_LIMIT = 16 << 20
PACK = 784


def dot(a, b, ca, cb):
    return lax.dot_general(a, b, (((ca,), (cb,)), ((), ())), preferred_element_type=f32)


def iota(shape, dim):
    return lax.broadcasted_iota(jnp.int32, shape, dim)


def roll(x, shift):
    return pltpu.roll(x, shift, 1)


def split(x):
    hi = x.astype(bf16)
    return hi, (x - hi.astype(f32)).astype(bf16)


def cost(flops, size):
    return pl.CostEstimate(flops=flops, bytes_accessed=size, transcendentals=0)


def chunk_lanes(rows, group):
    lane = iota((1, 128), 1)
    packed = None
    for j in range(4):
        if isinstance(group, int):
            half = rows[j][:, 128 * (group // 4) : 128 * (group // 4) + 128]
            shift = (32 * j - 32 * (group % 4)) % 128
            moved = roll(half, shift) if shift else half
        else:
            half = jnp.where(group >= 4, rows[j][:, 128:], rows[j][:, :128])
            moved = roll(half, lax.rem(32 * j + 128 - 32 * lax.rem(group, 4), 128))
        packed = moved if packed is None else jnp.where(lane // 32 == j, moved, packed)
    return packed


def solve(rhs, coupling):
    x = rhs
    for _ in range(3):
        x = rhs - sum(coupling[d] * roll(x, 32 * d) for d in (1, 2, 3))
    return x


def hbm_specs(count):
    return [pl.BlockSpec(memory_space=pltpu.HBM)] * count


def vmem_specs(count):
    return [pl.BlockSpec(memory_space=pltpu.VMEM)] * count


def start_all(copies):
    for copy in copies:
        copy.start()


def wait_all(copies):
    for copy in copies:
        copy.wait()


def copies_in(sources, targets, sems):
    return [pltpu.make_async_copy(x, y, sems.at[i]) for i, (x, y) in enumerate(zip(sources, targets))]


def in_hbm(arrays):
    return [pltpu.with_memory_space_constraint(x, pltpu.HBM) for x in arrays]


def scratch_like(arrays):
    return [pltpu.VMEM(x.shape, x.dtype) for x in arrays] + [pltpu.SemaphoreType.DMA((len(arrays),))]


def prepare_kernel(*refs):
    sources, (sent_ref, pack_ref), held, sems = refs[:5], refs[5:7], refs[7:12], refs[12]
    copies = copies_in(sources, held, sems)
    start_all(copies)
    wait_all(copies[1:])
    pack_weights(*held[1:], pack_ref)
    copies[0].wait()
    rows = [held[0][i].astype(f32) for i in range(4)]
    for t in range(8):
        block = chunk_lanes(rows, t).astype(bf16)
        for k in range(16):
            sent_ref[k, t] = block


def prepare(*arrays):
    return pl.pallas_call(
        prepare_kernel,
        in_specs=hbm_specs(5),
        out_specs=vmem_specs(2),
        out_shape=[pltpu.VMEM((16, 8, 16, 128), bf16), pltpu.VMEM((PACK, 128), bf16)],
        scratch_shapes=scratch_like(arrays),
        cost_estimate=cost(10000000, 1 << 20),
        compiler_params=pltpu.CompilerParams(vmem_limit_bytes=VMEM_LIMIT),
        name="prepare",
    )(*in_hbm(arrays))


def stack(rows):
    return jnp.concatenate(rows, axis=0)


def spread_rows(x):
    return jnp.broadcast_to(x[:, None, :], (8, 16, 128)).reshape(128, 128)


def state_kernel(*refs):
    state_source, sources, state_out, lows, state_ref, held, (sems, state_sems) = (
        refs[0], refs[1:6], refs[6], refs[7:11], refs[11], refs[12:17], refs[17:],
    )
    key_ref, value_ref, strength_ref, decay_ref, accepted_ref = held
    chip = lax.axis_index("tp") // 2
    groups = [2 * lax.rem(chip + step // 2, 4) + step % 2 for step in range(8)]

    def rows_of(step, count=1):
        return pl.ds(pl.multiple_of(32 * groups[step], 32), 32 * count)

    copies = copies_in(sources, held, sems)
    loads = [
        pltpu.make_async_copy(state_source.at[rows_of(2 * i, 2)], state_ref.at[rows_of(2 * i, 2)], state_sems.at[0, i])
        for i in range(4)
    ]
    stores = [
        pltpu.make_async_copy(state_ref.at[rows_of(2 * i, 2)], state_out.at[rows_of(2 * i, 2)], state_sems.at[1, i])
        for i in range(4)
    ]
    start_all(copies + loads)
    wait_all(copies)

    lane = iota((1, 128), 1)
    place = lane // 32
    strength = stack([chunk_lanes([strength_ref[j] for j in range(4)], x) for x in groups])
    decay = stack([chunk_lanes([decay_ref[j] for j in range(4)], x) for x in groups])
    accepted = stack([chunk_lanes([accepted_ref[...].astype(f32)] * 4, x) for x in groups])
    values = [value_ref[j].astype(f32) for j in range(4)]
    values = stack([chunk_lanes(values, x) for x in groups])
    live = jnp.where(place < accepted, 1.0, 0.0)
    beta = strength * live
    g = decay * live
    gam = g + sum(jnp.where(place >= d, roll(g, 32 * d), 0.0) for d in (1, 2, 3))
    last = g + sum(roll(g, 32 * d) for d in (1, 2, 3))
    row = iota((128, 128), 0)
    column = iota((128, 128), 1)
    order = jnp.where(column == (row % 32) * 4 + row // 32, 1.0, 0.0).astype(bf16)
    keys = [dot(order, key_ref[pl.ds(pl.multiple_of(128 * x, 128), 128), :], 1, 0).astype(bf16) for x in groups]
    grams = [dot(x, x, 1, 1) for x in keys]

    def diagonal(d):
        return stack(
            [jnp.sum(jnp.where(row == column - 32 * d, gram, 0.0), axis=0, keepdims=True) for gram in grams]
        )

    unit = lax.rsqrt(diagonal(0) + epsilon)
    coupling = {
        d: jnp.where(
            place >= d,
            beta * diagonal(d) * unit * roll(unit, 32 * d) * jnp.exp(jnp.minimum(gam - roll(gam, 32 * d), 0.0)),
            0.0,
        )
        for d in (1, 2, 3)
    }
    coupling = {d: spread_rows(x) for d, x in coupling.items()}
    own = iota((32, 16, 128), 0) == iota((32, 16, 128), 2) % 32
    seen = []
    for step in range(8):
        if step % 2 == 0:
            loads[step // 2].wait()
        high, low = split(state_ref[rows_of(step)].reshape(512, 128))
        read = dot(high, keys[step], 1, 1) + dot(low, keys[step], 1, 1)
        seen.append(jnp.sum(jnp.where(own, read.reshape(32, 16, 128), 0.0), axis=0))
    update = solve(spread_rows(beta) * values - spread_rows(beta * jnp.exp(gam) * unit) * stack(seen), coupling)
    update = update * spread_rows(jnp.exp(last - gam) * unit)
    keep = jnp.exp(last)
    for step in range(8):
        spread = jnp.broadcast_to(update[16 * step : 16 * step + 16][None], (32, 16, 128))
        high, low = split(jnp.where(own, spread, 0.0).reshape(512, 128))
        change = dot(high, keys[step], 1, 0) + dot(low, keys[step], 1, 0)
        kept = jnp.where(iota((32, 128), 0) == iota((32, 128), 1), keep[step : step + 1], 0.0)
        kept = jnp.broadcast_to(jnp.sum(kept, axis=1, keepdims=True), (32, 128))
        kept = jnp.broadcast_to(kept[:, None, :], (32, 16, 128))
        new = kept * state_ref[rows_of(step)] + change.reshape(32, 16, 128)
        state_ref[rows_of(step)] = new
        lows[step // 2][512 * (step % 2) : 512 * (step % 2) + 512, :] = new.reshape(512, 128).astype(bf16)
        if step % 2 == 1:
            stores[step // 2].start()
    wait_all(stores)


def new_state(state, *arrays):
    return pl.pallas_call(
        state_kernel,
        in_specs=hbm_specs(6),
        out_specs=hbm_specs(1) + vmem_specs(4),
        out_shape=[pltpu.HBM((256, 16, 128), f32)] + [pltpu.VMEM((1024, 128), bf16)] * 4,
        scratch_shapes=[pltpu.VMEM((256, 16, 128), f32), *scratch_like(arrays), pltpu.SemaphoreType.DMA((2, 4))],
        cost_estimate=cost(2000000000, 5 << 20),
        compiler_params=pltpu.CompilerParams(vmem_limit_bytes=VMEM_LIMIT),
        name="new_state",
    )(*in_hbm((state, *arrays)))


def pack_weights(value_ref, gate_ref, output_ref, gain_ref, pack_ref):
    row = iota((16, 16), 0)
    gain = jnp.where(row == iota((16, 16), 1), jnp.broadcast_to(gain_ref[...].astype(f32), (16, 16)), 0.0)
    gain = jnp.broadcast_to(jnp.sum(gain, axis=1, keepdims=True), (16, 128)).astype(bf16)
    source = iota((128, 128), 0)
    target = iota((128, 128), 1)
    order = jnp.where(target == (source % 16) * 8 + source // 16, 1.0, 0.0).astype(bf16)
    rows = jnp.concatenate([output_ref[:, 128 * b : 128 * b + 128] for b in range(16)], axis=0)
    rows = dot(rows, order, 1, 0)
    lane = iota((1, 128), 1)
    for c in range(16):
        packed = None
        for b in range(16):
            piece = rows[16 * b : 16 * b + 16, :]
            shift = (8 * (b - c)) % 128
            moved = roll(piece, shift) if shift else piece
            packed = moved if packed is None else jnp.where(lane // 8 == b, moved, packed)
        columns = slice(128 * c, 128 * c + 128)
        block = jnp.concatenate([value_ref[:, columns], gate_ref[:, columns], packed.astype(bf16)], axis=0)
        pack_ref[48 * c : 48 * c + 48, :] = block
    pack_ref[768:, :] = gain


def weight_rows(packs, first):
    return jnp.concatenate(
        [
            jnp.concatenate([x[48 * b + first : 48 * b + first + 16, :] for x in packs], axis=0)
            for b in range(16)
        ],
        axis=1,
    )


def rows_kernel(x_ref, *refs):
    packs, rate_ref, sources, rest = refs[:8], refs[8], refs[9:16], refs[16:]
    (high_ref, low_ref, pv_ref, gate_ref), held, sems = rest[:4], rest[4:11], rest[11]
    gain_ref, wq_ref, wk_ref, strength_ref, decay_ref, log_decay_ref, parent_ref = held
    copies = copies_in(sources, held, sems)
    start_all(copies)
    wait_all(copies)
    group = lax.axis_index("tp")
    x = x_ref[...].astype(f32)
    scale = lax.rsqrt(jnp.mean(x * x, axis=0, keepdims=True) + epsilon)
    column = iota((128, 128), 1) == iota((128, 128), 0)
    gain = jnp.concatenate(
        [jnp.where(column, gain_ref[b : b + 1, :].astype(f32), 0.0).astype(bf16) for b in range(16)], axis=0
    )
    gain = dot(gain, jnp.ones((128, 128), bf16), 1, 0)
    normed = (x * scale * gain).astype(bf16)

    def project(weight, dim):
        return dot(weight, normed, dim, 0)

    def rounded(x):
        return x.astype(bf16).astype(f32)

    queries = rounded(project(wq_ref[...], 0))
    keys = rounded(project(wk_ref[...], 0))
    first = iota((16, 2048), 0) == 0
    scalars = jnp.where(first, strength_ref[...].astype(f32), decay_ref[...].astype(f32))
    logits = project(scalars.astype(bf16), 1)
    both = jnp.concatenate([weight_rows(packs, 0), weight_rows(packs, 16)], axis=0)
    both = rounded(project(both, 1))
    values, zgate = both[:128], both[128:]
    gain = jnp.concatenate([pack[768:, :] for pack in packs], axis=0).astype(f32)

    def unit(x):
        return x * lax.rsqrt(jnp.sum(x * x, axis=0, keepdims=True) + epsilon)

    queries = unit(queries) * 128**-0.5
    keys = unit(keys)
    beta = jax.nn.sigmoid(logits[0:1, :])
    pre = logits[1:2, :]
    softplus = jnp.maximum(pre, 0.0) + jnp.log1p(jnp.exp(-jnp.abs(pre)))
    log_decay = chunk_lanes([log_decay_ref[i] for i in range(4)], group)
    parent = chunk_lanes([parent_ref[i : i + 1, :].astype(f32) for i in range(4)], group)
    g = log_decay - rate_ref[0, 0] * softplus
    place = (iota((1, 128), 1) // 32).astype(f32)
    hit = {d: jnp.where((parent == place - d) & (place >= d), 1.0, 0.0) for d in (1, 2, 3)}
    seen = {1: hit[1]}
    seen[2] = hit[2] + hit[1] * roll(seen[1], 32)
    seen[3] = hit[3] + hit[1] * roll(seen[2], 32) + hit[2] * roll(seen[1], 64)
    gam = g + sum(seen[d] * roll(g, 32 * d) for d in (1, 2, 3))
    coupling, reach = {}, {0: jnp.sum(queries * keys, axis=0, keepdims=True)}
    for d in (1, 2, 3):
        earlier = roll(keys, 32 * d)
        weight = jnp.exp(jnp.minimum(gam - roll(gam, 32 * d), 0.0)) * seen[d]
        coupling[d] = beta * weight * jnp.sum(keys * earlier, axis=0, keepdims=True)
        reach[d] = weight * jnp.sum(queries * earlier, axis=0, keepdims=True)
    solved_values = solve(beta * values, coupling)
    solved_keys = solve((beta * jnp.exp(gam)) * keys, coupling)

    def reached(x):
        return reach[0] * x + sum(reach[d] * roll(x, 32 * d) for d in (1, 2, 3))

    probe = jnp.exp(gam) * queries - reached(solved_keys)
    high_ref[...], low_ref[...] = split(probe)
    pv_ref[...] = reached(solved_values)
    gate_ref[...] = gain * (zgate * jax.nn.sigmoid(zgate))


def row_side(x, packs, rate, *arrays):
    return pl.pallas_call(
        rows_kernel,
        in_specs=vmem_specs(9) + [pl.BlockSpec(memory_space=pltpu.SMEM)] + hbm_specs(7),
        out_specs=vmem_specs(4),
        out_shape=[
            pltpu.VMEM((128, 128), bf16),
            pltpu.VMEM((128, 128), bf16),
            pltpu.VMEM((128, 128), f32),
            pltpu.VMEM((128, 128), f32),
        ],
        scratch_shapes=scratch_like(arrays),
        cost_estimate=cost(2000000000, 4 << 20),
        compiler_params=pltpu.CompilerParams(vmem_limit_bytes=VMEM_LIMIT),
        name="row_side",
    )(x, *packs, rate, *in_hbm(arrays))


def readout_kernel(high_ref, low_ref, pv_ref, gate_ref, *rest):
    packs, states, out_ref = rest[:8], rest[8:16], rest[16]
    core = lax.rem(lax.axis_index("tp"), 2)
    own = iota((32, 16, 128), 0) == iota((32, 16, 128), 2) % 32
    pieces = []
    for state in states:
        block = state[pl.ds(pl.multiple_of(512 * core, 512), 512), :]
        read = dot(block, high_ref[...], 1, 0) + dot(block, low_ref[...], 1, 0)
        pieces.append(jnp.sum(jnp.where(own, read.reshape(32, 16, 128), 0.0), axis=0))
    o = jnp.concatenate(pieces, axis=0) + pv_ref[...]
    o = o * lax.rsqrt(jnp.mean(o * o, axis=0, keepdims=True) + epsilon)
    o = (o * gate_ref[...]).astype(bf16)
    out_ref[...] = dot(o, weight_rows(packs, 32), 0, 0).astype(bf16)


def readout(high, low, pv, gate, packs, states):
    return pl.pallas_call(
        readout_kernel,
        in_specs=vmem_specs(20),
        out_specs=pl.BlockSpec(memory_space=pltpu.VMEM),
        out_shape=pltpu.VMEM((128, 2048), bf16),
        cost_estimate=cost(500000000, 3 << 20),
        compiler_params=pltpu.CompilerParams(vmem_limit_bytes=VMEM_LIMIT),
        name="readout",
    )(high, low, pv, gate, *packs, *states)


def total_kernel(part_ref, out_ref):
    total = jnp.sum(part_ref[...].astype(f32), axis=0)
    total = total * lax.rsqrt(jnp.mean(total * total, axis=1, keepdims=True) + epsilon)
    stacked = jnp.concatenate([total[:, 128 * c : 128 * c + 128] for c in range(16)], axis=0)
    out_ref[...] = stacked.T


def sum_heads(parts):
    return pl.pallas_call(
        total_kernel,
        in_specs=vmem_specs(1),
        out_specs=pl.BlockSpec(memory_space=pltpu.VMEM),
        out_shape=pltpu.VMEM((128, 128), f32),
        cost_estimate=cost(1000000, 1 << 19),
        compiler_params=pltpu.CompilerParams(vmem_limit_bytes=VMEM_LIMIT),
        name="sum_heads",
    )(parts)


def final_kernel(x_ref, gain_ref, out_ref, scratch):
    place = iota((128, 16), 0) // 8 == iota((128, 16), 1)
    gain = jnp.sum(jnp.where(place, gain_ref[...].astype(f32), 0.0), axis=1, keepdims=True)
    scratch[...] = x_ref[...].T * gain
    lane = iota((1, 128), 1)
    rows = [scratch[pl.ds(r, 16, 8), :] for r in range(8)]
    blocks = []
    for i in range(4):
        halves = []
        for h in range(2):
            packed = None
            for q in range(4):
                shift = (32 * q - 32 * i) % 128
                moved = roll(rows[4 * h + q], shift) if shift else rows[4 * h + q]
                packed = moved if packed is None else jnp.where(lane // 32 == q, moved, packed)
            halves.append(packed)
        blocks.append(jnp.concatenate(halves, axis=1))
    full = jnp.concatenate(blocks, axis=0).astype(bf16)
    source = iota((256, 256), 0)
    target = iota((256, 256), 1)
    wanted = (source % 8) * 32 + ((source // 8) % 4) * 8 + source // 32
    order = jnp.where(wanted == target, 1.0, 0.0).astype(bf16)
    out_ref[...] = dot(full, order, 1, 0).astype(bf16).reshape(4, 16, 256)


def final_rows(x, gain):
    return pl.pallas_call(
        final_kernel,
        in_specs=vmem_specs(2),
        out_specs=pl.BlockSpec(memory_space=pltpu.VMEM),
        out_shape=jax.ShapeDtypeStruct((4, 16, 256), bf16),
        scratch_shapes=[pltpu.VMEM((128, 128), f32)],
        cost_estimate=cost(10000000, 1 << 18),
        compiler_params=pltpu.CompilerParams(vmem_limit_bytes=VMEM_LIMIT),
        name="final_rows",
    )(x, gain)


def chip_permute(x, d):
    return lax.ppermute(x, "tp", [((i + 2 * d) % 8, i) for i in range(8)])


def core_permute(x):
    return lax.ppermute(x, "tp", [(i ^ 1, i) for i in range(8)])


def whole_step(
    tokens,
    input_norm_gain,
    query_weight,
    key_weight,
    value_weight,
    output_gate_weight,
    strength_weight,
    decay_weight,
    head_decay_rate,
    proposal_log_decay,
    head_norm_gain,
    output_weight,
    output_norm_gain,
    state,
    previous_keys,
    previous_values,
    previous_log_decay,
    previous_strengths,
    accepted,
    parent,
):
    sent, pack = prepare(
        jnp.transpose(tokens, (1, 2, 0)),
        jnp.transpose(value_weight[:, 0, :], (1, 0)),
        jnp.transpose(output_gate_weight[:, 0, :], (1, 0)),
        output_weight[0],
        head_norm_gain.reshape(1, 16),
    )
    near = [pack] + [chip_permute(pack, d) for d in (1, 2, 3)]
    x = lax.all_to_all(sent.reshape(128, 16, 128), BOTH, 0, 0, tiled=True).reshape(2048, 128)
    accepted_state, *lows = new_state(
        state.reshape(256, 16, 128),
        previous_keys.reshape(1024, 128),
        jnp.transpose(previous_values[:, :, 0, :], (1, 2, 0)),
        jnp.transpose(previous_strengths, (1, 2, 0)),
        jnp.transpose(previous_log_decay, (1, 2, 0)),
        accepted.reshape(1, 256),
    )
    near_states = [lows[0]] + [chip_permute(lows[4 - d], d) for d in (1, 2, 3)]
    packs = near + [core_permute(x) for x in near]
    states = near_states + [core_permute(x) for x in near_states]
    rows = row_side(
        x,
        packs,
        head_decay_rate.reshape(1, 1),
        input_norm_gain.reshape(16, 128),
        query_weight,
        key_weight,
        jnp.transpose(strength_weight, (1, 0)),
        jnp.transpose(decay_weight, (1, 0)),
        jnp.transpose(proposal_log_decay, (1, 2, 0)),
        jnp.transpose(parent, (1, 0)),
    )
    part = readout(*rows, packs, states)
    parts = lax.all_to_all(part.reshape(16, 8, 2048), "kv", 0, 0, tiled=True)
    blocks = lax.all_to_all(sum_heads(parts), BOTH, 0, 0, tiled=True)
    out = final_rows(blocks, output_norm_gain.reshape(1, 16))
    return jnp.transpose(out, (2, 0, 1)), accepted_state.reshape(state.shape)


def solution(mesh):
    placed = (
        P(None, None, ("kv", "tp")),
        P(),
        P(None, "kv"),
        P(None, "kv"),
        P(None, "kv", "tp"),
        P(None, "kv", "tp"),
        P(None, "kv"),
        P(None, "kv"),
        P("kv"),
        P(None, None, "kv"),
        P("tp"),
        P("kv", "tp", None),
        P(("kv", "tp")),
        P(None, "kv", "tp", None),
        P(None, None, "kv"),
        P(None, None, "kv", "tp"),
        P(None, None, "kv"),
        P(None, None, "kv"),
        P(),
        P(),
    )
    return jax.shard_map(
        whole_step,
        mesh=mesh,
        in_specs=placed,
        out_specs=(P(None, None, ("kv", "tp")), P(None, "kv", "tp", None)),
        check_vma=False,
    )
```

time: 94.9 us -> 87.1 us (0.918)
  blocking collectives: 14.4 us -> 31.9 us
  waiting for transfers between devices: 29 us -> 11.5 us
  starting transfers between devices: 30.4 us -> 22.4 us
  Pallas kernels: 12.3 us -> 14.6 us
  local copies, waits for them, and re-layouts: 6.67 us -> 4.84 us
    all_to_all x0 -> x1, blocking collectives: none -> 14 us  [whole_step(): blocks = lax.all_to_all(sum_heads(parts), BOTH, 0, 0, tiled=True)]
    all_to_all x3 -> x1, waiting for transfers between devices: 13.1 us -> 0.01 us  [whole_step(): lax.all_to_all(sent.reshape(128, 16, 128), BOTH, 0, 0, tiled=True)]
    all_to_all x3 -> x1, starting transfers between devices: 21.6 us -> 8.49 us  [whole_step(): lax.all_to_all(sent.reshape(128, 16, 128), BOTH, 0, 0, tiled=True)]
    ppermute x7 -> x14, starting transfers between devices: 8.86 us -> 13.9 us  [the longest x6 8.71 us: chip_permute(): return lax.ppermute(x, 'tp', [((i + 2 * d) % 8, i) for i in range(8)])]
    ppermute x7 -> x14, waiting for transfers between devices: 15.9 us -> 11.5 us  [the longest x6 11.5 us: chip_permute(): return lax.ppermute(x, 'tp', [((i + 2 * d) % 8, i) for i in range(8)])]
    all_to_all x1, blocking collectives: 14.4 us -> 17.9 us  [whole_step(): parts = lax.all_to_all(part.reshape(16, 8, 2048), 'kv', 0, 0, tiled=True)]
    pallas_call x4, Pallas kernels: 10.4 us -> 13.3 us  [the longest x1 4.94 us: new_state(): pl.pallas_call(state_kernel, in_specs=hbm_specs(6), out_specs=hbm_specs(1...]
    another operation x1 -> x0, local copies, waits for them, and re-layouts: 1.25 us -> none  [whole_step(): output_weight[0].reshape(16, 128, 16).transpose(0, 2, 1).reshape(16, 2048)]
  transfers between devices with their start and end apart: 10 -> 15, of which waited for: 5 -> 2; matrix products, arithmetic and copies ran while one was open for 2% -> 0% of each run, Pallas kernels for 9% -> 10%
where the time goes in v1:
time: 87.1 us; the launch traced here: 86.6 us
  blocking collectives  31.9 us (37%)
  starting transfers between devices  22.4 us (26%)
  Pallas kernels  14.6 us (17%)
  waiting for transfers between devices  11.5 us (13%)
  local copies, waits for them, and re-layouts  4.84 us (6%)
  between operations  1.42 us (2%)
    all_to_all x1, blocking collectives, whole_step(): parts = lax.all_to_all(part.reshape(16, 8, 2048), 'kv', 0, 0, tiled=True)  17.9 us
    all_to_all x1, blocking collectives, whole_step(): blocks = lax.all_to_all(sum_heads(parts), BOTH, 0, 0, tiled=True)  14 us
    ppermute x6, waiting for transfers between devices, chip_permute(): return lax.ppermute(x, 'tp', [((i + 2 * d) % 8, i) for i in range(8)])  11.5 us
    ppermute x6, starting transfers between devices, chip_permute(): return lax.ppermute(x, 'tp', [((i + 2 * d) % 8, i) for i in range(8)])  8.71 us
    all_to_all x1, starting transfers between devices, whole_step(): lax.all_to_all(sent.reshape(128, 16, 128), BOTH, 0, 0, tiled=True)  8.49 us
    ppermute x8, starting transfers between devices, core_permute(): return lax.ppermute(x, 'tp', [(i ^ 1, i) for i in range(8)])  5.19 us
    pallas_call x1, Pallas kernels, new_state(): pl.pallas_call(state_kernel, in_specs=hbm_specs(6), out_specs=hbm_specs(1...  4.94 us
    unnamed x18, local copies, waits for them, and re-layouts  4.84 us
  transfers between devices with their start and end apart: 15, of which 2 were waited for; matrix products, arithmetic and copies ran while one was open for 0% of the time, Pallas kernels for 10%

profile of v1, /device:TPU:1, one launch (start us, length us, event | category | flops | bytes accessed | tf_op | source)
XLA Modules:
  0.0 86.6 jit_solution(8834043301734836428)
XLA Ops:
  0.6 2.4 %prepare.1 = (bf16[16,8,16,128]{3,2,1,0:T(8,128)(2,1)}, bf16[784,128]{1,0:T(8,128)(2,1)S(1)}) custom-call(bf16[4,16,256]{2,1,0:T(8,128)(2,1)} %bitcast.44, bf16[16,2048]{1,0:T(8,128)(2,1)} %bitcast.41, bf16[16,2048]{1,0:T(8,128)(2,1)} %bitcast.42, bf16[16,2048]{1,0:T(8,128)(2,1)} %bitcast.43, bf16[1,16]{1,0:T(2,128)(2,1)} %bitcast.46), custom_call_target="tpu_custom_call" | custom-call | flops 10000000 | bytes 1048576 | tf_op jit(solution)/shard_map/prepare/pallas_call | solution.py:105
  3.1 1.5 %collective-permute-start.3 = (bf16[784,128]{1,0:T(8,128)(2,1)S(1)}, bf16[784,128]{1,0:T(8,128)(2,1)S(1)}, u32[]{:S(2)}, u32[]{:S(2)}) collective-permute-start(bf16[784,128]{1,0:T(8,128)(2,1)S(1)} %get-tuple-element.14.refs_0_.rest_0_), channel_id=1, source_target_pairs={{1,0},{0,1},{3,2},{2,3},{5,4},{4,5},{7,6},{6,7},{9,8},{8,9},{11,10... | collective-permute-start | bytes 602120 | tf_op jit(solution)/shard_map/ppermute | solution.py:428
  4.5 1.3 %collective-permute-start.2 = (bf16[784,128]{1,0:T(8,128)(2,1)S(1)}, bf16[784,128]{1,0:T(8,128)(2,1)S(1)}, u32[]{:S(2)}, u32[]{:S(2)}) collective-permute-start(bf16[784,128]{1,0:T(8,128)(2,1)S(1)} %get-tuple-element.14.refs_0_.rest_0_), channel_id=1, source_target_pairs={{6,0},{7,1},{0,2},{1,3},{2,4},{3,5},{4,6},{5,7},{14,8},{15,9},{8,1... | collective-permute-start | bytes 602120 | tf_op jit(solution)/shard_map/ppermute | solution.py:424
  5.8 2.5 %collective-permute-start.1 = (bf16[784,128]{1,0:T(8,128)(2,1)S(1)}, bf16[784,128]{1,0:T(8,128)(2,1)S(1)}, u32[]{:S(2)}, u32[]{:S(2)}) collective-permute-start(bf16[784,128]{1,0:T(8,128)(2,1)S(1)} %get-tuple-element.14.refs_0_.rest_0_), channel_id=1, source_target_pairs={{4,0},{5,1},{6,2},{7,3},{0,4},{1,5},{2,6},{3,7},{12,8},{13,9},{14,... | collective-permute-start | bytes 602120 | tf_op jit(solution)/shard_map/ppermute | solution.py:424
  8.3 1.1 %collective-permute-start = (bf16[784,128]{1,0:T(8,128)(2,1)S(1)}, bf16[784,128]{1,0:T(8,128)(2,1)}, u32[]{:S(2)}, u32[]{:S(2)}) collective-permute-start(bf16[784,128]{1,0:T(8,128)(2,1)S(1)} %get-tuple-element.14.refs_0_.rest_0_), channel_id=1, source_target_pairs={{2,0},{3,1},{4,2},{5,3},{6,4},{7,5},{0,6},{1,7},{10,8},{11,9},{12,... | collective-permute-start | bytes 602120 | tf_op jit(solution)/shard_map/ppermute | solution.py:424
  9.4 8.5 %all-to-all-start = ((bf16[128,16,128]{2,1,0:T(8,128)(2,1)}), bf16[128,16,128]{2,1,0:T(8,128)(2,1)S(1)}, u32[]{:S(2)}, u32[]{:S(2)}) async-start(bf16[128,16,128]{2,1,0:T(8,128)(2,1)} %bitcast.7), calls=%async_computation | async-start | bytes 1048576 | tf_op jit(solution)/shard_map/all_to_all | solution.py:461
  17.9 4.9 %new_state.1 = (f32[256,16,128]{2,1,0:T(8,128)}, bf16[1024,128]{1,0:T(8,128)(2,1)S(1)}, bf16[1024,128]{1,0:T(8,128)(2,1)S(1)}, bf16[1024,128]{1,0:T(8,128)(2,1)S(1)}, bf16[1024,128]{1,0:T(8,128)(2,1)S(1)}) custom-call(f32[256,16,128]{2,1,0:T(8,128)} %bitcast.47, bf16[1024,128]{1,0:T(8,128)(2,1)} %bitcast.48, bf16[4,16,256]{2,1,0:T(8,128)(2,1)} %bitcast.49, ...), custom_call_target="tpu_custom_call" | custom-call | flops 2000000000 | bytes 5242880 | tf_op jit(solution)/shard_map/new_state/pallas_call | solution.py:208
  22.9 2.6 %collective-permute-start.7 = (bf16[1024,128]{1,0:T(8,128)(2,1)S(1)}, bf16[1024,128]{1,0:T(8,128)(2,1)S(1)}, u32[]{:S(2)}, u32[]{:S(2)}) collective-permute-start(bf16[1024,128]{1,0:T(8,128)(2,1)S(1)} %get-tuple-element.20), channel_id=1, source_target_pairs={{2,0},{3,1},{4,2},{5,3},{6,4},{7,5},{0,6},{1,7},{10,8},{11,9},{12,... | collective-permute-start | bytes 786440 | tf_op jit(solution)/shard_map/ppermute | solution.py:424
  25.5 0.0 collective-permute-done.3.refs_4_.rest_4_
  25.5 0.6 collective-permute-start.8
  26.1 0.0 collective-permute-done.2.refs_3_.rest_3_
  26.1 0.6 collective-permute-start.9
  26.7 0.0 collective-permute-done.1.refs_2_.rest_2_
  26.7 1.2 %collective-permute-start.6 = (bf16[784,128]{1,0:T(8,128)(2,1)S(1)}, bf16[784,128]{1,0:T(8,128)(2,1)S(1)}, u32[]{:S(2)}, u32[]{:S(2)}) collective-permute-start(bf16[784,128]{1,0:T(8,128)(2,1)S(1)} %collective-permute-done.2.refs_3_.rest_3_), channel_id=1, source_target_pairs={{1,0},{0,1},{3,2},{2,3},{5,4},{4,5},{7,6},{6,7},{9,8},{8,9},{11,10... | collective-permute-start | bytes 602120 | tf_op jit(solution)/shard_map/ppermute | solution.py:428
  27.9 0.0 collective-permute-done.refs_1_.rest_1_
  27.9 0.1 collective-permute-start.5
  28.0 8.3 %collective-permute-done.7.rest_9_ = bf16[1024,128]{1,0:T(8,128)(2,1)S(1)} collective-permute-done((bf16[1024,128]{1,0:T(8,128)(2,1)S(1)}, bf16[1024,128]{1,0:T(8,128)(2,1)S(1)}, u32[]{:S(2)}, u32[]{:S(2)}) %collective-permute-start.7) | collective-permute-done | bytes 262176 | tf_op jit(solution)/shard_map/ppermute | solution.py:424
  36.3 1.4 %collective-permute-start.4 = (bf16[784,128]{1,0:T(8,128)(2,1)}, bf16[784,128]{1,0:T(8,128)(2,1)S(1)}, u32[]{:S(2)}, u32[]{:S(2)}) collective-permute-start(bf16[784,128]{1,0:T(8,128)(2,1)} %collective-permute-done.refs_1_.rest_1_), channel_id=1, source_target_pairs={{1,0},{0,1},{3,2},{2,3},{5,4},{4,5},{7,6},{6,7},{9,8},{8,9},{11,10... | collective-permute-start | bytes 602120 | tf_op jit(solution)/shard_map/ppermute | solution.py:428
  37.7 0.0 collective-permute-done.8.rest_10_
  37.7 0.0 collective-permute-start.10
  37.7 3.2 %collective-permute-done.9.rest_11_ = bf16[1024,128]{1,0:T(8,128)(2,1)S(1)} collective-permute-done((bf16[1024,128]{1,0:T(8,128)(2,1)S(1)}, bf16[1024,128]{1,0:T(8,128)(2,1)S(1)}, u32[]{:S(2)}, u32[]{:S(2)}) %collective-permute-start.9) | collective-permute-done | bytes 262176 | tf_op jit(solution)/shard_map/ppermute | solution.py:424
  40.9 0.5 collective-permute-start.11
  41.4 0.0 collective-permute-done.6.refs_7_.rest_7_
  41.4 0.7 copy-done
  42.1 0.0 collective-permute-start.12
  42.1 0.0 collective-permute-done.5.refs_6_.rest_6_
  42.1 0.7 copy-done.2
  42.8 0.5 collective-permute-start.13
  43.9 0.0 collective-permute-done.4.refs_5_.rest_5_
  43.9 0.0 copy-start.5
  43.9 0.7 copy-done.5
  44.6 0.0 all-to-all-done
  44.6 0.9 %copy-done.1 = bf16[784,128]{1,0:T(8,128)(2,1)S(1)} copy-done((bf16[784,128]{1,0:T(8,128)(2,1)S(1)}, bf16[784,128]{1,0:T(8,128)(2,1)}, u32[]{:S(2)}) %copy-start.1) | copy-done | bytes 200728
  45.5 0.9 %copy-done.3 = bf16[784,128]{1,0:T(8,128)(2,1)S(1)} copy-done((bf16[784,128]{1,0:T(8,128)(2,1)S(1)}, bf16[784,128]{1,0:T(8,128)(2,1)}, u32[]{:S(2)}) %copy-start.3) | copy-done | bytes 200728
  46.5 0.9 %copy-done.6 = bf16[784,128]{1,0:T(8,128)(2,1)S(1)} copy-done((bf16[784,128]{1,0:T(8,128)(2,1)S(1)}, bf16[784,128]{1,0:T(8,128)(2,1)}, u32[]{:S(2)}) %copy-start.6) | copy-done | bytes 200728
  47.4 4.0 %row_side.1 = (bf16[128,128]{1,0:T(8,128)(2,1)S(1)}, bf16[128,128]{1,0:T(8,128)(2,1)S(1)}, f32[128,128]{1,0:T(8,128)S(1)}, f32[128,128]{1,0:T(8,128)S(1)}) custom-call(bf16[2048,128]{1,0:T(8,128)(2,1)S(1)} %bitcast.37, bf16[784,128]{1,0:T(8,128)(2,1)S(1)} %get-tuple-element.14.refs_0_.rest_0_, bf16[784,128]{1,0:T(8,128)(2,1)} %collective-permute-done.refs_1_.rest_1_, ...), custom_call_target="tpu_custom_call" | custom-call | flops 2000000000 | bytes 4194304 | tf_op jit(solution)/shard_map/row_side/pallas_call | solution.py:322
  51.4 0.0 collective-permute-done.10.rest_12_
  51.4 0.0 collective-permute-done.11.rest_13_
  51.4 0.0 collective-permute-done.12.rest_14_
  51.5 0.0 collective-permute-done.13.rest_15_
  51.5 0.0 copy-done.4
  51.5 0.0 copy-start.8
  51.5 2.0 %readout.1 = bf16[128,2048]{1,0:T(8,128)(2,1)S(1)} custom-call(bf16[128,128]{1,0:T(8,128)(2,1)S(1)} %get-tuple-element.15.high_ref, bf16[128,128]{1,0:T(8,128)(2,1)S(1)} %get-tuple-element.16.low_ref, f32[128,128]{1,0:T(8,128)S(1)} %get-tuple-element.17.pv_ref, f32[128,128]{1,0:T(8,128)S(1)} %get-tuple-element.18.gate_ref, ...), custom_call_target="tpu_custom_call" | custom-call | flops 500000000 | bytes 3145728 | tf_op jit(solution)/shard_map/readout/pallas_call | solution.py:355
  53.5 17.9 %all_to_all.21.part_ref = bf16[16,8,2048]{2,1,0:T(8,128)(2,1)S(1)} all-to-all(bf16[16,8,2048]{2,1,0:T(8,128)(2,1)S(1)} %bitcast.36), channel_id=1, replica_groups=mesh['kv'=16,'tp'=8] {'kv'}, dimensions={0} | all-to-all | bytes 1048576 | tf_op jit(solution)/shard_map/all_to_all | solution.py:486
  71.4 0.3 sum_heads.1
  71.6 14.0 %all_to_all.22 = f32[128,1,128]{2,1,0:T(1,128)S(1)} all-to-all(f32[128,1,128]{2,1,0:T(1,128)S(1)} %bitcast.38), channel_id=1, replica_groups=mesh['kv'=16,'tp'=8] {'kv','tp'}, dimensions={0} | all-to-all | bytes 131072 | tf_op jit(solution)/shard_map/all_to_all | solution.py:487
  85.6 0.0 copy-done.8
  85.6 1.0 %final_rows.1 = bf16[4,16,256]{2,1,0:T(8,128)(2,1)} custom-call(f32[128,128]{1,0:T(8,128)S(1)} %bitcast.39, bf16[1,16]{1,0:T(2,128)(2,1)S(1)} %bitcast.40), custom_call_target="tpu_custom_call" | custom-call | flops 10000000 | bytes 262144 | tf_op jit(solution)/shard_map/final_rows/pallas_call | solution.py:411
  (8 shorter events, 0.0 us)
Async XLA Ops:
  3.1 22.5 %collective-permute-start.3 = (bf16[784,128]{1,0:T(8,128)(2,1)S(1)}, bf16[784,128]{1,0:T(8,128)(2,1)S(1)}, u32[]{:S(2)}, u32[]{:S(2)}) collective-permute-start(bf16[784,128]{1,0:T(8,128)(2,1)S(1)} %get-tuple-element.14.refs_0_.rest_0_), channel_id=1, source_target_pairs={{1,0},{0,1},{3,2},{2,3},{5,4},{4,5},{7,6},{6,7},{9,8},{8,9},{11,10... | collective-permute-start | bytes 602120 | tf_op jit(solution)/shard_map/ppermute | solution.py:428
  4.5 21.6 %collective-permute-start.2 = (bf16[784,128]{1,0:T(8,128)(2,1)S(1)}, bf16[784,128]{1,0:T(8,128)(2,1)S(1)}, u32[]{:S(2)}, u32[]{:S(2)}) collective-permute-start(bf16[784,128]{1,0:T(8,128)(2,1)S(1)} %get-tuple-element.14.refs_0_.rest_0_), channel_id=1, source_target_pairs={{6,0},{7,1},{0,2},{1,3},{2,4},{3,5},{4,6},{5,7},{14,8},{15,9},{8,1... | collective-permute-start | bytes 602120 | tf_op jit(solution)/shard_map/ppermute | solution.py:424
  5.8 20.8 %collective-permute-start.1 = (bf16[784,128]{1,0:T(8,128)(2,1)S(1)}, bf16[784,128]{1,0:T(8,128)(2,1)S(1)}, u32[]{:S(2)}, u32[]{:S(2)}) collective-permute-start(bf16[784,128]{1,0:T(8,128)(2,1)S(1)} %get-tuple-element.14.refs_0_.rest_0_), channel_id=1, source_target_pairs={{4,0},{5,1},{6,2},{7,3},{0,4},{1,5},{2,6},{3,7},{12,8},{13,9},{14,... | collective-permute-start | bytes 602120 | tf_op jit(solution)/shard_map/ppermute | solution.py:424
  8.3 19.6 %collective-permute-start = (bf16[784,128]{1,0:T(8,128)(2,1)S(1)}, bf16[784,128]{1,0:T(8,128)(2,1)}, u32[]{:S(2)}, u32[]{:S(2)}) collective-permute-start(bf16[784,128]{1,0:T(8,128)(2,1)S(1)} %get-tuple-element.14.refs_0_.rest_0_), channel_id=1, source_target_pairs={{2,0},{3,1},{4,2},{5,3},{6,4},{7,5},{0,6},{1,7},{10,8},{11,9},{12,... | collective-permute-start | bytes 602120 | tf_op jit(solution)/shard_map/ppermute | solution.py:424
  9.4 35.2 %all-to-all-start = ((bf16[128,16,128]{2,1,0:T(8,128)(2,1)}), bf16[128,16,128]{2,1,0:T(8,128)(2,1)S(1)}, u32[]{:S(2)}, u32[]{:S(2)}) async-start(bf16[128,16,128]{2,1,0:T(8,128)(2,1)} %bitcast.7), calls=%async_computation | async-start | bytes 1048576 | tf_op jit(solution)/shard_map/all_to_all | solution.py:461
  22.9 13.4 %collective-permute-start.7 = (bf16[1024,128]{1,0:T(8,128)(2,1)S(1)}, bf16[1024,128]{1,0:T(8,128)(2,1)S(1)}, u32[]{:S(2)}, u32[]{:S(2)}) collective-permute-start(bf16[1024,128]{1,0:T(8,128)(2,1)S(1)} %get-tuple-element.20), channel_id=1, source_target_pairs={{2,0},{3,1},{4,2},{5,3},{6,4},{7,5},{0,6},{1,7},{10,8},{11,9},{12,... | collective-permute-start | bytes 786440 | tf_op jit(solution)/shard_map/ppermute | solution.py:424
  25.5 12.1 %collective-permute-start.8 = (bf16[1024,128]{1,0:T(8,128)(2,1)S(1)}, bf16[1024,128]{1,0:T(8,128)(2,1)S(1)}, u32[]{:S(2)}, u32[]{:S(2)}) collective-permute-start(bf16[1024,128]{1,0:T(8,128)(2,1)S(1)} %get-tuple-element.21), channel_id=1, source_target_pairs={{4,0},{5,1},{6,2},{7,3},{0,4},{1,5},{2,6},{3,7},{12,8},{13,9},{14,... | collective-permute-start | bytes 786440 | tf_op jit(solution)/shard_map/ppermute | solution.py:424
  26.1 14.8 %collective-permute-start.9 = (bf16[1024,128]{1,0:T(8,128)(2,1)S(1)}, bf16[1024,128]{1,0:T(8,128)(2,1)S(1)}, u32[]{:S(2)}, u32[]{:S(2)}) collective-permute-start(bf16[1024,128]{1,0:T(8,128)(2,1)S(1)} %get-tuple-element.22), channel_id=1, source_target_pairs={{6,0},{7,1},{0,2},{1,3},{2,4},{3,5},{4,6},{5,7},{14,8},{15,9},{8,1... | collective-permute-start | bytes 786440 | tf_op jit(solution)/shard_map/ppermute | solution.py:424
  26.7 14.7 %collective-permute-start.6 = (bf16[784,128]{1,0:T(8,128)(2,1)S(1)}, bf16[784,128]{1,0:T(8,128)(2,1)S(1)}, u32[]{:S(2)}, u32[]{:S(2)}) collective-permute-start(bf16[784,128]{1,0:T(8,128)(2,1)S(1)} %collective-permute-done.2.refs_3_.rest_3_), channel_id=1, source_target_pairs={{1,0},{0,1},{3,2},{2,3},{5,4},{4,5},{7,6},{6,7},{9,8},{8,9},{11,10... | collective-permute-start | bytes 602120 | tf_op jit(solution)/shard_map/ppermute | solution.py:428
  27.9 14.2 %collective-permute-start.5 = (bf16[784,128]{1,0:T(8,128)(2,1)S(1)}, bf16[784,128]{1,0:T(8,128)(2,1)S(1)}, u32[]{:S(2)}, u32[]{:S(2)}) collective-permute-start(bf16[784,128]{1,0:T(8,128)(2,1)S(1)} %collective-permute-done.1.refs_2_.rest_2_), channel_id=1, source_target_pairs={{1,0},{0,1},{3,2},{2,3},{5,4},{4,5},{7,6},{6,7},{9,8},{8,9},{11,10... | collective-permute-start | bytes 602120 | tf_op jit(solution)/shard_map/ppermute | solution.py:428
  36.3 7.6 %collective-permute-start.4 = (bf16[784,128]{1,0:T(8,128)(2,1)}, bf16[784,128]{1,0:T(8,128)(2,1)S(1)}, u32[]{:S(2)}, u32[]{:S(2)}) collective-permute-start(bf16[784,128]{1,0:T(8,128)(2,1)} %collective-permute-done.refs_1_.rest_1_), channel_id=1, source_target_pairs={{1,0},{0,1},{3,2},{2,3},{5,4},{4,5},{7,6},{6,7},{9,8},{8,9},{11,10... | collective-permute-start | bytes 602120 | tf_op jit(solution)/shard_map/ppermute | solution.py:428
  37.7 13.8 %collective-permute-start.10 = (bf16[1024,128]{1,0:T(8,128)(2,1)S(1)}, bf16[1024,128]{1,0:T(8,128)(2,1)S(1)}, u32[]{:S(2)}, u32[]{:S(2)}) collective-permute-start(bf16[1024,128]{1,0:T(8,128)(2,1)S(1)} %get-tuple-element.19.rest_8_), channel_id=1, source_target_pairs={{1,0},{0,1},{3,2},{2,3},{5,4},{4,5},{7,6},{6,7},{9,8},{8,9},{11,10... | collective-permute-start | bytes 786440 | tf_op jit(solution)/shard_map/ppermute | solution.py:428
  40.9 10.6 %collective-permute-start.11 = (bf16[1024,128]{1,0:T(8,128)(2,1)S(1)}, bf16[1024,128]{1,0:T(8,128)(2,1)S(1)}, u32[]{:S(2)}, u32[]{:S(2)}) collective-permute-start(bf16[1024,128]{1,0:T(8,128)(2,1)S(1)} %collective-permute-done.7.rest_9_), channel_id=1, source_target_pairs={{1,0},{0,1},{3,2},{2,3},{5,4},{4,5},{7,6},{6,7},{9,8},{8,9},{11,10... | collective-permute-start | bytes 786440 | tf_op jit(solution)/shard_map/ppermute | solution.py:428
  41.4 0.7 copy-start
  42.1 9.4 %collective-permute-start.12 = (bf16[1024,128]{1,0:T(8,128)(2,1)S(1)}, bf16[1024,128]{1,0:T(8,128)(2,1)S(1)}, u32[]{:S(2)}, u32[]{:S(2)}) collective-permute-start(bf16[1024,128]{1,0:T(8,128)(2,1)S(1)} %collective-permute-done.8.rest_10_), channel_id=1, source_target_pairs={{1,0},{0,1},{3,2},{2,3},{5,4},{4,5},{7,6},{6,7},{9,8},{8,9},{11,10... | collective-permute-start | bytes 786440 | tf_op jit(solution)/shard_map/ppermute | solution.py:428
  42.1 0.7 copy-start.2
  42.8 8.7 %collective-permute-start.13 = (bf16[1024,128]{1,0:T(8,128)(2,1)S(1)}, bf16[1024,128]{1,0:T(8,128)(2,1)S(1)}, u32[]{:S(2)}, u32[]{:S(2)}) collective-permute-start(bf16[1024,128]{1,0:T(8,128)(2,1)S(1)} %collective-permute-done.9.rest_11_), channel_id=1, source_target_pairs={{1,0},{0,1},{3,2},{2,3},{5,4},{4,5},{7,6},{6,7},{9,8},{8,9},{11,10... | collective-permute-start | bytes 786440 | tf_op jit(solution)/shard_map/ppermute | solution.py:428
  43.9 0.7 copy-start.5
  44.6 0.9 %copy-start.1 = (bf16[784,128]{1,0:T(8,128)(2,1)S(1)}, bf16[784,128]{1,0:T(8,128)(2,1)}, u32[]{:S(2)}) copy-start(bf16[784,128]{1,0:T(8,128)(2,1)} %copy-done) | copy-start | bytes 602116
  45.5 0.9 %copy-start.3 = (bf16[784,128]{1,0:T(8,128)(2,1)S(1)}, bf16[784,128]{1,0:T(8,128)(2,1)}, u32[]{:S(2)}) copy-start(bf16[784,128]{1,0:T(8,128)(2,1)} %copy-done.2) | copy-start | bytes 602116
  46.5 0.9 %copy-start.6 = (bf16[784,128]{1,0:T(8,128)(2,1)S(1)}, bf16[784,128]{1,0:T(8,128)(2,1)}, u32[]{:S(2)}) copy-start(bf16[784,128]{1,0:T(8,128)(2,1)} %copy-done.5) | copy-start | bytes 602116
  47.4 4.1 %copy-start.4 = (bf16[784,128]{1,0:T(8,128)(2,1)S(1)}, bf16[784,128]{1,0:T(8,128)(2,1)}, u32[]{:S(2)}) copy-start(bf16[784,128]{1,0:T(8,128)(2,1)} %copy-done.2) | copy-start | bytes 602116
  47.4 4.1 %copy-start.7 = (bf16[784,128]{1,0:T(8,128)(2,1)S(1)}, bf16[784,128]{1,0:T(8,128)(2,1)}, u32[]{:S(2)}) copy-start(bf16[784,128]{1,0:T(8,128)(2,1)} %copy-done.5) | copy-start | bytes 602116
  51.5 34.1 %copy-start.8 = (bf16[16]{0:T(256)(128)(2,1)S(1)}, bf16[16]{0:T(256)(128)(2,1)}, u32[]{:S(2)}) copy-start(bf16[16]{0:T(256)(128)(2,1)} %param.32) | copy-start | bytes 100

commit v2 on v1

--- a/solution.py
+++ b/solution.py
@@ -88,9 +88,15 @@
 
 
 def prepare_kernel(*refs):
-    sources, (sent_ref, pack_ref), held, sems = refs[:5], refs[5:7], refs[7:12], refs[12]
-    copies = copies_in(sources, held, sems)
-    start_all(copies)
+    sources, state_source, (sent_ref, pack_ref), kept, rest = refs[:15], refs[15], refs[16:18], refs[18:28], refs[28:]
+    low_ref, held, sems, state_ref = rest[0], rest[1:6], rest[6:9], rest[9]
+    copies = copies_in(sources[:5], held, sems[0])
+    ahead = copies_in(sources[5:], kept, sems[1])
+    chip = lax.axis_index("tp") // 2
+    for i in range(3):
+        rows = pl.ds(pl.multiple_of(64 * lax.rem(chip + 1 + i, 4), 64), 64)
+        ahead.append(pltpu.make_async_copy(state_source.at[rows], state_ref.at[pl.ds(64 * i, 64)], sems[2].at[i]))
+    start_all(copies + ahead)
     wait_all(copies[1:])
     pack_weights(*held[1:], pack_ref)
     copies[0].wait()
@@ -99,19 +105,25 @@
         block = chunk_lanes(rows, t).astype(bf16)
         for k in range(16):
             sent_ref[k, t] = block
-
-
-def prepare(*arrays):
+    wait_all(ahead)
+    for i in range(6):
+        low_ref[512 * i : 512 * i + 512, :] = state_ref[32 * i : 32 * i + 32].reshape(512, 128).astype(bf16)
+
+
+def prepare(first, ahead, state):
     return pl.pallas_call(
         prepare_kernel,
-        in_specs=hbm_specs(5),
-        out_specs=vmem_specs(2),
-        out_shape=[pltpu.VMEM((16, 8, 16, 128), bf16), pltpu.VMEM((PACK, 128), bf16)],
-        scratch_shapes=scratch_like(arrays),
+        in_specs=hbm_specs(16),
+        out_specs=vmem_specs(13),
+        out_shape=[pltpu.VMEM((16, 8, 16, 128), bf16), pltpu.VMEM((PACK, 128), bf16)]
+        + [pltpu.VMEM(x.shape, x.dtype) for x in ahead]
+        + [pltpu.VMEM((3072, 128), bf16)],
+        scratch_shapes=scratch_like(first)
+        + [pltpu.SemaphoreType.DMA((10,)), pltpu.SemaphoreType.DMA((3,)), pltpu.VMEM((192, 16, 128), f32)],
         cost_estimate=cost(10000000, 1 << 20),
         compiler_params=pltpu.CompilerParams(vmem_limit_bytes=VMEM_LIMIT),
         name="prepare",
-    )(*in_hbm(arrays))
+    )(*in_hbm((*first, *ahead, state)))
 
 
 def stack(rows):
@@ -119,32 +131,15 @@
 
 
 def spread_rows(x):
-    return jnp.broadcast_to(x[:, None, :], (8, 16, 128)).reshape(128, 128)
-
-
-def state_kernel(*refs):
-    state_source, sources, state_out, lows, state_ref, held, (sems, state_sems) = (
-        refs[0], refs[1:6], refs[6], refs[7:11], refs[11], refs[12:17], refs[17:],
-    )
-    key_ref, value_ref, strength_ref, decay_ref, accepted_ref = held
+    count = x.shape[0]
+    return jnp.broadcast_to(x[:, None, :], (count, 16, 128)).reshape(16 * count, 128)
+
+
+def state_update(chips, operands, read, emit):
+    key_ref, value_ref, strength_ref, decay_ref, accepted_ref = operands
+    steps = range(2 * len(chips))
     chip = lax.axis_index("tp") // 2
-    groups = [2 * lax.rem(chip + step // 2, 4) + step % 2 for step in range(8)]
-
-    def rows_of(step, count=1):
-        return pl.ds(pl.multiple_of(32 * groups[step], 32), 32 * count)
-
-    copies = copies_in(sources, held, sems)
-    loads = [
-        pltpu.make_async_copy(state_source.at[rows_of(2 * i, 2)], state_ref.at[rows_of(2 * i, 2)], state_sems.at[0, i])
-        for i in range(4)
-    ]
-    stores = [
-        pltpu.make_async_copy(state_ref.at[rows_of(2 * i, 2)], state_out.at[rows_of(2 * i, 2)], state_sems.at[1, i])
-        for i in range(4)
-    ]
-    start_all(copies + loads)
-    wait_all(copies)
-
+    groups = [2 * lax.rem(chip + chips[step // 2], 4) + step % 2 for step in steps]
     lane = iota((1, 128), 1)
     place = lane // 32
     strength = stack([chunk_lanes([strength_ref[j] for j in range(4)], x) for x in groups])
@@ -180,41 +175,92 @@
     coupling = {d: spread_rows(x) for d, x in coupling.items()}
     own = iota((32, 16, 128), 0) == iota((32, 16, 128), 2) % 32
     seen = []
-    for step in range(8):
-        if step % 2 == 0:
-            loads[step // 2].wait()
-        high, low = split(state_ref[rows_of(step)].reshape(512, 128))
-        read = dot(high, keys[step], 1, 1) + dot(low, keys[step], 1, 1)
-        seen.append(jnp.sum(jnp.where(own, read.reshape(32, 16, 128), 0.0), axis=0))
+    for step in steps:
+        product = dot(read(step).astype(bf16), keys[step], 1, 1)
+        seen.append(jnp.sum(jnp.where(own, product.reshape(32, 16, 128), 0.0), axis=0))
     update = solve(spread_rows(beta) * values - spread_rows(beta * jnp.exp(gam) * unit) * stack(seen), coupling)
     update = update * spread_rows(jnp.exp(last - gam) * unit)
     keep = jnp.exp(last)
-    for step in range(8):
+    for step in steps:
         spread = jnp.broadcast_to(update[16 * step : 16 * step + 16][None], (32, 16, 128))
-        high, low = split(jnp.where(own, spread, 0.0).reshape(512, 128))
-        change = dot(high, keys[step], 1, 0) + dot(low, keys[step], 1, 0)
+        change = dot(jnp.where(own, spread, 0.0).reshape(512, 128).astype(bf16), keys[step], 1, 0)
         kept = jnp.where(iota((32, 128), 0) == iota((32, 128), 1), keep[step : step + 1], 0.0)
         kept = jnp.broadcast_to(jnp.sum(kept, axis=1, keepdims=True), (32, 128))
         kept = jnp.broadcast_to(kept[:, None, :], (32, 16, 128))
-        new = kept * state_ref[rows_of(step)] + change.reshape(32, 16, 128)
-        state_ref[rows_of(step)] = new
-        lows[step // 2][512 * (step % 2) : 512 * (step % 2) + 512, :] = new.reshape(512, 128).astype(bf16)
+        emit(step, kept.reshape(512, 128) * read(step).astype(f32) + change)
+
+
+def other_chips_kernel(state_ref, *refs):
+    operands, lows = refs[:5], refs[5:]
+
+    def emit(step, new):
+        lows[step // 2][512 * (step % 2) : 512 * (step % 2) + 512, :] = new.astype(bf16)
+
+    state_update((1, 2, 3), operands, lambda step: state_ref[512 * step : 512 * step + 512, :], emit)
+
+
+def other_chips_state(state, operands):
+    return pl.pallas_call(
+        other_chips_kernel,
+        in_specs=vmem_specs(6),
+        out_specs=vmem_specs(3),
+        out_shape=[pltpu.VMEM((1024, 128), bf16)] * 3,
+        cost_estimate=cost(1500000000, 3 << 20),
+        compiler_params=pltpu.CompilerParams(vmem_limit_bytes=VMEM_LIMIT),
+        name="other_chips_state",
+    )(state, *operands)
+
+
+def all_chips_kernel(source, key_source, *refs):
+    operands, (state_out, low_ref, state_ref, key_ref, sems) = refs[:4], refs[4:]
+    chip = lax.axis_index("tp") // 2
+
+    def rows_of(i):
+        return pl.ds(pl.multiple_of(64 * lax.rem(chip + i, 4), 64), 64)
+
+    def held(i):
+        return pl.ds(64 * i, 64)
+
+    loads = [pltpu.make_async_copy(source.at[rows_of(i)], state_ref.at[held(i)], sems.at[0, i]) for i in range(4)]
+    stores = [pltpu.make_async_copy(state_ref.at[held(i)], state_out.at[rows_of(i)], sems.at[1, i]) for i in range(4)]
+    keys = pltpu.make_async_copy(key_source, key_ref, sems.at[0, 4])
+    keys.start()
+    start_all(loads)
+    keys.wait()
+    arrived = set()
+
+    def read(step):
+        if step // 2 not in arrived:
+            arrived.add(step // 2)
+            loads[step // 2].wait()
+        return state_ref[32 * step : 32 * step + 32].reshape(512, 128)
+
+    def emit(step, new):
+        state_ref[32 * step : 32 * step + 32] = new.reshape(32, 16, 128)
+        if step < 2:
+            low_ref[512 * step : 512 * step + 512, :] = new.astype(bf16)
         if step % 2 == 1:
             stores[step // 2].start()
+
+    state_update((0, 1, 2, 3), (key_ref, *operands), read, emit)
     wait_all(stores)
 
 
-def new_state(state, *arrays):
-    return pl.pallas_call(
-        state_kernel,
-        in_specs=hbm_specs(6),
-        out_specs=hbm_specs(1) + vmem_specs(4),
-        out_shape=[pltpu.HBM((256, 16, 128), f32)] + [pltpu.VMEM((1024, 128), bf16)] * 4,
-        scratch_shapes=[pltpu.VMEM((256, 16, 128), f32), *scratch_like(arrays), pltpu.SemaphoreType.DMA((2, 4))],
-        cost_estimate=cost(2000000000, 5 << 20),
-        compiler_params=pltpu.CompilerParams(vmem_limit_bytes=VMEM_LIMIT),
-        name="new_state",
-    )(*in_hbm((state, *arrays)))
+def all_chips_state(state, keys, operands):
+    return pl.pallas_call(
+        all_chips_kernel,
+        in_specs=hbm_specs(2) + vmem_specs(4),
+        out_specs=hbm_specs(1) + vmem_specs(1),
+        out_shape=[pltpu.HBM((256, 16, 128), f32), pltpu.VMEM((1024, 128), bf16)],
+        scratch_shapes=[
+            pltpu.VMEM((256, 16, 128), f32),
+            pltpu.VMEM((1024, 128), bf16),
+            pltpu.SemaphoreType.DMA((2, 5)),
+        ],
+        cost_estimate=cost(2000000000, 4 << 20),
+        compiler_params=pltpu.CompilerParams(vmem_limit_bytes=VMEM_LIMIT),
+        name="all_chips_state",
+    )(*in_hbm((state, keys)), *operands)
 
 
 def pack_weights(value_ref, gate_ref, output_ref, gain_ref, pack_ref):
@@ -251,12 +297,14 @@
 
 
 def rows_kernel(x_ref, *refs):
-    packs, rate_ref, sources, rest = refs[:8], refs[8], refs[9:16], refs[16:]
-    (high_ref, low_ref, pv_ref, gate_ref), held, sems = rest[:4], rest[4:11], rest[11]
-    gain_ref, wq_ref, wk_ref, strength_ref, decay_ref, log_decay_ref, parent_ref = held
+    packs, small, rate_ref, sources, outs, held, sems = (
+        refs[:8], refs[8:13], refs[13], refs[14:16], refs[16:20], refs[20:22], refs[22],
+    )
+    gain_ref, strength_ref, decay_ref, log_decay_ref, parent_ref = small
+    high_ref, low_ref, pv_ref, gate_ref = outs
+    wq_ref, wk_ref = held
     copies = copies_in(sources, held, sems)
     start_all(copies)
-    wait_all(copies)
     group = lax.axis_index("tp")
     x = x_ref[...].astype(f32)
     scale = lax.rsqrt(jnp.mean(x * x, axis=0, keepdims=True) + epsilon)
@@ -273,14 +321,16 @@
     def rounded(x):
         return x.astype(bf16).astype(f32)
 
-    queries = rounded(project(wq_ref[...], 0))
-    keys = rounded(project(wk_ref[...], 0))
     first = iota((16, 2048), 0) == 0
     scalars = jnp.where(first, strength_ref[...].astype(f32), decay_ref[...].astype(f32))
-    logits = project(scalars.astype(bf16), 1)
+    scalars = scalars.astype(bf16)
     both = jnp.concatenate([weight_rows(packs, 0), weight_rows(packs, 16)], axis=0)
     both = rounded(project(both, 1))
     values, zgate = both[:128], both[128:]
+    logits = project(scalars, 1)
+    wait_all(copies)
+    queries = rounded(project(wq_ref[...], 0))
+    keys = rounded(project(wk_ref[...], 0))
     gain = jnp.concatenate([pack[768:, :] for pack in packs], axis=0).astype(f32)
 
     def unit(x):
@@ -318,10 +368,10 @@
     gate_ref[...] = gain * (zgate * jax.nn.sigmoid(zgate))
 
 
-def row_side(x, packs, rate, *arrays):
+def row_side(x, packs, small, rate, *weights):
     return pl.pallas_call(
         rows_kernel,
-        in_specs=vmem_specs(9) + [pl.BlockSpec(memory_space=pltpu.SMEM)] + hbm_specs(7),
+        in_specs=vmem_specs(14) + [pl.BlockSpec(memory_space=pltpu.SMEM)] + hbm_specs(2),
         out_specs=vmem_specs(4),
         out_shape=[
             pltpu.VMEM((128, 128), bf16),
@@ -329,11 +379,11 @@
             pltpu.VMEM((128, 128), f32),
             pltpu.VMEM((128, 128), f32),
         ],
-        scratch_shapes=scratch_like(arrays),
+        scratch_shapes=scratch_like(weights),
         cost_estimate=cost(2000000000, 4 << 20),
         compiler_params=pltpu.CompilerParams(vmem_limit_bytes=VMEM_LIMIT),
         name="row_side",
-    )(x, *packs, rate, *in_hbm(arrays))
+    )(x, *packs, *small, rate, *in_hbm(weights))
 
 
 def readout_kernel(high_ref, low_ref, pv_ref, gate_ref, *rest):
@@ -450,38 +500,37 @@
     accepted,
     parent,
 ):
-    sent, pack = prepare(
-        jnp.transpose(tokens, (1, 2, 0)),
-        jnp.transpose(value_weight[:, 0, :], (1, 0)),
-        jnp.transpose(output_gate_weight[:, 0, :], (1, 0)),
-        output_weight[0],
-        head_norm_gain.reshape(1, 16),
+    sent, pack, *ahead, other_rows = prepare(
+        (
+            jnp.transpose(tokens, (1, 2, 0)),
+            jnp.transpose(value_weight[:, 0, :], (1, 0)),
+            jnp.transpose(output_gate_weight[:, 0, :], (1, 0)),
+            output_weight[0],
+            head_norm_gain.reshape(1, 16),
+        ),
+        (
+            previous_keys.reshape(1024, 128),
+            jnp.transpose(previous_values[:, :, 0, :], (1, 2, 0)),
+            jnp.transpose(previous_strengths, (1, 2, 0)),
+            jnp.transpose(previous_log_decay, (1, 2, 0)),
+            accepted.reshape(1, 256),
+            input_norm_gain.reshape(16, 128),
+            jnp.transpose(strength_weight, (1, 0)),
+            jnp.transpose(decay_weight, (1, 0)),
+            jnp.transpose(proposal_log_decay, (1, 2, 0)),
+            jnp.transpose(parent, (1, 0)),
+        ),
+        state.reshape(256, 16, 128),
     )
+    ahead, small = ahead[:5], ahead[5:]
     near = [pack] + [chip_permute(pack, d) for d in (1, 2, 3)]
     x = lax.all_to_all(sent.reshape(128, 16, 128), BOTH, 0, 0, tiled=True).reshape(2048, 128)
-    accepted_state, *lows = new_state(
-        state.reshape(256, 16, 128),
-        previous_keys.reshape(1024, 128),
-        jnp.transpose(previous_values[:, :, 0, :], (1, 2, 0)),
-        jnp.transpose(previous_strengths, (1, 2, 0)),
-        jnp.transpose(previous_log_decay, (1, 2, 0)),
-        accepted.reshape(1, 256),
-    )
-    near_states = [lows[0]] + [chip_permute(lows[4 - d], d) for d in (1, 2, 3)]
+    lows = other_chips_state(other_rows, ahead)
+    accepted_state, own_low = all_chips_state(state.reshape(256, 16, 128), previous_keys.reshape(1024, 128), ahead[1:])
+    near_states = [own_low] + [chip_permute(lows[3 - d], d) for d in (1, 2, 3)]
     packs = near + [core_permute(x) for x in near]
     states = near_states + [core_permute(x) for x in near_states]
-    rows = row_side(
-        x,
-        packs,
-        head_decay_rate.reshape(1, 1),
-        input_norm_gain.reshape(16, 128),
-        query_weight,
-        key_weight,
-        jnp.transpose(strength_weight, (1, 0)),
-        jnp.transpose(decay_weight, (1, 0)),
-        jnp.transpose(proposal_log_decay, (1, 2, 0)),
-        jnp.transpose(parent, (1, 0)),
-    )
+    rows = row_side(x, packs, small, head_decay_rate.reshape(1, 1), query_weight, key_weight)
     part = readout(*rows, packs, states)
     parts = lax.all_to_all(part.reshape(16, 8, 2048), "kv", 0, 0, tiled=True)
     blocks = lax.all_to_all(sum_heads(parts), BOTH, 0, 0, tiled=True)

time: 87.1 us -> 88.1 us (1.011)
  starting transfers between devices: 22.4 us -> 23.5 us
  local copies, waits for them, and re-layouts: 4.84 us -> 5.77 us
    all_to_all x1, starting transfers between devices: 8.49 us -> 9.54 us  [whole_step(): lax.all_to_all(sent.reshape(128, 16, 128), BOTH, 0, 0, tiled=True)]
    ppermute x8, starting transfers between devices: 5.19 us -> 6.16 us  [core_permute(): return lax.ppermute(x, 'tp', [(i ^ 1, i) for i in range(8)])]
    ppermute x6, starting transfers between devices: 8.71 us -> 7.75 us  [chip_permute(): return lax.ppermute(x, 'tp', [((i + 2 * d) % 8, i) for i in range(8)])]
    pallas_call x1, Pallas kernels: 1.97 us -> 1.04 us  [readout(): pl.pallas_call(readout_kernel, in_specs=vmem_specs(20), out_specs=pl.Bloc...]
    unnamed x18 -> x20, local copies, waits for them, and re-layouts: 4.84 us -> 5.77 us
    pallas_call x3 -> x4, Pallas kernels: 11.4 us -> 11.7 us  [the longest x1 4.43 us: all_chips_state(): pl.pallas_call(all_chips_kernel, in_specs=hbm_specs(2) + vmem_specs(4), o...]
  transfers between devices with their start and end apart: 15 -> 15, of which waited for: 2 -> 3; matrix products, arithmetic and copies ran while one was open for 0% -> 0% of each run, Pallas kernels for 10% -> 10%
where the time goes in v2:
time: 88.1 us; the launch traced here: 87.7 us
  blocking collectives  31.9 us (36%)
  starting transfers between devices  23.5 us (27%)
  Pallas kernels  14 us (16%)
  waiting for transfers between devices  11.2 us (13%)
  local copies, waits for them, and re-layouts  5.77 us (7%)
  between operations  1.44 us (2%)
    all_to_all x1, blocking collectives, whole_step(): parts = lax.all_to_all(part.reshape(16, 8, 2048), 'kv', 0, 0, tiled=True)  17.9 us
    all_to_all x1, blocking collectives, whole_step(): blocks = lax.all_to_all(sum_heads(parts), BOTH, 0, 0, tiled=True)  14 us
    ppermute x6, waiting for transfers between devices, chip_permute(): return lax.ppermute(x, 'tp', [((i + 2 * d) % 8, i) for i in range(8)])  11.2 us
    all_to_all x1, starting transfers between devices, whole_step(): lax.all_to_all(sent.reshape(128, 16, 128), BOTH, 0, 0, tiled=True)  9.54 us
    ppermute x6, starting transfers between devices, chip_permute(): return lax.ppermute(x, 'tp', [((i + 2 * d) % 8, i) for i in range(8)])  7.75 us
    ppermute x8, starting transfers between devices, core_permute(): return lax.ppermute(x, 'tp', [(i ^ 1, i) for i in range(8)])  6.16 us
    unnamed x20, local copies, waits for them, and re-layouts  5.77 us
    pallas_call x1, Pallas kernels, all_chips_state(): pl.pallas_call(all_chips_kernel, in_specs=hbm_specs(2) + vmem_specs(4), o...  4.43 us
  transfers between devices with their start and end apart: 15, of which 3 were waited for; matrix products, arithmetic and copies ran while one was open for 0% of the time, Pallas kernels for 10%

profile of v2, /device:TPU:1, one launch (start us, length us, event | category | flops | bytes accessed | tf_op | source)
XLA Modules:
  0.0 87.7 jit_solution(3243326595001844415)
XLA Ops:
  0.6 2.7 %prepare.1 = (bf16[16,8,16,128]{3,2,1,0:T(8,128)(2,1)}, bf16[784,128]{1,0:T(8,128)(2,1)S(1)}, bf16[1024,128]{1,0:T(8,128)(2,1)S(1)}, bf16[4,16,256]{2,1,0:T(8,12...) custom-call(bf16[4,16,256]{2,1,0:T(8,128)(2,1)} %bitcast.48, ...), custom_call_target="tpu_custom_call" | custom-call | flops 10000000 | bytes 1048576 | tf_op jit(solution)/shard_map/prepare/pallas_call | solution.py:114
  3.4 1.5 %collective-permute-start.3 = (bf16[784,128]{1,0:T(8,128)(2,1)S(1)}, bf16[784,128]{1,0:T(8,128)(2,1)S(1)}, u32[]{:S(2)}, u32[]{:S(2)}) collective-permute-start(bf16[784,128]{1,0:T(8,128)(2,1)S(1)} %get-tuple-element.25.refs_0_.rest_0_), channel_id=1, source_target_pairs={{1,0},{0,1},{3,2},{2,3},{5,4},{4,5},{7,6},{6,7},{9,8},{8,9},{11,10... | collective-permute-start | bytes 602120 | tf_op jit(solution)/shard_map/ppermute | solution.py:478
  4.8 1.3 %collective-permute-start.2 = (bf16[784,128]{1,0:T(8,128)(2,1)S(1)}, bf16[784,128]{1,0:T(8,128)(2,1)S(1)}, u32[]{:S(2)}, u32[]{:S(2)}) collective-permute-start(bf16[784,128]{1,0:T(8,128)(2,1)S(1)} %get-tuple-element.25.refs_0_.rest_0_), channel_id=1, source_target_pairs={{6,0},{7,1},{0,2},{1,3},{2,4},{3,5},{4,6},{5,7},{14,8},{15,9},{8,1... | collective-permute-start | bytes 602120 | tf_op jit(solution)/shard_map/ppermute | solution.py:474
  6.2 1.3 %other_chips_state.1 = (bf16[1024,128]{1,0:T(8,128)(2,1)S(1)}, bf16[1024,128]{1,0:T(8,128)(2,1)S(1)}, bf16[1024,128]{1,0:T(8,128)(2,1)S(1)}) custom-call(bf16[3072,128]{1,0:T(8,128)(2,1)S(1)} %get-tuple-element.40.state_ref, bf16[1024,128]{1,0:T(8,128)(2,1)S(1)} %get-tuple-element.41.refs_0_, bf16[4,16,256]{2,1,0:T(8,128)(2,1)S(1)} %get-tuple-element.35.refs_0_.refs_1_, ...), custom_call_target="tpu_custom_call" | custom-call | flops 1500000000 | bytes 3145728 | tf_op jit(solution)/shard_map/other_chips_state/pallas_call | solution.py:203
  7.5 1.4 %collective-permute-start.7 = (bf16[1024,128]{1,0:T(8,128)(2,1)S(1)}, bf16[1024,128]{1,0:T(8,128)(2,1)S(1)}, u32[]{:S(2)}, u32[]{:S(2)}) collective-permute-start(bf16[1024,128]{1,0:T(8,128)(2,1)S(1)} %get-tuple-element.42), channel_id=1, source_target_pairs={{2,0},{3,1},{4,2},{5,3},{6,4},{7,5},{0,6},{1,7},{10,8},{11,9},{12,... | collective-permute-start | bytes 786440 | tf_op jit(solution)/shard_map/ppermute | solution.py:474
  8.9 9.5 %all-to-all-start = ((bf16[128,16,128]{2,1,0:T(8,128)(2,1)}), bf16[128,16,128]{2,1,0:T(8,128)(2,1)S(1)}, u32[]{:S(2)}, u32[]{:S(2)}) async-start(bf16[128,16,128]{2,1,0:T(8,128)(2,1)} %bitcast.19), calls=%async_computation | async-start | bytes 1048576 | tf_op jit(solution)/shard_map/all_to_all | solution.py:527
  18.5 2.9 %collective-permute-start.1 = (bf16[784,128]{1,0:T(8,128)(2,1)S(1)}, bf16[784,128]{1,0:T(8,128)(2,1)S(1)}, u32[]{:S(2)}, u32[]{:S(2)}) collective-permute-start(bf16[784,128]{1,0:T(8,128)(2,1)S(1)} %get-tuple-element.25.refs_0_.rest_0_), channel_id=1, source_target_pairs={{4,0},{5,1},{6,2},{7,3},{0,4},{1,5},{2,6},{3,7},{12,8},{13,9},{14,... | collective-permute-start | bytes 602120 | tf_op jit(solution)/shard_map/ppermute | solution.py:474
  21.4 0.9 %collective-permute-start = (bf16[784,128]{1,0:T(8,128)(2,1)S(1)}, bf16[784,128]{1,0:T(8,128)(2,1)S(1)}, u32[]{:S(2)}, u32[]{:S(2)}) collective-permute-start(bf16[784,128]{1,0:T(8,128)(2,1)S(1)} %get-tuple-element.25.refs_0_.rest_0_), channel_id=1, source_target_pairs={{2,0},{3,1},{4,2},{5,3},{6,4},{7,5},{0,6},{1,7},{10,8},{11,9},{12,... | collective-permute-start | bytes 602120 | tf_op jit(solution)/shard_map/ppermute | solution.py:474
  22.3 0.0 collective-permute-done.3.refs_4_.rest_4_
  22.3 1.2 %collective-permute-start.8 = (bf16[1024,128]{1,0:T(8,128)(2,1)S(1)}, bf16[1024,128]{1,0:T(8,128)(2,1)S(1)}, u32[]{:S(2)}, u32[]{:S(2)}) collective-permute-start(bf16[1024,128]{1,0:T(8,128)(2,1)S(1)} %get-tuple-element.43), channel_id=1, source_target_pairs={{4,0},{5,1},{6,2},{7,3},{0,4},{1,5},{2,6},{3,7},{12,8},{13,9},{14,... | collective-permute-start | bytes 786440 | tf_op jit(solution)/shard_map/ppermute | solution.py:474
  23.5 0.0 collective-permute-done.2.refs_3_.rest_3_
  23.5 0.0 collective-permute-start.9
  23.5 7.8 %collective-permute-done.1.refs_2_.rest_2_ = bf16[784,128]{1,0:T(8,128)(2,1)S(1)} collective-permute-done((bf16[784,128]{1,0:T(8,128)(2,1)S(1)}, bf16[784,128]{1,0:T(8,128)(2,1)S(1)}, u32[]{:S(2)}, u32[]{:S(2)}) %collective-permute-start.1) | collective-permute-done | bytes 200736 | tf_op jit(solution)/shard_map/ppermute | solution.py:474
  31.3 1.5 %collective-permute-start.6 = (bf16[784,128]{1,0:T(8,128)(2,1)S(1)}, bf16[784,128]{1,0:T(8,128)(2,1)S(1)}, u32[]{:S(2)}, u32[]{:S(2)}) collective-permute-start(bf16[784,128]{1,0:T(8,128)(2,1)S(1)} %collective-permute-done.2.refs_3_.rest_3_), channel_id=1, source_target_pairs={{1,0},{0,1},{3,2},{2,3},{5,4},{4,5},{7,6},{6,7},{9,8},{8,9},{11,10... | collective-permute-start | bytes 602120 | tf_op jit(solution)/shard_map/ppermute | solution.py:478
  32.8 1.3 %collective-permute-done.refs_1_.rest_1_ = bf16[784,128]{1,0:T(8,128)(2,1)S(1)} collective-permute-done((bf16[784,128]{1,0:T(8,128)(2,1)S(1)}, bf16[784,128]{1,0:T(8,128)(2,1)S(1)}, u32[]{:S(2)}, u32[]{:S(2)}) %collective-permute-start) | collective-permute-done | bytes 200736 | tf_op jit(solution)/shard_map/ppermute | solution.py:474
  34.0 1.5 %collective-permute-start.5 = (bf16[784,128]{1,0:T(8,128)(2,1)S(1)}, bf16[784,128]{1,0:T(8,128)(2,1)S(1)}, u32[]{:S(2)}, u32[]{:S(2)}) collective-permute-start(bf16[784,128]{1,0:T(8,128)(2,1)S(1)} %collective-permute-done.1.refs_2_.rest_2_), channel_id=1, source_target_pairs={{1,0},{0,1},{3,2},{2,3},{5,4},{4,5},{7,6},{6,7},{9,8},{8,9},{11,10... | collective-permute-start | bytes 602120 | tf_op jit(solution)/shard_map/ppermute | solution.py:478
  35.6 0.0 collective-permute-done.7.rest_9_
  35.6 0.1 collective-permute-start.4
  35.7 4.4 %all_chips_state.1 = (f32[256,16,128]{2,1,0:T(8,128)}, bf16[1024,128]{1,0:T(8,128)(2,1)S(1)}) custom-call(f32[256,16,128]{2,1,0:T(8,128)} %bitcast.42, bf16[1024,128]{1,0:T(8,128)(2,1)} %bitcast.44, bf16[4,16,256]{2,1,0:T(8,128)(2,1)S(1)} %get-tuple-element.35.refs_0_.refs_1_, f32[4,1,256]{2,1,0:T(1,128)S(1)} %get-tuple-element.36.refs_1_.refs_2_, ...), custom_call_target="tpu_custom_call" | custom-call | flops 2000000000 | bytes 4194304 | tf_op jit(solution)/shard_map/all_chips_state/pallas_call | solution.py:250
  40.1 0.0 copy-done
  40.1 0.0 collective-permute-done.8.rest_10_
  40.1 0.5 collective-permute-start.10
  40.6 2.2 %collective-permute-done.9.rest_11_ = bf16[1024,128]{1,0:T(8,128)(2,1)S(1)} collective-permute-done((bf16[1024,128]{1,0:T(8,128)(2,1)S(1)}, bf16[1024,128]{1,0:T(8,128)(2,1)S(1)}, u32[]{:S(2)}, u32[]{:S(2)}) %collective-permute-start.9) | collective-permute-done | bytes 262176 | tf_op jit(solution)/shard_map/ppermute | solution.py:474
  42.8 0.5 collective-permute-start.11
  43.3 0.0 collective-permute-done.6.refs_7_.rest_7_
  43.3 0.7 copy-done.2
  44.0 0.0 collective-permute-start.12
  44.0 0.0 collective-permute-done.5.refs_6_.rest_6_
  44.0 0.7 copy-done.4
  44.7 0.5 collective-permute-start.13
  45.9 0.0 collective-permute-done.4.refs_5_.rest_5_
  45.9 0.7 copy-done.7
  46.6 0.0 all-to-all-done
  46.6 0.9 %copy-done.1 = bf16[784,128]{1,0:T(8,128)(2,1)S(1)} copy-done((bf16[784,128]{1,0:T(8,128)(2,1)S(1)}, bf16[784,128]{1,0:T(8,128)(2,1)}, u32[]{:S(2)}) %copy-start.1) | copy-done | bytes 200728
  47.5 0.9 %copy-done.3 = bf16[784,128]{1,0:T(8,128)(2,1)S(1)} copy-done((bf16[784,128]{1,0:T(8,128)(2,1)S(1)}, bf16[784,128]{1,0:T(8,128)(2,1)}, u32[]{:S(2)}) %copy-start.3) | copy-done | bytes 200728
  48.4 0.9 %copy-done.5 = bf16[784,128]{1,0:T(8,128)(2,1)S(1)} copy-done((bf16[784,128]{1,0:T(8,128)(2,1)S(1)}, bf16[784,128]{1,0:T(8,128)(2,1)}, u32[]{:S(2)}) %copy-start.5) | copy-done | bytes 200728
  49.4 0.9 %copy-done.8 = bf16[784,128]{1,0:T(8,128)(2,1)S(1)} copy-done((bf16[784,128]{1,0:T(8,128)(2,1)S(1)}, bf16[784,128]{1,0:T(8,128)(2,1)}, u32[]{:S(2)}) %copy-start.8) | copy-done | bytes 200728
  50.3 3.2 %row_side.1 = (bf16[128,128]{1,0:T(8,128)(2,1)S(1)}, bf16[128,128]{1,0:T(8,128)(2,1)S(1)}, f32[128,128]{1,0:T(8,128)S(1)}, f32[128,128]{1,0:T(8,128)S(1)}) custom-call(bf16[2048,128]{1,0:T(8,128)(2,1)S(1)} %bitcast.37, bf16[784,128]{1,0:T(8,128)(2,1)S(1)} %get-tuple-element.25.refs_0_.rest_0_, bf16[784,128]{1,0:T(8,128)(2,1)S(1)} %copy-done.1, ...), custom_call_target="tpu_custom_call" | custom-call | flops 2000000000 | bytes 4194304 | tf_op jit(solution)/shard_map/row_side/pallas_call | solution.py:372
  53.5 0.0 collective-permute-done.10.rest_12_
  53.5 0.0 collective-permute-done.11.rest_13_
  53.5 0.0 collective-permute-done.12.rest_14_
  53.5 0.0 collective-permute-done.13.rest_15_
  53.5 0.0 copy-start.9
  53.5 1.0 %readout.1 = bf16[128,2048]{1,0:T(8,128)(2,1)S(1)} custom-call(bf16[128,128]{1,0:T(8,128)(2,1)S(1)} %get-tuple-element.31.high_ref, bf16[128,128]{1,0:T(8,128)(2,1)S(1)} %get-tuple-element.32.low_ref, f32[128,128]{1,0:T(8,128)S(1)} %get-tuple-element.33.pv_ref, f32[128,128]{1,0:T(8,128)S(1)} %get-tuple-element.34.gate_ref, ...), custom_call_target="tpu_custom_call" | custom-call | flops 500000000 | bytes 3145728 | tf_op jit(solution)/shard_map/readout/pallas_call | solution.py:405
  54.6 17.9 %all_to_all.21.part_ref = bf16[16,8,2048]{2,1,0:T(8,128)(2,1)S(1)} all-to-all(bf16[16,8,2048]{2,1,0:T(8,128)(2,1)S(1)} %bitcast.36), channel_id=1, replica_groups=mesh['kv'=16,'tp'=8] {'kv'}, dimensions={0} | all-to-all | bytes 1048576 | tf_op jit(solution)/shard_map/all_to_all | solution.py:535
  72.5 0.3 sum_heads.1
  72.7 14.0 %all_to_all.22 = f32[128,1,128]{2,1,0:T(1,128)S(1)} all-to-all(f32[128,1,128]{2,1,0:T(1,128)S(1)} %bitcast.38), channel_id=1, replica_groups=mesh['kv'=16,'tp'=8] {'kv','tp'}, dimensions={0} | all-to-all | bytes 131072 | tf_op jit(solution)/shard_map/all_to_all | solution.py:536
  86.7 1.0 %final_rows.1 = bf16[4,16,256]{2,1,0:T(8,128)(2,1)} custom-call(f32[128,128]{1,0:T(8,128)S(1)} %bitcast.39, bf16[1,16]{1,0:T(2,128)(2,1)S(1)} %bitcast.40), custom_call_target="tpu_custom_call" | custom-call | flops 10000000 | bytes 262144 | tf_op jit(solution)/shard_map/final_rows/pallas_call | solution.py:461
  (11 shorter events, 0.0 us)
Async XLA Ops:
  3.4 18.9 %collective-permute-start.3 = (bf16[784,128]{1,0:T(8,128)(2,1)S(1)}, bf16[784,128]{1,0:T(8,128)(2,1)S(1)}, u32[]{:S(2)}, u32[]{:S(2)}) collective-permute-start(bf16[784,128]{1,0:T(8,128)(2,1)S(1)} %get-tuple-element.25.refs_0_.rest_0_), channel_id=1, source_target_pairs={{1,0},{0,1},{3,2},{2,3},{5,4},{4,5},{7,6},{6,7},{9,8},{8,9},{11,10... | collective-permute-start | bytes 602120 | tf_op jit(solution)/shard_map/ppermute | solution.py:478
  4.8 18.7 %collective-permute-start.2 = (bf16[784,128]{1,0:T(8,128)(2,1)S(1)}, bf16[784,128]{1,0:T(8,128)(2,1)S(1)}, u32[]{:S(2)}, u32[]{:S(2)}) collective-permute-start(bf16[784,128]{1,0:T(8,128)(2,1)S(1)} %get-tuple-element.25.refs_0_.rest_0_), channel_id=1, source_target_pairs={{6,0},{7,1},{0,2},{1,3},{2,4},{3,5},{4,6},{5,7},{14,8},{15,9},{8,1... | collective-permute-start | bytes 602120 | tf_op jit(solution)/shard_map/ppermute | solution.py:474
  7.5 28.1 %collective-permute-start.7 = (bf16[1024,128]{1,0:T(8,128)(2,1)S(1)}, bf16[1024,128]{1,0:T(8,128)(2,1)S(1)}, u32[]{:S(2)}, u32[]{:S(2)}) collective-permute-start(bf16[1024,128]{1,0:T(8,128)(2,1)S(1)} %get-tuple-element.42), channel_id=1, source_target_pairs={{2,0},{3,1},{4,2},{5,3},{6,4},{7,5},{0,6},{1,7},{10,8},{11,9},{12,... | collective-permute-start | bytes 786440 | tf_op jit(solution)/shard_map/ppermute | solution.py:474
  8.9 37.6 %all-to-all-start = ((bf16[128,16,128]{2,1,0:T(8,128)(2,1)}), bf16[128,16,128]{2,1,0:T(8,128)(2,1)S(1)}, u32[]{:S(2)}, u32[]{:S(2)}) async-start(bf16[128,16,128]{2,1,0:T(8,128)(2,1)} %bitcast.19), calls=%async_computation | async-start | bytes 1048576 | tf_op jit(solution)/shard_map/all_to_all | solution.py:527
  18.5 12.8 %collective-permute-start.1 = (bf16[784,128]{1,0:T(8,128)(2,1)S(1)}, bf16[784,128]{1,0:T(8,128)(2,1)S(1)}, u32[]{:S(2)}, u32[]{:S(2)}) collective-permute-start(bf16[784,128]{1,0:T(8,128)(2,1)S(1)} %get-tuple-element.25.refs_0_.rest_0_), channel_id=1, source_target_pairs={{4,0},{5,1},{6,2},{7,3},{0,4},{1,5},{2,6},{3,7},{12,8},{13,9},{14,... | collective-permute-start | bytes 602120 | tf_op jit(solution)/shard_map/ppermute | solution.py:474
  21.4 12.6 %collective-permute-start = (bf16[784,128]{1,0:T(8,128)(2,1)S(1)}, bf16[784,128]{1,0:T(8,128)(2,1)S(1)}, u32[]{:S(2)}, u32[]{:S(2)}) collective-permute-start(bf16[784,128]{1,0:T(8,128)(2,1)S(1)} %get-tuple-element.25.refs_0_.rest_0_), channel_id=1, source_target_pairs={{2,0},{3,1},{4,2},{5,3},{6,4},{7,5},{0,6},{1,7},{10,8},{11,9},{12,... | collective-permute-start | bytes 602120 | tf_op jit(solution)/shard_map/ppermute | solution.py:474
  22.3 17.8 %collective-permute-start.8 = (bf16[1024,128]{1,0:T(8,128)(2,1)S(1)}, bf16[1024,128]{1,0:T(8,128)(2,1)S(1)}, u32[]{:S(2)}, u32[]{:S(2)}) collective-permute-start(bf16[1024,128]{1,0:T(8,128)(2,1)S(1)} %get-tuple-element.43), channel_id=1, source_target_pairs={{4,0},{5,1},{6,2},{7,3},{0,4},{1,5},{2,6},{3,7},{12,8},{13,9},{14,... | collective-permute-start | bytes 786440 | tf_op jit(solution)/shard_map/ppermute | solution.py:474
  23.5 19.3 %collective-permute-start.9 = (bf16[1024,128]{1,0:T(8,128)(2,1)S(1)}, bf16[1024,128]{1,0:T(8,128)(2,1)S(1)}, u32[]{:S(2)}, u32[]{:S(2)}) collective-permute-start(bf16[1024,128]{1,0:T(8,128)(2,1)S(1)} %get-tuple-element.44), channel_id=1, source_target_pairs={{6,0},{7,1},{0,2},{1,3},{2,4},{3,5},{4,6},{5,7},{14,8},{15,9},{8,1... | collective-permute-start | bytes 786440 | tf_op jit(solution)/shard_map/ppermute | solution.py:474
  31.3 12.1 %collective-permute-start.6 = (bf16[784,128]{1,0:T(8,128)(2,1)S(1)}, bf16[784,128]{1,0:T(8,128)(2,1)S(1)}, u32[]{:S(2)}, u32[]{:S(2)}) collective-permute-start(bf16[784,128]{1,0:T(8,128)(2,1)S(1)} %collective-permute-done.2.refs_3_.rest_3_), channel_id=1, source_target_pairs={{1,0},{0,1},{3,2},{2,3},{5,4},{4,5},{7,6},{6,7},{9,8},{8,9},{11,10... | collective-permute-start | bytes 602120 | tf_op jit(solution)/shard_map/ppermute | solution.py:478
  34.0 6.1 %copy-start = (bf16[784,128]{1,0:T(8,128)(2,1)}, bf16[784,128]{1,0:T(8,128)(2,1)S(1)}, u32[]{:S(2)}) copy-start(bf16[784,128]{1,0:T(8,128)(2,1)S(1)} %collective-permute-done.refs_1_.rest_1_) | copy-start | bytes 602116
  34.0 10.0 %collective-permute-start.5 = (bf16[784,128]{1,0:T(8,128)(2,1)S(1)}, bf16[784,128]{1,0:T(8,128)(2,1)S(1)}, u32[]{:S(2)}, u32[]{:S(2)}) collective-permute-start(bf16[784,128]{1,0:T(8,128)(2,1)S(1)} %collective-permute-done.1.refs_2_.rest_2_), channel_id=1, source_target_pairs={{1,0},{0,1},{3,2},{2,3},{5,4},{4,5},{7,6},{6,7},{9,8},{8,9},{11,10... | collective-permute-start | bytes 602120 | tf_op jit(solution)/shard_map/ppermute | solution.py:478
  35.6 10.3 %collective-permute-start.4 = (bf16[784,128]{1,0:T(8,128)(2,1)S(1)}, bf16[784,128]{1,0:T(8,128)(2,1)S(1)}, u32[]{:S(2)}, u32[]{:S(2)}) collective-permute-start(bf16[784,128]{1,0:T(8,128)(2,1)S(1)} %collective-permute-done.refs_1_.rest_1_), channel_id=1, source_target_pairs={{1,0},{0,1},{3,2},{2,3},{5,4},{4,5},{7,6},{6,7},{9,8},{8,9},{11,10... | collective-permute-start | bytes 602120 | tf_op jit(solution)/shard_map/ppermute | solution.py:478
  40.1 13.3 %collective-permute-start.10 = (bf16[1024,128]{1,0:T(8,128)(2,1)S(1)}, bf16[1024,128]{1,0:T(8,128)(2,1)S(1)}, u32[]{:S(2)}, u32[]{:S(2)}) collective-permute-start(bf16[1024,128]{1,0:T(8,128)(2,1)S(1)} %get-tuple-element.39.rest_8_), channel_id=1, source_target_pairs={{1,0},{0,1},{3,2},{2,3},{5,4},{4,5},{7,6},{6,7},{9,8},{8,9},{11,10... | collective-permute-start | bytes 786440 | tf_op jit(solution)/shard_map/ppermute | solution.py:478
  42.8 10.7 %collective-permute-start.11 = (bf16[1024,128]{1,0:T(8,128)(2,1)S(1)}, bf16[1024,128]{1,0:T(8,128)(2,1)S(1)}, u32[]{:S(2)}, u32[]{:S(2)}) collective-permute-start(bf16[1024,128]{1,0:T(8,128)(2,1)S(1)} %collective-permute-done.7.rest_9_), channel_id=1, source_target_pairs={{1,0},{0,1},{3,2},{2,3},{5,4},{4,5},{7,6},{6,7},{9,8},{8,9},{11,10... | collective-permute-start | bytes 786440 | tf_op jit(solution)/shard_map/ppermute | solution.py:478
  43.3 0.7 copy-start.2
  44.0 9.5 %collective-permute-start.12 = (bf16[1024,128]{1,0:T(8,128)(2,1)S(1)}, bf16[1024,128]{1,0:T(8,128)(2,1)S(1)}, u32[]{:S(2)}, u32[]{:S(2)}) collective-permute-start(bf16[1024,128]{1,0:T(8,128)(2,1)S(1)} %collective-permute-done.8.rest_10_), channel_id=1, source_target_pairs={{1,0},{0,1},{3,2},{2,3},{5,4},{4,5},{7,6},{6,7},{9,8},{8,9},{11,10... | collective-permute-start | bytes 786440 | tf_op jit(solution)/shard_map/ppermute | solution.py:478
  44.0 0.7 copy-start.4
  44.7 8.8 %collective-permute-start.13 = (bf16[1024,128]{1,0:T(8,128)(2,1)S(1)}, bf16[1024,128]{1,0:T(8,128)(2,1)S(1)}, u32[]{:S(2)}, u32[]{:S(2)}) collective-permute-start(bf16[1024,128]{1,0:T(8,128)(2,1)S(1)} %collective-permute-done.9.rest_11_), channel_id=1, source_target_pairs={{1,0},{0,1},{3,2},{2,3},{5,4},{4,5},{7,6},{6,7},{9,8},{8,9},{11,10... | collective-permute-start | bytes 786440 | tf_op jit(solution)/shard_map/ppermute | solution.py:478
  45.9 0.7 copy-start.7
  46.6 0.9 %copy-start.1 = (bf16[784,128]{1,0:T(8,128)(2,1)S(1)}, bf16[784,128]{1,0:T(8,128)(2,1)}, u32[]{:S(2)}) copy-start(bf16[784,128]{1,0:T(8,128)(2,1)} %copy-done) | copy-start | bytes 602116
  47.5 0.9 %copy-start.3 = (bf16[784,128]{1,0:T(8,128)(2,1)S(1)}, bf16[784,128]{1,0:T(8,128)(2,1)}, u32[]{:S(2)}) copy-start(bf16[784,128]{1,0:T(8,128)(2,1)} %copy-done.2) | copy-start | bytes 602116
  48.4 0.9 %copy-start.5 = (bf16[784,128]{1,0:T(8,128)(2,1)S(1)}, bf16[784,128]{1,0:T(8,128)(2,1)}, u32[]{:S(2)}) copy-start(bf16[784,128]{1,0:T(8,128)(2,1)} %copy-done.4) | copy-start | bytes 602116
  49.4 0.9 %copy-start.8 = (bf16[784,128]{1,0:T(8,128)(2,1)S(1)}, bf16[784,128]{1,0:T(8,128)(2,1)}, u32[]{:S(2)}) copy-start(bf16[784,128]{1,0:T(8,128)(2,1)} %copy-done.7) | copy-start | bytes 602116
  50.3 3.2 %copy-start.6 = (bf16[784,128]{1,0:T(8,128)(2,1)S(1)}, bf16[784,128]{1,0:T(8,128)(2,1)}, u32[]{:S(2)}) copy-start(bf16[784,128]{1,0:T(8,128)(2,1)} %copy-done.4) | copy-start | bytes 602116
  53.5 33.2 %copy-start.9 = (bf16[16]{0:T(256)(128)(2,1)S(1)}, bf16[16]{0:T(256)(128)(2,1)}, u32[]{:S(2)}) copy-start(bf16[16]{0:T(256)(128)(2,1)} %param.32) | copy-start | bytes 100

commit v3 on v2

--- a/solution.py
+++ b/solution.py
@@ -12,6 +12,7 @@
 BOTH = ("kv", "tp")
 VMEM_LIMIT = 16 << 20
 PACK = 784
+BUNDLE = 1024 + PACK
 
 
 def dot(a, b, ca, cb):
@@ -24,11 +25,6 @@
 
 def roll(x, shift):
     return pltpu.roll(x, shift, 1)
-
-
-def split(x):
-    hi = x.astype(bf16)
-    return hi, (x - hi.astype(f32)).astype(bf16)
 
 
 def cost(flops, size):
@@ -88,36 +84,49 @@
 
 
 def prepare_kernel(*refs):
-    sources, state_source, (sent_ref, pack_ref), kept, rest = refs[:15], refs[15], refs[16:18], refs[18:28], refs[28:]
+    sources, state_source, (sent_ref, pack_ref, bundle_ref), kept, rest = (
+        refs[:15], refs[15], refs[16:19], refs[19:29], refs[29:],
+    )
     low_ref, held, sems, state_ref = rest[0], rest[1:6], rest[6:9], rest[9]
     copies = copies_in(sources[:5], held, sems[0])
     ahead = copies_in(sources[5:], kept, sems[1])
     chip = lax.axis_index("tp") // 2
-    for i in range(3):
-        rows = pl.ds(pl.multiple_of(64 * lax.rem(chip + 1 + i, 4), 64), 64)
-        ahead.append(pltpu.make_async_copy(state_source.at[rows], state_ref.at[pl.ds(64 * i, 64)], sems[2].at[i]))
-    start_all(copies + ahead)
+    loads = []
+    for i, offset in enumerate((2, 1, 3)):
+        rows = pl.ds(pl.multiple_of(64 * lax.rem(chip + offset, 4), 64), 64)
+        loads.append(pltpu.make_async_copy(state_source.at[rows], state_ref.at[pl.ds(64 * i, 64)], sems[2].at[i]))
+    start_all(copies + ahead + loads)
     wait_all(copies[1:])
     pack_weights(*held[1:], pack_ref)
+    bundle_ref[1024:, :] = pack_ref[...]
     copies[0].wait()
     rows = [held[0][i].astype(f32) for i in range(4)]
     for t in range(8):
         block = chunk_lanes(rows, t).astype(bf16)
         for k in range(16):
             sent_ref[k, t] = block
-    wait_all(ahead)
-    for i in range(6):
-        low_ref[512 * i : 512 * i + 512, :] = state_ref[32 * i : 32 * i + 32].reshape(512, 128).astype(bf16)
+    wait_all(ahead + loads[:1])
+
+    def read(step):
+        return state_ref[32 * step : 32 * step + 32].reshape(512, 128)
+
+    def emit(step, new):
+        bundle_ref[512 * step : 512 * step + 512, :] = new.astype(bf16)
+
+    state_update((2,), kept[:5], read, emit)
+    wait_all(loads[1:])
+    for i in range(4):
+        low_ref[512 * i : 512 * i + 512, :] = read(2 + i).astype(bf16)
 
 
 def prepare(first, ahead, state):
     return pl.pallas_call(
         prepare_kernel,
         in_specs=hbm_specs(16),
-        out_specs=vmem_specs(13),
-        out_shape=[pltpu.VMEM((16, 8, 16, 128), bf16), pltpu.VMEM((PACK, 128), bf16)]
+        out_specs=vmem_specs(14),
+        out_shape=[pltpu.VMEM((16, 8, 16, 128), bf16), pltpu.VMEM((PACK, 128), bf16), pltpu.VMEM((BUNDLE, 128), bf16)]
         + [pltpu.VMEM(x.shape, x.dtype) for x in ahead]
-        + [pltpu.VMEM((3072, 128), bf16)],
+        + [pltpu.VMEM((2048, 128), bf16)],
         scratch_shapes=scratch_like(first)
         + [pltpu.SemaphoreType.DMA((10,)), pltpu.SemaphoreType.DMA((3,)), pltpu.VMEM((192, 16, 128), f32)],
         cost_estimate=cost(10000000, 1 << 20),
@@ -196,16 +205,16 @@
     def emit(step, new):
         lows[step // 2][512 * (step % 2) : 512 * (step % 2) + 512, :] = new.astype(bf16)
 
-    state_update((1, 2, 3), operands, lambda step: state_ref[512 * step : 512 * step + 512, :], emit)
+    state_update((1, 3), operands, lambda step: state_ref[512 * step : 512 * step + 512, :], emit)
 
 
 def other_chips_state(state, operands):
     return pl.pallas_call(
         other_chips_kernel,
         in_specs=vmem_specs(6),
-        out_specs=vmem_specs(3),
-        out_shape=[pltpu.VMEM((1024, 128), bf16)] * 3,
-        cost_estimate=cost(1500000000, 3 << 20),
+        out_specs=vmem_specs(2),
+        out_shape=[pltpu.VMEM((1024, 128), bf16)] * 2,
+        cost_estimate=cost(1000000000, 2 << 20),
         compiler_params=pltpu.CompilerParams(vmem_limit_bytes=VMEM_LIMIT),
         name="other_chips_state",
     )(state, *operands)
@@ -286,22 +295,24 @@
     pack_ref[768:, :] = gain
 
 
+def pack_rows(ref, first, count):
+    base = ref.shape[0] - PACK
+    return ref[base + first : base + first + count, :]
+
+
 def weight_rows(packs, first):
     return jnp.concatenate(
-        [
-            jnp.concatenate([x[48 * b + first : 48 * b + first + 16, :] for x in packs], axis=0)
-            for b in range(16)
-        ],
+        [stack([pack_rows(x, 48 * b + first, 16) for x in packs]) for b in range(16)],
         axis=1,
     )
 
 
 def rows_kernel(x_ref, *refs):
     packs, small, rate_ref, sources, outs, held, sems = (
-        refs[:8], refs[8:13], refs[13], refs[14:16], refs[16:20], refs[20:22], refs[22],
+        refs[:8], refs[8:13], refs[13], refs[14:16], refs[16:19], refs[19:21], refs[21],
     )
     gain_ref, strength_ref, decay_ref, log_decay_ref, parent_ref = small
-    high_ref, low_ref, pv_ref, gate_ref = outs
+    probe_ref, pv_ref, gate_ref = outs
     wq_ref, wk_ref = held
     copies = copies_in(sources, held, sems)
     start_all(copies)
@@ -331,7 +342,7 @@
     wait_all(copies)
     queries = rounded(project(wq_ref[...], 0))
     keys = rounded(project(wk_ref[...], 0))
-    gain = jnp.concatenate([pack[768:, :] for pack in packs], axis=0).astype(f32)
+    gain = jnp.concatenate([pack_rows(pack, 768, 16) for pack in packs], axis=0).astype(f32)
 
     def unit(x):
         return x * lax.rsqrt(jnp.sum(x * x, axis=0, keepdims=True) + epsilon)
@@ -363,7 +374,7 @@
         return reach[0] * x + sum(reach[d] * roll(x, 32 * d) for d in (1, 2, 3))
 
     probe = jnp.exp(gam) * queries - reached(solved_keys)
-    high_ref[...], low_ref[...] = split(probe)
+    probe_ref[...] = probe.astype(bf16)
     pv_ref[...] = reached(solved_values)
     gate_ref[...] = gain * (zgate * jax.nn.sigmoid(zgate))
 
@@ -372,9 +383,8 @@
     return pl.pallas_call(
         rows_kernel,
         in_specs=vmem_specs(14) + [pl.BlockSpec(memory_space=pltpu.SMEM)] + hbm_specs(2),
-        out_specs=vmem_specs(4),
+        out_specs=vmem_specs(3),
         out_shape=[
-            pltpu.VMEM((128, 128), bf16),
             pltpu.VMEM((128, 128), bf16),
             pltpu.VMEM((128, 128), f32),
             pltpu.VMEM((128, 128), f32),
@@ -386,14 +396,14 @@
     )(x, *packs, *small, rate, *in_hbm(weights))
 
 
-def readout_kernel(high_ref, low_ref, pv_ref, gate_ref, *rest):
+def readout_kernel(probe_ref, pv_ref, gate_ref, *rest):
     packs, states, out_ref = rest[:8], rest[8:16], rest[16]
     core = lax.rem(lax.axis_index("tp"), 2)
     own = iota((32, 16, 128), 0) == iota((32, 16, 128), 2) % 32
     pieces = []
     for state in states:
         block = state[pl.ds(pl.multiple_of(512 * core, 512), 512), :]
-        read = dot(block, high_ref[...], 1, 0) + dot(block, low_ref[...], 1, 0)
+        read = dot(block, probe_ref[...], 1, 0)
         pieces.append(jnp.sum(jnp.where(own, read.reshape(32, 16, 128), 0.0), axis=0))
     o = jnp.concatenate(pieces, axis=0) + pv_ref[...]
     o = o * lax.rsqrt(jnp.mean(o * o, axis=0, keepdims=True) + epsilon)
@@ -401,16 +411,16 @@
     out_ref[...] = dot(o, weight_rows(packs, 32), 0, 0).astype(bf16)
 
 
-def readout(high, low, pv, gate, packs, states):
+def readout(probe, pv, gate, packs, states):
     return pl.pallas_call(
         readout_kernel,
-        in_specs=vmem_specs(20),
+        in_specs=vmem_specs(19),
         out_specs=pl.BlockSpec(memory_space=pltpu.VMEM),
         out_shape=pltpu.VMEM((128, 2048), bf16),
         cost_estimate=cost(500000000, 3 << 20),
         compiler_params=pltpu.CompilerParams(vmem_limit_bytes=VMEM_LIMIT),
         name="readout",
-    )(high, low, pv, gate, *packs, *states)
+    )(probe, pv, gate, *packs, *states)
 
 
 def total_kernel(part_ref, out_ref):
@@ -500,7 +510,7 @@
     accepted,
     parent,
 ):
-    sent, pack, *ahead, other_rows = prepare(
+    sent, pack, bundle, *ahead, other_rows = prepare(
         (
             jnp.transpose(tokens, (1, 2, 0)),
             jnp.transpose(value_weight[:, 0, :], (1, 0)),
@@ -523,13 +533,14 @@
         state.reshape(256, 16, 128),
     )
     ahead, small = ahead[:5], ahead[5:]
-    near = [pack] + [chip_permute(pack, d) for d in (1, 2, 3)]
+    near = [pack, chip_permute(pack, 1), chip_permute(bundle, 2), chip_permute(pack, 3)]
     x = lax.all_to_all(sent.reshape(128, 16, 128), BOTH, 0, 0, tiled=True).reshape(2048, 128)
     lows = other_chips_state(other_rows, ahead)
     accepted_state, own_low = all_chips_state(state.reshape(256, 16, 128), previous_keys.reshape(1024, 128), ahead[1:])
-    near_states = [own_low] + [chip_permute(lows[3 - d], d) for d in (1, 2, 3)]
+    one, three = chip_permute(lows[1], 1), chip_permute(lows[0], 3)
     packs = near + [core_permute(x) for x in near]
-    states = near_states + [core_permute(x) for x in near_states]
+    partner_low = core_permute(own_low)
+    states = [own_low, one, near[2], three, partner_low, core_permute(one), packs[6], core_permute(three)]
     rows = row_side(x, packs, small, head_decay_rate.reshape(1, 1), query_weight, key_weight)
     part = readout(*rows, packs, states)
     parts = lax.all_to_all(part.reshape(16, 8, 2048), "kv", 0, 0, tiled=True)

time: 88.1 us -> 81.5 us (0.925)
  waiting for transfers between devices: 11.2 us -> 4.61 us
  blocking collectives: 31.9 us -> 33.5 us
  starting transfers between devices: 23.5 us -> 22.2 us
    ppermute x6 -> x5, waiting for transfers between devices: 11.2 us -> 4.58 us  [chip_permute(): return lax.ppermute(x, 'tp', [((i + 2 * d) % 8, i) for i in range(8)])]
    all_to_all x1, blocking collectives: 14 us -> 15.9 us  [whole_step(): blocks = lax.all_to_all(sum_heads(parts), BOTH, 0, 0, tiled=True)]
    ppermute x6 -> x5, starting transfers between devices: 7.75 us -> 9.26 us  [chip_permute(): return lax.ppermute(x, 'tp', [((i + 2 * d) % 8, i) for i in range(8)])]
    ppermute x8 -> x7, starting transfers between devices: 6.16 us -> 4.75 us  [core_permute(): return lax.ppermute(x, 'tp', [(i ^ 1, i) for i in range(8)])]
    all_to_all x1, starting transfers between devices: 9.54 us -> 8.22 us  [whole_step(): lax.all_to_all(sent.reshape(128, 16, 128), BOTH, 0, 0, tiled=True)]
    unnamed x20 -> x22, local copies, waits for them, and re-layouts: 5.77 us -> 5.09 us
  transfers between devices with their start and end apart: 15 -> 13, of which waited for: 3 -> 1; matrix products, arithmetic and copies ran while one was open for 0% -> 0% of each run, Pallas kernels for 10% -> 11%
where the time goes in v3:
time: 81.5 us; the launch traced here: 81.1 us
  blocking collectives  33.5 us (41%)
  starting transfers between devices  22.2 us (27%)
  Pallas kernels  14.1 us (17%)
  local copies, waits for them, and re-layouts  5.09 us (6%)
  waiting for transfers between devices  4.61 us (6%)
  between operations  1.45 us (2%)
    all_to_all x1, blocking collectives, whole_step(): parts = lax.all_to_all(part.reshape(16, 8, 2048), 'kv', 0, 0, tiled=True)  17.6 us
    all_to_all x1, blocking collectives, whole_step(): blocks = lax.all_to_all(sum_heads(parts), BOTH, 0, 0, tiled=True)  15.9 us
    ppermute x5, starting transfers between devices, chip_permute(): return lax.ppermute(x, 'tp', [((i + 2 * d) % 8, i) for i in range(8)])  9.26 us
    all_to_all x1, starting transfers between devices, whole_step(): lax.all_to_all(sent.reshape(128, 16, 128), BOTH, 0, 0, tiled=True)  8.22 us
    unnamed x22, local copies, waits for them, and re-layouts  5.09 us
    ppermute x7, starting transfers between devices, core_permute(): return lax.ppermute(x, 'tp', [(i ^ 1, i) for i in range(8)])  4.75 us
    ppermute x5, waiting for transfers between devices, chip_permute(): return lax.ppermute(x, 'tp', [((i + 2 * d) % 8, i) for i in range(8)])  4.58 us
    pallas_call x1, Pallas kernels, all_chips_state(): pl.pallas_call(all_chips_kernel, in_specs=hbm_specs(2) + vmem_specs(4), o...  4.43 us
  transfers between devices with their start and end apart: 13, of which 1 were waited for; matrix products, arithmetic and copies ran while one was open for 0% of the time, Pallas kernels for 11%

profile of v3, /device:TPU:1, one launch (start us, length us, event | category | flops | bytes accessed | tf_op | source)
XLA Modules:
  0.0 81.1 jit_solution(14197750097320228439)
XLA Ops:
  0.6 3.6 %prepare.1 = (bf16[16,8,16,128]{3,2,1,0:T(8,128)(2,1)}, bf16[784,128]{1,0:T(8,128)(2,1)S(1)}, bf16[1808,128]{1,0:T(8,128)(2,1)S(1)}, bf16[1024,128]{1,0:T(8,128)...) custom-call(bf16[4,16,256]{2,1,0:T(8,128)(2,1)} %bitcast.48, ...), custom_call_target="tpu_custom_call" | custom-call | flops 10000000 | bytes 1048576 | tf_op jit(solution)/shard_map/prepare/pallas_call | solution.py:123
  4.2 3.6 %collective-permute-start.1 = (bf16[1808,128]{1,0:T(8,128)(2,1)S(1)}, bf16[1808,128]{1,0:T(8,128)(2,1)S(1)}, u32[]{:S(2)}, u32[]{:S(2)}) collective-permute-start(bf16[1808,128]{1,0:T(8,128)(2,1)S(1)} %get-tuple-element.25), channel_id=1, source_target_pairs={{4,0},{5,1},{6,2},{7,3},{0,4},{1,5},{2,6},{3,7},{12,8},{13,9},{14,... | collective-permute-start | bytes 1388552 | tf_op jit(solution)/shard_map/ppermute | solution.py:484
  7.9 1.0 %collective-permute-start.3 = (bf16[784,128]{1,0:T(8,128)(2,1)S(1)}, bf16[784,128]{1,0:T(8,128)(2,1)S(1)}, u32[]{:S(2)}, u32[]{:S(2)}) collective-permute-start(bf16[784,128]{1,0:T(8,128)(2,1)S(1)} %get-tuple-element.24.refs_0_.rest_0_), channel_id=1, source_target_pairs={{1,0},{0,1},{3,2},{2,3},{5,4},{4,5},{7,6},{6,7},{9,8},{8,9},{11,10... | collective-permute-start | bytes 602120 | tf_op jit(solution)/shard_map/ppermute | solution.py:488
  8.8 8.2 %all-to-all-start = ((bf16[128,16,128]{2,1,0:T(8,128)(2,1)}), bf16[128,16,128]{2,1,0:T(8,128)(2,1)S(1)}, u32[]{:S(2)}, u32[]{:S(2)}) async-start(bf16[128,16,128]{2,1,0:T(8,128)(2,1)} %bitcast.19), calls=%async_computation | async-start | bytes 1048576 | tf_op jit(solution)/shard_map/all_to_all | solution.py:537
  17.1 1.4 %collective-permute-start.2 = (bf16[784,128]{1,0:T(8,128)(2,1)S(1)}, bf16[784,128]{1,0:T(8,128)(2,1)S(1)}, u32[]{:S(2)}, u32[]{:S(2)}) collective-permute-start(bf16[784,128]{1,0:T(8,128)(2,1)S(1)} %get-tuple-element.24.refs_0_.rest_0_), channel_id=1, source_target_pairs={{6,0},{7,1},{0,2},{1,3},{2,4},{3,5},{4,6},{5,7},{14,8},{15,9},{8,1... | collective-permute-start | bytes 602120 | tf_op jit(solution)/shard_map/ppermute | solution.py:484
  18.5 0.0 collective-permute-done.1.refs_2_.rest_2_.rest_10_
  18.5 1.3 %collective-permute-start.5 = (bf16[1808,128]{1,0:T(8,128)(2,1)S(1)}, bf16[1808,128]{1,0:T(8,128)(2,1)S(1)}, u32[]{:S(2)}, u32[]{:S(2)}) collective-permute-start(bf16[1808,128]{1,0:T(8,128)(2,1)S(1)} %collective-permute-done.1.refs_2_.rest_2_.rest_10_), channel_id=1, source_target_pairs={{1,0},{0,1},{3,2},{2,3},{5,4},{4,5},{7,6},{6,7},{9,8},{8,9},{11,10... | collective-permute-start | bytes 1388552 | tf_op jit(solution)/shard_map/ppermute | solution.py:488
  19.8 2.7 %collective-permute-start = (bf16[784,128]{1,0:T(8,128)(2,1)S(1)}, bf16[784,128]{1,0:T(8,128)(2,1)S(1)}, u32[]{:S(2)}, u32[]{:S(2)}) collective-permute-start(bf16[784,128]{1,0:T(8,128)(2,1)S(1)} %get-tuple-element.24.refs_0_.rest_0_), channel_id=1, source_target_pairs={{2,0},{3,1},{4,2},{5,3},{6,4},{7,5},{0,6},{1,7},{10,8},{11,9},{12,... | collective-permute-start | bytes 602120 | tf_op jit(solution)/shard_map/ppermute | solution.py:484
  22.5 1.0 %other_chips_state.1 = (bf16[1024,128]{1,0:T(8,128)(2,1)S(1)}, bf16[1024,128]{1,0:T(8,128)(2,1)S(1)}) custom-call(bf16[2048,128]{1,0:T(8,128)(2,1)S(1)} %get-tuple-element.39.state_ref, bf16[1024,128]{1,0:T(8,128)(2,1)S(1)} %get-tuple-element.40.refs_0_, bf16[4,16,256]{2,1,0:T(8,128)(2,1)S(1)} %get-tuple-element.34.refs_0_.refs_1_, ...), custom_call_target="tpu_custom_call" | custom-call | flops 1000000000 | bytes 2097152 | tf_op jit(solution)/shard_map/other_chips_state/pallas_call | solution.py:212
  23.5 1.4 %collective-permute-start.7 = (bf16[1024,128]{1,0:T(8,128)(2,1)S(1)}, bf16[1024,128]{1,0:T(8,128)(2,1)S(1)}, u32[]{:S(2)}, u32[]{:S(2)}) collective-permute-start(bf16[1024,128]{1,0:T(8,128)(2,1)S(1)} %get-tuple-element.41), channel_id=1, source_target_pairs={{2,0},{3,1},{4,2},{5,3},{6,4},{7,5},{0,6},{1,7},{10,8},{11,9},{12,... | collective-permute-start | bytes 786440 | tf_op jit(solution)/shard_map/ppermute | solution.py:484
  24.9 0.0 collective-permute-done.3.refs_4_.rest_4_
  24.9 0.1 collective-permute-start.8
  25.1 4.6 %collective-permute-done.2.refs_3_.rest_3_ = bf16[784,128]{1,0:T(8,128)(2,1)S(1)} collective-permute-done((bf16[784,128]{1,0:T(8,128)(2,1)S(1)}, bf16[784,128]{1,0:T(8,128)(2,1)S(1)}, u32[]{:S(2)}, u32[]{:S(2)}) %collective-permute-start.2) | collective-permute-done | bytes 200736 | tf_op jit(solution)/shard_map/ppermute | solution.py:484
  29.6 1.4 %collective-permute-start.6 = (bf16[784,128]{1,0:T(8,128)(2,1)S(1)}, bf16[784,128]{1,0:T(8,128)(2,1)S(1)}, u32[]{:S(2)}, u32[]{:S(2)}) collective-permute-start(bf16[784,128]{1,0:T(8,128)(2,1)S(1)} %collective-permute-done.2.refs_3_.rest_3_), channel_id=1, source_target_pairs={{1,0},{0,1},{3,2},{2,3},{5,4},{4,5},{7,6},{6,7},{9,8},{8,9},{11,10... | collective-permute-start | bytes 602120 | tf_op jit(solution)/shard_map/ppermute | solution.py:488
  31.0 0.0 collective-permute-done.refs_1_.rest_1_
  31.0 0.1 collective-permute-start.4
  31.1 4.4 %all_chips_state.1 = (f32[256,16,128]{2,1,0:T(8,128)}, bf16[1024,128]{1,0:T(8,128)(2,1)S(1)}) custom-call(f32[256,16,128]{2,1,0:T(8,128)} %bitcast.42, bf16[1024,128]{1,0:T(8,128)(2,1)} %bitcast.44, bf16[4,16,256]{2,1,0:T(8,128)(2,1)S(1)} %get-tuple-element.34.refs_0_.refs_1_, f32[4,1,256]{2,1,0:T(1,128)S(1)} %get-tuple-element.35.refs_1_.refs_2_, ...), custom_call_target="tpu_custom_call" | custom-call | flops 2000000000 | bytes 4194304 | tf_op jit(solution)/shard_map/all_chips_state/pallas_call | solution.py:259
  35.5 0.0 copy-done
  35.5 0.0 copy-done.2
  35.5 0.0 collective-permute-done.7.rest_9_
  35.6 0.5 collective-permute-start.9
  36.1 0.0 collective-permute-done.8.rest_11_
  36.1 0.1 collective-permute-start.10
  36.2 0.0 collective-permute-done.6.refs_7_.rest_7_
  36.2 0.7 copy-done.5
  36.8 0.4 collective-permute-start.11
  37.9 0.0 collective-permute-done.4.refs_5_.rest_5_
  37.9 0.0 copy-start.8
  37.9 0.7 copy-done.8
  38.6 0.0 all-to-all-done
  38.6 0.0 collective-permute-done.5.refs_6_.rest_6_.rest_14_
  38.6 0.9 %copy-done.1 = bf16[784,128]{1,0:T(8,128)(2,1)S(1)} copy-done((bf16[784,128]{1,0:T(8,128)(2,1)S(1)}, bf16[784,128]{1,0:T(8,128)(2,1)}, u32[]{:S(2)}) %copy-start.1) | copy-done | bytes 200728
  39.5 0.9 %copy-done.3 = bf16[784,128]{1,0:T(8,128)(2,1)S(1)} copy-done((bf16[784,128]{1,0:T(8,128)(2,1)S(1)}, bf16[784,128]{1,0:T(8,128)(2,1)}, u32[]{:S(2)}) %copy-start.3) | copy-done | bytes 200728
  40.5 0.9 %copy-done.6 = bf16[784,128]{1,0:T(8,128)(2,1)S(1)} copy-done((bf16[784,128]{1,0:T(8,128)(2,1)S(1)}, bf16[784,128]{1,0:T(8,128)(2,1)}, u32[]{:S(2)}) %copy-start.6) | copy-done | bytes 200728
  41.4 0.9 %copy-done.9 = bf16[784,128]{1,0:T(8,128)(2,1)S(1)} copy-done((bf16[784,128]{1,0:T(8,128)(2,1)S(1)}, bf16[784,128]{1,0:T(8,128)(2,1)}, u32[]{:S(2)}) %copy-start.9) | copy-done | bytes 200728
  42.3 3.1 %row_side.1 = (bf16[128,128]{1,0:T(8,128)(2,1)S(1)}, f32[128,128]{1,0:T(8,128)S(1)}, f32[128,128]{1,0:T(8,128)S(1)}) custom-call(bf16[2048,128]{1,0:T(8,128)(2,1)S(1)} %bitcast.37, bf16[784,128]{1,0:T(8,128)(2,1)S(1)} %get-tuple-element.24.refs_0_.rest_0_, bf16[784,128]{1,0:T(8,128)(2,1)S(1)} %copy-done.3, ...), custom_call_target="tpu_custom_call" | custom-call | flops 2000000000 | bytes 4194304 | tf_op jit(solution)/shard_map/row_side/pallas_call | solution.py:383
  45.4 0.0 collective-permute-done.9.rest_12_
  45.4 0.0 collective-permute-done.10.rest_13_
  45.4 0.0 collective-permute-done.11.rest_15_
  45.4 0.0 copy-done.4
  45.4 0.0 copy-done.7
  45.5 0.0 copy-start.10
  45.5 0.8 readout.1
  46.2 17.6 %all_to_all.21.part_ref = bf16[16,8,2048]{2,1,0:T(8,128)(2,1)S(1)} all-to-all(bf16[16,8,2048]{2,1,0:T(8,128)(2,1)S(1)} %bitcast.36), channel_id=1, replica_groups=mesh['kv'=16,'tp'=8] {'kv'}, dimensions={0} | all-to-all | bytes 1048576 | tf_op jit(solution)/shard_map/all_to_all | solution.py:546
  63.9 0.3 sum_heads.1
  64.1 15.9 %all_to_all.22 = f32[128,1,128]{2,1,0:T(1,128)S(1)} all-to-all(f32[128,1,128]{2,1,0:T(1,128)S(1)} %bitcast.38), channel_id=1, replica_groups=mesh['kv'=16,'tp'=8] {'kv','tp'}, dimensions={0} | all-to-all | bytes 131072 | tf_op jit(solution)/shard_map/all_to_all | solution.py:547
  80.1 0.0 copy-done.10
  80.1 1.0 %final_rows.1 = bf16[4,16,256]{2,1,0:T(8,128)(2,1)} custom-call(f32[128,128]{1,0:T(8,128)S(1)} %bitcast.39, bf16[1,16]{1,0:T(2,128)(2,1)S(1)} %bitcast.40), custom_call_target="tpu_custom_call" | custom-call | flops 10000000 | bytes 262144 | tf_op jit(solution)/shard_map/final_rows/pallas_call | solution.py:471
  (9 shorter events, 0.0 us)
Async XLA Ops:
  4.2 14.3 %collective-permute-start.1 = (bf16[1808,128]{1,0:T(8,128)(2,1)S(1)}, bf16[1808,128]{1,0:T(8,128)(2,1)S(1)}, u32[]{:S(2)}, u32[]{:S(2)}) collective-permute-start(bf16[1808,128]{1,0:T(8,128)(2,1)S(1)} %get-tuple-element.25), channel_id=1, source_target_pairs={{4,0},{5,1},{6,2},{7,3},{0,4},{1,5},{2,6},{3,7},{12,8},{13,9},{14,... | collective-permute-start | bytes 1388552 | tf_op jit(solution)/shard_map/ppermute | solution.py:484
  7.9 17.1 %collective-permute-start.3 = (bf16[784,128]{1,0:T(8,128)(2,1)S(1)}, bf16[784,128]{1,0:T(8,128)(2,1)S(1)}, u32[]{:S(2)}, u32[]{:S(2)}) collective-permute-start(bf16[784,128]{1,0:T(8,128)(2,1)S(1)} %get-tuple-element.24.refs_0_.rest_0_), channel_id=1, source_target_pairs={{1,0},{0,1},{3,2},{2,3},{5,4},{4,5},{7,6},{6,7},{9,8},{8,9},{11,10... | collective-permute-start | bytes 602120 | tf_op jit(solution)/shard_map/ppermute | solution.py:488
  8.8 29.8 %all-to-all-start = ((bf16[128,16,128]{2,1,0:T(8,128)(2,1)}), bf16[128,16,128]{2,1,0:T(8,128)(2,1)S(1)}, u32[]{:S(2)}, u32[]{:S(2)}) async-start(bf16[128,16,128]{2,1,0:T(8,128)(2,1)} %bitcast.19), calls=%async_computation | async-start | bytes 1048576 | tf_op jit(solution)/shard_map/all_to_all | solution.py:537
  17.1 12.6 %collective-permute-start.2 = (bf16[784,128]{1,0:T(8,128)(2,1)S(1)}, bf16[784,128]{1,0:T(8,128)(2,1)S(1)}, u32[]{:S(2)}, u32[]{:S(2)}) collective-permute-start(bf16[784,128]{1,0:T(8,128)(2,1)S(1)} %get-tuple-element.24.refs_0_.rest_0_), channel_id=1, source_target_pairs={{6,0},{7,1},{0,2},{1,3},{2,4},{3,5},{4,6},{5,7},{14,8},{15,9},{8,1... | collective-permute-start | bytes 602120 | tf_op jit(solution)/shard_map/ppermute | solution.py:484
  18.5 20.1 %collective-permute-start.5 = (bf16[1808,128]{1,0:T(8,128)(2,1)S(1)}, bf16[1808,128]{1,0:T(8,128)(2,1)S(1)}, u32[]{:S(2)}, u32[]{:S(2)}) collective-permute-start(bf16[1808,128]{1,0:T(8,128)(2,1)S(1)} %collective-permute-done.1.refs_2_.rest_2_.rest_10_), channel_id=1, source_target_pairs={{1,0},{0,1},{3,2},{2,3},{5,4},{4,5},{7,6},{6,7},{9,8},{8,9},{11,10... | collective-permute-start | bytes 1388552 | tf_op jit(solution)/shard_map/ppermute | solution.py:488
  19.8 11.2 %collective-permute-start = (bf16[784,128]{1,0:T(8,128)(2,1)S(1)}, bf16[784,128]{1,0:T(8,128)(2,1)S(1)}, u32[]{:S(2)}, u32[]{:S(2)}) collective-permute-start(bf16[784,128]{1,0:T(8,128)(2,1)S(1)} %get-tuple-element.24.refs_0_.rest_0_), channel_id=1, source_target_pairs={{2,0},{3,1},{4,2},{5,3},{6,4},{7,5},{0,6},{1,7},{10,8},{11,9},{12,... | collective-permute-start | bytes 602120 | tf_op jit(solution)/shard_map/ppermute | solution.py:484
  23.5 12.0 %collective-permute-start.7 = (bf16[1024,128]{1,0:T(8,128)(2,1)S(1)}, bf16[1024,128]{1,0:T(8,128)(2,1)S(1)}, u32[]{:S(2)}, u32[]{:S(2)}) collective-permute-start(bf16[1024,128]{1,0:T(8,128)(2,1)S(1)} %get-tuple-element.41), channel_id=1, source_target_pairs={{2,0},{3,1},{4,2},{5,3},{6,4},{7,5},{0,6},{1,7},{10,8},{11,9},{12,... | collective-permute-start | bytes 786440 | tf_op jit(solution)/shard_map/ppermute | solution.py:484
  24.9 11.1 %collective-permute-start.8 = (bf16[1024,128]{1,0:T(8,128)(2,1)S(1)}, bf16[1024,128]{1,0:T(8,128)(2,1)S(1)}, u32[]{:S(2)}, u32[]{:S(2)}) collective-permute-start(bf16[1024,128]{1,0:T(8,128)(2,1)S(1)} %get-tuple-element.42), channel_id=1, source_target_pairs={{6,0},{7,1},{0,2},{1,3},{2,4},{3,5},{4,6},{5,7},{14,8},{15,9},{8,1... | collective-permute-start | bytes 786440 | tf_op jit(solution)/shard_map/ppermute | solution.py:484
  29.6 5.9 %copy-start = (bf16[784,128]{1,0:T(8,128)(2,1)}, bf16[784,128]{1,0:T(8,128)(2,1)S(1)}, u32[]{:S(2)}) copy-start(bf16[784,128]{1,0:T(8,128)(2,1)S(1)} %collective-permute-done.2.refs_3_.rest_3_) | copy-start | bytes 602116
  29.6 6.5 %collective-permute-start.6 = (bf16[784,128]{1,0:T(8,128)(2,1)S(1)}, bf16[784,128]{1,0:T(8,128)(2,1)S(1)}, u32[]{:S(2)}, u32[]{:S(2)}) collective-permute-start(bf16[784,128]{1,0:T(8,128)(2,1)S(1)} %collective-permute-done.2.refs_3_.rest_3_), channel_id=1, source_target_pairs={{1,0},{0,1},{3,2},{2,3},{5,4},{4,5},{7,6},{6,7},{9,8},{8,9},{11,10... | collective-permute-start | bytes 602120 | tf_op jit(solution)/shard_map/ppermute | solution.py:488
  31.0 4.5 %copy-start.2 = (bf16[784,128]{1,0:T(8,128)(2,1)}, bf16[784,128]{1,0:T(8,128)(2,1)S(1)}, u32[]{:S(2)}) copy-start(bf16[784,128]{1,0:T(8,128)(2,1)S(1)} %collective-permute-done.refs_1_.rest_1_) | copy-start | bytes 602116
  31.0 6.9 %collective-permute-start.4 = (bf16[784,128]{1,0:T(8,128)(2,1)S(1)}, bf16[784,128]{1,0:T(8,128)(2,1)S(1)}, u32[]{:S(2)}, u32[]{:S(2)}) collective-permute-start(bf16[784,128]{1,0:T(8,128)(2,1)S(1)} %collective-permute-done.refs_1_.rest_1_), channel_id=1, source_target_pairs={{1,0},{0,1},{3,2},{2,3},{5,4},{4,5},{7,6},{6,7},{9,8},{8,9},{11,10... | collective-permute-start | bytes 602120 | tf_op jit(solution)/shard_map/ppermute | solution.py:488
  35.6 9.8 %collective-permute-start.9 = (bf16[1024,128]{1,0:T(8,128)(2,1)S(1)}, bf16[1024,128]{1,0:T(8,128)(2,1)S(1)}, u32[]{:S(2)}, u32[]{:S(2)}) collective-permute-start(bf16[1024,128]{1,0:T(8,128)(2,1)S(1)} %get-tuple-element.38.rest_8_), channel_id=1, source_target_pairs={{1,0},{0,1},{3,2},{2,3},{5,4},{4,5},{7,6},{6,7},{9,8},{8,9},{11,10... | collective-permute-start | bytes 786440 | tf_op jit(solution)/shard_map/ppermute | solution.py:488
  36.1 9.4 %collective-permute-start.10 = (bf16[1024,128]{1,0:T(8,128)(2,1)S(1)}, bf16[1024,128]{1,0:T(8,128)(2,1)S(1)}, u32[]{:S(2)}, u32[]{:S(2)}) collective-permute-start(bf16[1024,128]{1,0:T(8,128)(2,1)S(1)} %collective-permute-done.7.rest_9_), channel_id=1, source_target_pairs={{1,0},{0,1},{3,2},{2,3},{5,4},{4,5},{7,6},{6,7},{9,8},{8,9},{11,10... | collective-permute-start | bytes 786440 | tf_op jit(solution)/shard_map/ppermute | solution.py:488
  36.2 0.7 copy-start.5
  36.8 8.6 %collective-permute-start.11 = (bf16[1024,128]{1,0:T(8,128)(2,1)S(1)}, bf16[1024,128]{1,0:T(8,128)(2,1)S(1)}, u32[]{:S(2)}, u32[]{:S(2)}) collective-permute-start(bf16[1024,128]{1,0:T(8,128)(2,1)S(1)} %collective-permute-done.8.rest_11_), channel_id=1, source_target_pairs={{1,0},{0,1},{3,2},{2,3},{5,4},{4,5},{7,6},{6,7},{9,8},{8,9},{11,10... | collective-permute-start | bytes 786440 | tf_op jit(solution)/shard_map/ppermute | solution.py:488
  37.9 0.7 copy-start.8
  38.6 0.9 %copy-start.1 = (bf16[784,128]{1,0:T(8,128)(2,1)S(1)}, bf16[784,128]{1,0:T(8,128)(2,1)}, u32[]{:S(2)}) copy-start(bf16[784,128]{1,0:T(8,128)(2,1)} %copy-done) | copy-start | bytes 602116
  39.5 0.9 %copy-start.3 = (bf16[784,128]{1,0:T(8,128)(2,1)S(1)}, bf16[784,128]{1,0:T(8,128)(2,1)}, u32[]{:S(2)}) copy-start(bf16[784,128]{1,0:T(8,128)(2,1)} %copy-done.2) | copy-start | bytes 602116
  40.5 0.9 %copy-start.6 = (bf16[784,128]{1,0:T(8,128)(2,1)S(1)}, bf16[784,128]{1,0:T(8,128)(2,1)}, u32[]{:S(2)}) copy-start(bf16[784,128]{1,0:T(8,128)(2,1)} %copy-done.5) | copy-start | bytes 602116
  41.4 0.9 %copy-start.9 = (bf16[784,128]{1,0:T(8,128)(2,1)S(1)}, bf16[784,128]{1,0:T(8,128)(2,1)}, u32[]{:S(2)}) copy-start(bf16[784,128]{1,0:T(8,128)(2,1)} %copy-done.8) | copy-start | bytes 602116
  42.3 3.1 %copy-start.4 = (bf16[784,128]{1,0:T(8,128)(2,1)S(1)}, bf16[784,128]{1,0:T(8,128)(2,1)}, u32[]{:S(2)}) copy-start(bf16[784,128]{1,0:T(8,128)(2,1)} %copy-done.2) | copy-start | bytes 602116
  42.3 3.1 %copy-start.7 = (bf16[784,128]{1,0:T(8,128)(2,1)S(1)}, bf16[784,128]{1,0:T(8,128)(2,1)}, u32[]{:S(2)}) copy-start(bf16[784,128]{1,0:T(8,128)(2,1)} %copy-done.5) | copy-start | bytes 602116
  45.5 34.6 %copy-start.10 = (bf16[16]{0:T(256)(128)(2,1)S(1)}, bf16[16]{0:T(256)(128)(2,1)}, u32[]{:S(2)}) copy-start(bf16[16]{0:T(256)(128)(2,1)} %param.32) | copy-start | bytes 100

commit v4 on v3

--- a/solution.py
+++ b/solution.py
@@ -84,10 +84,10 @@
 
 
 def prepare_kernel(*refs):
-    sources, state_source, (sent_ref, pack_ref, bundle_ref), kept, rest = (
+    sources, state_source, (sent_out, pack_ref, bundle_ref), kept, rest = (
         refs[:15], refs[15], refs[16:19], refs[19:29], refs[29:],
     )
-    low_ref, held, sems, state_ref = rest[0], rest[1:6], rest[6:9], rest[9]
+    low_ref, held, sems, state_ref, sent_ref, sent_sem = rest[0], rest[1:6], rest[6:9], rest[9], rest[10], rest[11]
     copies = copies_in(sources[:5], held, sems[0])
     ahead = copies_in(sources[5:], kept, sems[1])
     chip = lax.axis_index("tp") // 2
@@ -95,17 +95,19 @@
     for i, offset in enumerate((2, 1, 3)):
         rows = pl.ds(pl.multiple_of(64 * lax.rem(chip + offset, 4), 64), 64)
         loads.append(pltpu.make_async_copy(state_source.at[rows], state_ref.at[pl.ds(64 * i, 64)], sems[2].at[i]))
-    start_all(copies + ahead + loads)
-    wait_all(copies[1:])
-    pack_weights(*held[1:], pack_ref)
-    bundle_ref[1024:, :] = pack_ref[...]
+    start_all(copies[:1] + loads[:1] + ahead[:5] + copies[1:] + loads[1:] + ahead[5:])
     copies[0].wait()
     rows = [held[0][i].astype(f32) for i in range(4)]
     for t in range(8):
         block = chunk_lanes(rows, t).astype(bf16)
         for k in range(16):
             sent_ref[k, t] = block
-    wait_all(ahead + loads[:1])
+    send = pltpu.make_async_copy(sent_ref, sent_out, sent_sem)
+    send.start()
+    wait_all(copies[1:])
+    pack_weights(*held[1:], pack_ref)
+    bundle_ref[1024:, :] = pack_ref[...]
+    wait_all(ahead[:5] + loads[:1])
 
     def read(step):
         return state_ref[32 * step : 32 * step + 32].reshape(512, 128)
@@ -117,18 +119,20 @@
     wait_all(loads[1:])
     for i in range(4):
         low_ref[512 * i : 512 * i + 512, :] = read(2 + i).astype(bf16)
+    wait_all(ahead[5:] + [send])
 
 
 def prepare(first, ahead, state):
     return pl.pallas_call(
         prepare_kernel,
         in_specs=hbm_specs(16),
-        out_specs=vmem_specs(14),
-        out_shape=[pltpu.VMEM((16, 8, 16, 128), bf16), pltpu.VMEM((PACK, 128), bf16), pltpu.VMEM((BUNDLE, 128), bf16)]
+        out_specs=hbm_specs(1) + vmem_specs(13),
+        out_shape=[pltpu.HBM((16, 8, 16, 128), bf16), pltpu.VMEM((PACK, 128), bf16), pltpu.VMEM((BUNDLE, 128), bf16)]
         + [pltpu.VMEM(x.shape, x.dtype) for x in ahead]
         + [pltpu.VMEM((2048, 128), bf16)],
         scratch_shapes=scratch_like(first)
-        + [pltpu.SemaphoreType.DMA((10,)), pltpu.SemaphoreType.DMA((3,)), pltpu.VMEM((192, 16, 128), f32)],
+        + [pltpu.SemaphoreType.DMA((10,)), pltpu.SemaphoreType.DMA((3,)), pltpu.VMEM((192, 16, 128), f32)]
+        + [pltpu.VMEM((16, 8, 16, 128), bf16), pltpu.SemaphoreType.DMA],
         cost_estimate=cost(10000000, 1 << 20),
         compiler_params=pltpu.CompilerParams(vmem_limit_bytes=VMEM_LIMIT),
         name="prepare",

time: 81.5 us -> 80.7 us (level)
  no operation moved by 1% of the time
where the time goes in v4:
time: 80.7 us; the launch traced here: 80.3 us
  blocking collectives  33.6 us (42%)
  starting transfers between devices  22.2 us (28%)
  Pallas kernels  13.4 us (17%)
  local copies, waits for them, and re-layouts  5.09 us (6%)
  waiting for transfers between devices  4.59 us (6%)
  between operations  1.45 us (2%)
    all_to_all x1, blocking collectives, whole_step(): parts = lax.all_to_all(part.reshape(16, 8, 2048), 'kv', 0, 0, tiled=True)  17.6 us
    all_to_all x1, blocking collectives, whole_step(): blocks = lax.all_to_all(sum_heads(parts), BOTH, 0, 0, tiled=True)  15.9 us
    ppermute x5, starting transfers between devices, chip_permute(): return lax.ppermute(x, 'tp', [((i + 2 * d) % 8, i) for i in range(8)])  9.26 us
    all_to_all x1, starting transfers between devices, whole_step(): lax.all_to_all(sent.reshape(128, 16, 128), BOTH, 0, 0, tiled=True)  8.22 us
    unnamed x22, local copies, waits for them, and re-layouts  5.09 us
    ppermute x7, starting transfers between devices, core_permute(): return lax.ppermute(x, 'tp', [(i ^ 1, i) for i in range(8)])  4.75 us
    ppermute x5, waiting for transfers between devices, chip_permute(): return lax.ppermute(x, 'tp', [((i + 2 * d) % 8, i) for i in range(8)])  4.57 us
    pallas_call x1, Pallas kernels, all_chips_state(): pl.pallas_call(all_chips_kernel, in_specs=hbm_specs(2) + vmem_specs(4), o...  4.43 us
  transfers between devices with their start and end apart: 13, of which 1 were waited for; matrix products, arithmetic and copies ran while one was open for 0% of the time, Pallas kernels for 11%

profile of v4, /device:TPU:1, one launch (start us, length us, event | category | flops | bytes accessed | tf_op | source)
XLA Modules:
  0.0 80.3 jit_solution(3957140620764184050)
XLA Ops:
  0.6 2.8 %prepare.1 = (bf16[16,8,16,128]{3,2,1,0:T(8,128)(2,1)}, bf16[784,128]{1,0:T(8,128)(2,1)S(1)}, bf16[1808,128]{1,0:T(8,128)(2,1)S(1)}, bf16[1024,128]{1,0:T(8,128)...) custom-call(bf16[4,16,256]{2,1,0:T(8,128)(2,1)} %bitcast.49, ...), custom_call_target="tpu_custom_call" | custom-call | flops 10000000 | bytes 1048576 | tf_op jit(solution)/shard_map/prepare/pallas_call | solution.py:126
  3.5 3.6 %collective-permute-start.1 = (bf16[1808,128]{1,0:T(8,128)(2,1)S(1)}, bf16[1808,128]{1,0:T(8,128)(2,1)S(1)}, u32[]{:S(2)}, u32[]{:S(2)}) collective-permute-start(bf16[1808,128]{1,0:T(8,128)(2,1)S(1)} %get-tuple-element.25), channel_id=1, source_target_pairs={{4,0},{5,1},{6,2},{7,3},{0,4},{1,5},{2,6},{3,7},{12,8},{13,9},{14,... | collective-permute-start | bytes 1388552 | tf_op jit(solution)/shard_map/ppermute | solution.py:488
  7.1 1.0 %collective-permute-start.3 = (bf16[784,128]{1,0:T(8,128)(2,1)S(1)}, bf16[784,128]{1,0:T(8,128)(2,1)S(1)}, u32[]{:S(2)}, u32[]{:S(2)}) collective-permute-start(bf16[784,128]{1,0:T(8,128)(2,1)S(1)} %get-tuple-element.24.refs_0_.rest_0_), channel_id=1, source_target_pairs={{1,0},{0,1},{3,2},{2,3},{5,4},{4,5},{7,6},{6,7},{9,8},{8,9},{11,10... | collective-permute-start | bytes 602120 | tf_op jit(solution)/shard_map/ppermute | solution.py:492
  8.1 8.2 %all-to-all-start = ((bf16[128,16,128]{2,1,0:T(8,128)(2,1)}), bf16[128,16,128]{2,1,0:T(8,128)(2,1)S(1)}, u32[]{:S(2)}, u32[]{:S(2)}) async-start(bf16[128,16,128]{2,1,0:T(8,128)(2,1)} %bitcast.43), calls=%async_computation | async-start | bytes 1048576 | tf_op jit(solution)/shard_map/all_to_all | solution.py:541
  16.3 1.4 %collective-permute-start.2 = (bf16[784,128]{1,0:T(8,128)(2,1)S(1)}, bf16[784,128]{1,0:T(8,128)(2,1)S(1)}, u32[]{:S(2)}, u32[]{:S(2)}) collective-permute-start(bf16[784,128]{1,0:T(8,128)(2,1)S(1)} %get-tuple-element.24.refs_0_.rest_0_), channel_id=1, source_target_pairs={{6,0},{7,1},{0,2},{1,3},{2,4},{3,5},{4,6},{5,7},{14,8},{15,9},{8,1... | collective-permute-start | bytes 602120 | tf_op jit(solution)/shard_map/ppermute | solution.py:488
  17.7 0.0 collective-permute-done.1.refs_2_.rest_2_.rest_10_
  17.7 1.3 %collective-permute-start.5 = (bf16[1808,128]{1,0:T(8,128)(2,1)S(1)}, bf16[1808,128]{1,0:T(8,128)(2,1)S(1)}, u32[]{:S(2)}, u32[]{:S(2)}) collective-permute-start(bf16[1808,128]{1,0:T(8,128)(2,1)S(1)} %collective-permute-done.1.refs_2_.rest_2_.rest_10_), channel_id=1, source_target_pairs={{1,0},{0,1},{3,2},{2,3},{5,4},{4,5},{7,6},{6,7},{9,8},{8,9},{11,10... | collective-permute-start | bytes 1388552 | tf_op jit(solution)/shard_map/ppermute | solution.py:492
  19.1 2.7 %collective-permute-start = (bf16[784,128]{1,0:T(8,128)(2,1)S(1)}, bf16[784,128]{1,0:T(8,128)(2,1)S(1)}, u32[]{:S(2)}, u32[]{:S(2)}) collective-permute-start(bf16[784,128]{1,0:T(8,128)(2,1)S(1)} %get-tuple-element.24.refs_0_.rest_0_), channel_id=1, source_target_pairs={{2,0},{3,1},{4,2},{5,3},{6,4},{7,5},{0,6},{1,7},{10,8},{11,9},{12,... | collective-permute-start | bytes 602120 | tf_op jit(solution)/shard_map/ppermute | solution.py:488
  21.8 1.0 %other_chips_state.1 = (bf16[1024,128]{1,0:T(8,128)(2,1)S(1)}, bf16[1024,128]{1,0:T(8,128)(2,1)S(1)}) custom-call(bf16[2048,128]{1,0:T(8,128)(2,1)S(1)} %get-tuple-element.39.state_ref, bf16[1024,128]{1,0:T(8,128)(2,1)S(1)} %get-tuple-element.40.refs_0_, bf16[4,16,256]{2,1,0:T(8,128)(2,1)S(1)} %get-tuple-element.34.refs_0_.refs_1_, ...), custom_call_target="tpu_custom_call" | custom-call | flops 1000000000 | bytes 2097152 | tf_op jit(solution)/shard_map/other_chips_state/pallas_call | solution.py:216
  22.8 1.4 %collective-permute-start.7 = (bf16[1024,128]{1,0:T(8,128)(2,1)S(1)}, bf16[1024,128]{1,0:T(8,128)(2,1)S(1)}, u32[]{:S(2)}, u32[]{:S(2)}) collective-permute-start(bf16[1024,128]{1,0:T(8,128)(2,1)S(1)} %get-tuple-element.41), channel_id=1, source_target_pairs={{2,0},{3,1},{4,2},{5,3},{6,4},{7,5},{0,6},{1,7},{10,8},{11,9},{12,... | collective-permute-start | bytes 786440 | tf_op jit(solution)/shard_map/ppermute | solution.py:488
  24.2 0.0 collective-permute-done.3.refs_4_.rest_4_
  24.2 0.1 collective-permute-start.8
  24.3 4.6 %collective-permute-done.2.refs_3_.rest_3_ = bf16[784,128]{1,0:T(8,128)(2,1)S(1)} collective-permute-done((bf16[784,128]{1,0:T(8,128)(2,1)S(1)}, bf16[784,128]{1,0:T(8,128)(2,1)S(1)}, u32[]{:S(2)}, u32[]{:S(2)}) %collective-permute-start.2) | collective-permute-done | bytes 200736 | tf_op jit(solution)/shard_map/ppermute | solution.py:488
  28.9 1.4 %collective-permute-start.6 = (bf16[784,128]{1,0:T(8,128)(2,1)S(1)}, bf16[784,128]{1,0:T(8,128)(2,1)S(1)}, u32[]{:S(2)}, u32[]{:S(2)}) collective-permute-start(bf16[784,128]{1,0:T(8,128)(2,1)S(1)} %collective-permute-done.2.refs_3_.rest_3_), channel_id=1, source_target_pairs={{1,0},{0,1},{3,2},{2,3},{5,4},{4,5},{7,6},{6,7},{9,8},{8,9},{11,10... | collective-permute-start | bytes 602120 | tf_op jit(solution)/shard_map/ppermute | solution.py:492
  30.3 0.0 collective-permute-done.refs_1_.rest_1_
  30.3 0.1 collective-permute-start.4
  30.4 4.4 %all_chips_state.1 = (f32[256,16,128]{2,1,0:T(8,128)}, bf16[1024,128]{1,0:T(8,128)(2,1)S(1)}) custom-call(f32[256,16,128]{2,1,0:T(8,128)} %bitcast.42, bf16[1024,128]{1,0:T(8,128)(2,1)} %bitcast.45, bf16[4,16,256]{2,1,0:T(8,128)(2,1)S(1)} %get-tuple-element.34.refs_0_.refs_1_, f32[4,1,256]{2,1,0:T(1,128)S(1)} %get-tuple-element.35.refs_1_.refs_2_, ...), custom_call_target="tpu_custom_call" | custom-call | flops 2000000000 | bytes 4194304 | tf_op jit(solution)/shard_map/all_chips_state/pallas_call | solution.py:263
  34.8 0.0 copy-done
  34.8 0.0 copy-done.2
  34.8 0.0 collective-permute-done.7.rest_9_
  34.8 0.5 collective-permute-start.9
  35.3 0.0 collective-permute-done.8.rest_11_
  35.3 0.1 collective-permute-start.10
  35.4 0.0 collective-permute-done.6.refs_7_.rest_7_
  35.4 0.7 copy-done.5
  36.1 0.4 collective-permute-start.11
  37.2 0.0 collective-permute-done.4.refs_5_.rest_5_
  37.2 0.0 copy-start.8
  37.2 0.7 copy-done.8
  37.9 0.0 all-to-all-done
  37.9 0.0 collective-permute-done.5.refs_6_.rest_6_.rest_14_
  37.9 0.9 %copy-done.1 = bf16[784,128]{1,0:T(8,128)(2,1)S(1)} copy-done((bf16[784,128]{1,0:T(8,128)(2,1)S(1)}, bf16[784,128]{1,0:T(8,128)(2,1)}, u32[]{:S(2)}) %copy-start.1) | copy-done | bytes 200728
  38.8 0.9 %copy-done.3 = bf16[784,128]{1,0:T(8,128)(2,1)S(1)} copy-done((bf16[784,128]{1,0:T(8,128)(2,1)S(1)}, bf16[784,128]{1,0:T(8,128)(2,1)}, u32[]{:S(2)}) %copy-start.3) | copy-done | bytes 200728
  39.7 0.9 %copy-done.6 = bf16[784,128]{1,0:T(8,128)(2,1)S(1)} copy-done((bf16[784,128]{1,0:T(8,128)(2,1)S(1)}, bf16[784,128]{1,0:T(8,128)(2,1)}, u32[]{:S(2)}) %copy-start.6) | copy-done | bytes 200728
  40.7 0.9 %copy-done.9 = bf16[784,128]{1,0:T(8,128)(2,1)S(1)} copy-done((bf16[784,128]{1,0:T(8,128)(2,1)S(1)}, bf16[784,128]{1,0:T(8,128)(2,1)}, u32[]{:S(2)}) %copy-start.9) | copy-done | bytes 200728
  41.6 3.1 %row_side.1 = (bf16[128,128]{1,0:T(8,128)(2,1)S(1)}, f32[128,128]{1,0:T(8,128)S(1)}, f32[128,128]{1,0:T(8,128)S(1)}) custom-call(bf16[2048,128]{1,0:T(8,128)(2,1)S(1)} %bitcast.37, bf16[784,128]{1,0:T(8,128)(2,1)S(1)} %get-tuple-element.24.refs_0_.rest_0_, bf16[784,128]{1,0:T(8,128)(2,1)S(1)} %copy-done.3, ...), custom_call_target="tpu_custom_call" | custom-call | flops 2000000000 | bytes 4194304 | tf_op jit(solution)/shard_map/row_side/pallas_call | solution.py:387
  44.7 0.0 collective-permute-done.9.rest_12_
  44.7 0.0 collective-permute-done.10.rest_13_
  44.7 0.0 collective-permute-done.11.rest_15_
  44.7 0.0 copy-done.4
  44.7 0.0 copy-done.7
  44.7 0.0 copy-start.10
  44.7 0.8 readout.1
  45.5 17.6 %all_to_all.21.part_ref = bf16[16,8,2048]{2,1,0:T(8,128)(2,1)S(1)} all-to-all(bf16[16,8,2048]{2,1,0:T(8,128)(2,1)S(1)} %bitcast.36), channel_id=1, replica_groups=mesh['kv'=16,'tp'=8] {'kv'}, dimensions={0} | all-to-all | bytes 1048576 | tf_op jit(solution)/shard_map/all_to_all | solution.py:550
  63.1 0.3 sum_heads.1
  63.4 15.9 %all_to_all.22 = f32[128,1,128]{2,1,0:T(1,128)S(1)} all-to-all(f32[128,1,128]{2,1,0:T(1,128)S(1)} %bitcast.38), channel_id=1, replica_groups=mesh['kv'=16,'tp'=8] {'kv','tp'}, dimensions={0} | all-to-all | bytes 131072 | tf_op jit(solution)/shard_map/all_to_all | solution.py:551
  79.3 0.0 copy-done.10
  79.3 1.0 %final_rows.1 = bf16[4,16,256]{2,1,0:T(8,128)(2,1)} custom-call(f32[128,128]{1,0:T(8,128)S(1)} %bitcast.39, bf16[1,16]{1,0:T(2,128)(2,1)S(1)} %bitcast.40), custom_call_target="tpu_custom_call" | custom-call | flops 10000000 | bytes 262144 | tf_op jit(solution)/shard_map/final_rows/pallas_call | solution.py:475
  (9 shorter events, 0.0 us)
Async XLA Ops:
  3.5 14.2 %collective-permute-start.1 = (bf16[1808,128]{1,0:T(8,128)(2,1)S(1)}, bf16[1808,128]{1,0:T(8,128)(2,1)S(1)}, u32[]{:S(2)}, u32[]{:S(2)}) collective-permute-start(bf16[1808,128]{1,0:T(8,128)(2,1)S(1)} %get-tuple-element.25), channel_id=1, source_target_pairs={{4,0},{5,1},{6,2},{7,3},{0,4},{1,5},{2,6},{3,7},{12,8},{13,9},{14,... | collective-permute-start | bytes 1388552 | tf_op jit(solution)/shard_map/ppermute | solution.py:488
  7.1 17.1 %collective-permute-start.3 = (bf16[784,128]{1,0:T(8,128)(2,1)S(1)}, bf16[784,128]{1,0:T(8,128)(2,1)S(1)}, u32[]{:S(2)}, u32[]{:S(2)}) collective-permute-start(bf16[784,128]{1,0:T(8,128)(2,1)S(1)} %get-tuple-element.24.refs_0_.rest_0_), channel_id=1, source_target_pairs={{1,0},{0,1},{3,2},{2,3},{5,4},{4,5},{7,6},{6,7},{9,8},{8,9},{11,10... | collective-permute-start | bytes 602120 | tf_op jit(solution)/shard_map/ppermute | solution.py:492
  8.1 29.8 %all-to-all-start = ((bf16[128,16,128]{2,1,0:T(8,128)(2,1)}), bf16[128,16,128]{2,1,0:T(8,128)(2,1)S(1)}, u32[]{:S(2)}, u32[]{:S(2)}) async-start(bf16[128,16,128]{2,1,0:T(8,128)(2,1)} %bitcast.43), calls=%async_computation | async-start | bytes 1048576 | tf_op jit(solution)/shard_map/all_to_all | solution.py:541
  16.3 12.6 %collective-permute-start.2 = (bf16[784,128]{1,0:T(8,128)(2,1)S(1)}, bf16[784,128]{1,0:T(8,128)(2,1)S(1)}, u32[]{:S(2)}, u32[]{:S(2)}) collective-permute-start(bf16[784,128]{1,0:T(8,128)(2,1)S(1)} %get-tuple-element.24.refs_0_.rest_0_), channel_id=1, source_target_pairs={{6,0},{7,1},{0,2},{1,3},{2,4},{3,5},{4,6},{5,7},{14,8},{15,9},{8,1... | collective-permute-start | bytes 602120 | tf_op jit(solution)/shard_map/ppermute | solution.py:488
  17.7 20.1 %collective-permute-start.5 = (bf16[1808,128]{1,0:T(8,128)(2,1)S(1)}, bf16[1808,128]{1,0:T(8,128)(2,1)S(1)}, u32[]{:S(2)}, u32[]{:S(2)}) collective-permute-start(bf16[1808,128]{1,0:T(8,128)(2,1)S(1)} %collective-permute-done.1.refs_2_.rest_2_.rest_10_), channel_id=1, source_target_pairs={{1,0},{0,1},{3,2},{2,3},{5,4},{4,5},{7,6},{6,7},{9,8},{8,9},{11,10... | collective-permute-start | bytes 1388552 | tf_op jit(solution)/shard_map/ppermute | solution.py:492
  19.1 11.2 %collective-permute-start = (bf16[784,128]{1,0:T(8,128)(2,1)S(1)}, bf16[784,128]{1,0:T(8,128)(2,1)S(1)}, u32[]{:S(2)}, u32[]{:S(2)}) collective-permute-start(bf16[784,128]{1,0:T(8,128)(2,1)S(1)} %get-tuple-element.24.refs_0_.rest_0_), channel_id=1, source_target_pairs={{2,0},{3,1},{4,2},{5,3},{6,4},{7,5},{0,6},{1,7},{10,8},{11,9},{12,... | collective-permute-start | bytes 602120 | tf_op jit(solution)/shard_map/ppermute | solution.py:488
  22.8 12.0 %collective-permute-start.7 = (bf16[1024,128]{1,0:T(8,128)(2,1)S(1)}, bf16[1024,128]{1,0:T(8,128)(2,1)S(1)}, u32[]{:S(2)}, u32[]{:S(2)}) collective-permute-start(bf16[1024,128]{1,0:T(8,128)(2,1)S(1)} %get-tuple-element.41), channel_id=1, source_target_pairs={{2,0},{3,1},{4,2},{5,3},{6,4},{7,5},{0,6},{1,7},{10,8},{11,9},{12,... | collective-permute-start | bytes 786440 | tf_op jit(solution)/shard_map/ppermute | solution.py:488
  24.2 11.1 %collective-permute-start.8 = (bf16[1024,128]{1,0:T(8,128)(2,1)S(1)}, bf16[1024,128]{1,0:T(8,128)(2,1)S(1)}, u32[]{:S(2)}, u32[]{:S(2)}) collective-permute-start(bf16[1024,128]{1,0:T(8,128)(2,1)S(1)} %get-tuple-element.42), channel_id=1, source_target_pairs={{6,0},{7,1},{0,2},{1,3},{2,4},{3,5},{4,6},{5,7},{14,8},{15,9},{8,1... | collective-permute-start | bytes 786440 | tf_op jit(solution)/shard_map/ppermute | solution.py:488
  28.9 5.9 %copy-start = (bf16[784,128]{1,0:T(8,128)(2,1)}, bf16[784,128]{1,0:T(8,128)(2,1)S(1)}, u32[]{:S(2)}) copy-start(bf16[784,128]{1,0:T(8,128)(2,1)S(1)} %collective-permute-done.2.refs_3_.rest_3_) | copy-start | bytes 602116
  28.9 6.5 %collective-permute-start.6 = (bf16[784,128]{1,0:T(8,128)(2,1)S(1)}, bf16[784,128]{1,0:T(8,128)(2,1)S(1)}, u32[]{:S(2)}, u32[]{:S(2)}) collective-permute-start(bf16[784,128]{1,0:T(8,128)(2,1)S(1)} %collective-permute-done.2.refs_3_.rest_3_), channel_id=1, source_target_pairs={{1,0},{0,1},{3,2},{2,3},{5,4},{4,5},{7,6},{6,7},{9,8},{8,9},{11,10... | collective-permute-start | bytes 602120 | tf_op jit(solution)/shard_map/ppermute | solution.py:492
  30.3 4.5 %copy-start.2 = (bf16[784,128]{1,0:T(8,128)(2,1)}, bf16[784,128]{1,0:T(8,128)(2,1)S(1)}, u32[]{:S(2)}) copy-start(bf16[784,128]{1,0:T(8,128)(2,1)S(1)} %collective-permute-done.refs_1_.rest_1_) | copy-start | bytes 602116
  30.3 6.9 %collective-permute-start.4 = (bf16[784,128]{1,0:T(8,128)(2,1)S(1)}, bf16[784,128]{1,0:T(8,128)(2,1)S(1)}, u32[]{:S(2)}, u32[]{:S(2)}) collective-permute-start(bf16[784,128]{1,0:T(8,128)(2,1)S(1)} %collective-permute-done.refs_1_.rest_1_), channel_id=1, source_target_pairs={{1,0},{0,1},{3,2},{2,3},{5,4},{4,5},{7,6},{6,7},{9,8},{8,9},{11,10... | collective-permute-start | bytes 602120 | tf_op jit(solution)/shard_map/ppermute | solution.py:492
  34.8 9.8 %collective-permute-start.9 = (bf16[1024,128]{1,0:T(8,128)(2,1)S(1)}, bf16[1024,128]{1,0:T(8,128)(2,1)S(1)}, u32[]{:S(2)}, u32[]{:S(2)}) collective-permute-start(bf16[1024,128]{1,0:T(8,128)(2,1)S(1)} %get-tuple-element.38.rest_8_), channel_id=1, source_target_pairs={{1,0},{0,1},{3,2},{2,3},{5,4},{4,5},{7,6},{6,7},{9,8},{8,9},{11,10... | collective-permute-start | bytes 786440 | tf_op jit(solution)/shard_map/ppermute | solution.py:492
  35.3 9.4 %collective-permute-start.10 = (bf16[1024,128]{1,0:T(8,128)(2,1)S(1)}, bf16[1024,128]{1,0:T(8,128)(2,1)S(1)}, u32[]{:S(2)}, u32[]{:S(2)}) collective-permute-start(bf16[1024,128]{1,0:T(8,128)(2,1)S(1)} %collective-permute-done.7.rest_9_), channel_id=1, source_target_pairs={{1,0},{0,1},{3,2},{2,3},{5,4},{4,5},{7,6},{6,7},{9,8},{8,9},{11,10... | collective-permute-start | bytes 786440 | tf_op jit(solution)/shard_map/ppermute | solution.py:492
  35.4 0.7 copy-start.5
  36.1 8.6 %collective-permute-start.11 = (bf16[1024,128]{1,0:T(8,128)(2,1)S(1)}, bf16[1024,128]{1,0:T(8,128)(2,1)S(1)}, u32[]{:S(2)}, u32[]{:S(2)}) collective-permute-start(bf16[1024,128]{1,0:T(8,128)(2,1)S(1)} %collective-permute-done.8.rest_11_), channel_id=1, source_target_pairs={{1,0},{0,1},{3,2},{2,3},{5,4},{4,5},{7,6},{6,7},{9,8},{8,9},{11,10... | collective-permute-start | bytes 786440 | tf_op jit(solution)/shard_map/ppermute | solution.py:492
  37.2 0.7 copy-start.8
  37.9 0.9 %copy-start.1 = (bf16[784,128]{1,0:T(8,128)(2,1)S(1)}, bf16[784,128]{1,0:T(8,128)(2,1)}, u32[]{:S(2)}) copy-start(bf16[784,128]{1,0:T(8,128)(2,1)} %copy-done) | copy-start | bytes 602116
  38.8 0.9 %copy-start.3 = (bf16[784,128]{1,0:T(8,128)(2,1)S(1)}, bf16[784,128]{1,0:T(8,128)(2,1)}, u32[]{:S(2)}) copy-start(bf16[784,128]{1,0:T(8,128)(2,1)} %copy-done.2) | copy-start | bytes 602116
  39.7 0.9 %copy-start.6 = (bf16[784,128]{1,0:T(8,128)(2,1)S(1)}, bf16[784,128]{1,0:T(8,128)(2,1)}, u32[]{:S(2)}) copy-start(bf16[784,128]{1,0:T(8,128)(2,1)} %copy-done.5) | copy-start | bytes 602116
  40.7 0.9 %copy-start.9 = (bf16[784,128]{1,0:T(8,128)(2,1)S(1)}, bf16[784,128]{1,0:T(8,128)(2,1)}, u32[]{:S(2)}) copy-start(bf16[784,128]{1,0:T(8,128)(2,1)} %copy-done.8) | copy-start | bytes 602116
  41.6 3.1 %copy-start.4 = (bf16[784,128]{1,0:T(8,128)(2,1)S(1)}, bf16[784,128]{1,0:T(8,128)(2,1)}, u32[]{:S(2)}) copy-start(bf16[784,128]{1,0:T(8,128)(2,1)} %copy-done.2) | copy-start | bytes 602116
  41.6 3.1 %copy-start.7 = (bf16[784,128]{1,0:T(8,128)(2,1)S(1)}, bf16[784,128]{1,0:T(8,128)(2,1)}, u32[]{:S(2)}) copy-start(bf16[784,128]{1,0:T(8,128)(2,1)} %copy-done.5) | copy-start | bytes 602116
  44.7 34.6 %copy-start.10 = (bf16[16]{0:T(256)(128)(2,1)S(1)}, bf16[16]{0:T(256)(128)(2,1)}, u32[]{:S(2)}) copy-start(bf16[16]{0:T(256)(128)(2,1)} %param.32) | copy-start | bytes 100

commit v5 on v4

--- a/solution.py
+++ b/solution.py
@@ -318,7 +318,12 @@
     gain_ref, strength_ref, decay_ref, log_decay_ref, parent_ref = small
     probe_ref, pv_ref, gate_ref = outs
     wq_ref, wk_ref = held
-    copies = copies_in(sources, held, sems)
+    halves = [pl.ds(1024 * i, 1024) for i in range(2)]
+    copies = [
+        pltpu.make_async_copy(source.at[half], target.at[half], sems.at[i, j])
+        for i, half in enumerate(halves)
+        for j, (source, target) in enumerate(zip(sources, held))
+    ]
     start_all(copies)
     group = lax.axis_index("tp")
     x = x_ref[...].astype(f32)
@@ -343,9 +348,13 @@
     both = rounded(project(both, 1))
     values, zgate = both[:128], both[128:]
     logits = project(scalars, 1)
-    wait_all(copies)
-    queries = rounded(project(wq_ref[...], 0))
-    keys = rounded(project(wk_ref[...], 0))
+    queries = keys = 0.0
+    for i, half in enumerate(halves):
+        wait_all(copies[2 * i : 2 * i + 2])
+        part = normed[1024 * i : 1024 * i + 1024]
+        queries = queries + dot(wq_ref[half, :], part, 0, 0)
+        keys = keys + dot(wk_ref[half, :], part, 0, 0)
+    queries, keys = rounded(queries), rounded(keys)
     gain = jnp.concatenate([pack_rows(pack, 768, 16) for pack in packs], axis=0).astype(f32)
 
     def unit(x):
@@ -393,7 +402,7 @@
             pltpu.VMEM((128, 128), f32),
             pltpu.VMEM((128, 128), f32),
         ],
-        scratch_shapes=scratch_like(weights),
+        scratch_shapes=[pltpu.VMEM(w.shape, w.dtype) for w in weights] + [pltpu.SemaphoreType.DMA((2, 2))],
         cost_estimate=cost(2000000000, 4 << 20),
         compiler_params=pltpu.CompilerParams(vmem_limit_bytes=VMEM_LIMIT),
         name="row_side",

time: 80.7 us -> 80.7 us (level)
  no operation moved by 1% of the time
where the time goes in v5:
time: 80.7 us; the launch traced here: 80.3 us
  blocking collectives  33.6 us (42%)
  starting transfers between devices  22.2 us (28%)
  Pallas kernels  13.4 us (17%)
  local copies, waits for them, and re-layouts  5.09 us (6%)
  waiting for transfers between devices  4.59 us (6%)
  between operations  1.45 us (2%)
    all_to_all x1, blocking collectives, whole_step(): parts = lax.all_to_all(part.reshape(16, 8, 2048), 'kv', 0, 0, tiled=True)  17.6 us
    all_to_all x1, blocking collectives, whole_step(): blocks = lax.all_to_all(sum_heads(parts), BOTH, 0, 0, tiled=True)  15.9 us
    ppermute x5, starting transfers between devices, chip_permute(): return lax.ppermute(x, 'tp', [((i + 2 * d) % 8, i) for i in range(8)])  9.26 us
    all_to_all x1, starting transfers between devices, whole_step(): lax.all_to_all(sent.reshape(128, 16, 128), BOTH, 0, 0, tiled=True)  8.22 us
    unnamed x22, local copies, waits for them, and re-layouts  5.09 us
    ppermute x7, starting transfers between devices, core_permute(): return lax.ppermute(x, 'tp', [(i ^ 1, i) for i in range(8)])  4.75 us
    ppermute x5, waiting for transfers between devices, chip_permute(): return lax.ppermute(x, 'tp', [((i + 2 * d) % 8, i) for i in range(8)])  4.57 us
    pallas_call x1, Pallas kernels, all_chips_state(): pl.pallas_call(all_chips_kernel, in_specs=hbm_specs(2) + vmem_specs(4), o...  4.43 us
  transfers between devices with their start and end apart: 13, of which 1 were waited for; matrix products, arithmetic and copies ran while one was open for 0% of the time, Pallas kernels for 11%

profile of v5, /device:TPU:1, one launch (start us, length us, event | category | flops | bytes accessed | tf_op | source)
XLA Modules:
  0.0 80.3 jit_solution(151016863703897970)
XLA Ops:
  0.6 2.8 %prepare.1 = (bf16[16,8,16,128]{3,2,1,0:T(8,128)(2,1)}, bf16[784,128]{1,0:T(8,128)(2,1)S(1)}, bf16[1808,128]{1,0:T(8,128)(2,1)S(1)}, bf16[1024,128]{1,0:T(8,128)...) custom-call(bf16[4,16,256]{2,1,0:T(8,128)(2,1)} %bitcast.49, ...), custom_call_target="tpu_custom_call" | custom-call | flops 10000000 | bytes 1048576 | tf_op jit(solution)/shard_map/prepare/pallas_call | solution.py:126
  3.5 3.6 %collective-permute-start.1 = (bf16[1808,128]{1,0:T(8,128)(2,1)S(1)}, bf16[1808,128]{1,0:T(8,128)(2,1)S(1)}, u32[]{:S(2)}, u32[]{:S(2)}) collective-permute-start(bf16[1808,128]{1,0:T(8,128)(2,1)S(1)} %get-tuple-element.25), channel_id=1, source_target_pairs={{4,0},{5,1},{6,2},{7,3},{0,4},{1,5},{2,6},{3,7},{12,8},{13,9},{14,... | collective-permute-start | bytes 1388552 | tf_op jit(solution)/shard_map/ppermute | solution.py:497
  7.1 1.0 %collective-permute-start.3 = (bf16[784,128]{1,0:T(8,128)(2,1)S(1)}, bf16[784,128]{1,0:T(8,128)(2,1)S(1)}, u32[]{:S(2)}, u32[]{:S(2)}) collective-permute-start(bf16[784,128]{1,0:T(8,128)(2,1)S(1)} %get-tuple-element.24.refs_0_.rest_0_), channel_id=1, source_target_pairs={{1,0},{0,1},{3,2},{2,3},{5,4},{4,5},{7,6},{6,7},{9,8},{8,9},{11,10... | collective-permute-start | bytes 602120 | tf_op jit(solution)/shard_map/ppermute | solution.py:501
  8.1 8.2 %all-to-all-start = ((bf16[128,16,128]{2,1,0:T(8,128)(2,1)}), bf16[128,16,128]{2,1,0:T(8,128)(2,1)S(1)}, u32[]{:S(2)}, u32[]{:S(2)}) async-start(bf16[128,16,128]{2,1,0:T(8,128)(2,1)} %bitcast.43), calls=%async_computation | async-start | bytes 1048576 | tf_op jit(solution)/shard_map/all_to_all | solution.py:550
  16.3 1.4 %collective-permute-start.2 = (bf16[784,128]{1,0:T(8,128)(2,1)S(1)}, bf16[784,128]{1,0:T(8,128)(2,1)S(1)}, u32[]{:S(2)}, u32[]{:S(2)}) collective-permute-start(bf16[784,128]{1,0:T(8,128)(2,1)S(1)} %get-tuple-element.24.refs_0_.rest_0_), channel_id=1, source_target_pairs={{6,0},{7,1},{0,2},{1,3},{2,4},{3,5},{4,6},{5,7},{14,8},{15,9},{8,1... | collective-permute-start | bytes 602120 | tf_op jit(solution)/shard_map/ppermute | solution.py:497
  17.7 0.0 collective-permute-done.1.refs_2_.rest_2_.rest_10_
  17.7 1.3 %collective-permute-start.5 = (bf16[1808,128]{1,0:T(8,128)(2,1)S(1)}, bf16[1808,128]{1,0:T(8,128)(2,1)S(1)}, u32[]{:S(2)}, u32[]{:S(2)}) collective-permute-start(bf16[1808,128]{1,0:T(8,128)(2,1)S(1)} %collective-permute-done.1.refs_2_.rest_2_.rest_10_), channel_id=1, source_target_pairs={{1,0},{0,1},{3,2},{2,3},{5,4},{4,5},{7,6},{6,7},{9,8},{8,9},{11,10... | collective-permute-start | bytes 1388552 | tf_op jit(solution)/shard_map/ppermute | solution.py:501
  19.1 2.7 %collective-permute-start = (bf16[784,128]{1,0:T(8,128)(2,1)S(1)}, bf16[784,128]{1,0:T(8,128)(2,1)S(1)}, u32[]{:S(2)}, u32[]{:S(2)}) collective-permute-start(bf16[784,128]{1,0:T(8,128)(2,1)S(1)} %get-tuple-element.24.refs_0_.rest_0_), channel_id=1, source_target_pairs={{2,0},{3,1},{4,2},{5,3},{6,4},{7,5},{0,6},{1,7},{10,8},{11,9},{12,... | collective-permute-start | bytes 602120 | tf_op jit(solution)/shard_map/ppermute | solution.py:497
  21.8 1.0 %other_chips_state.1 = (bf16[1024,128]{1,0:T(8,128)(2,1)S(1)}, bf16[1024,128]{1,0:T(8,128)(2,1)S(1)}) custom-call(bf16[2048,128]{1,0:T(8,128)(2,1)S(1)} %get-tuple-element.39.state_ref, bf16[1024,128]{1,0:T(8,128)(2,1)S(1)} %get-tuple-element.40.refs_0_, bf16[4,16,256]{2,1,0:T(8,128)(2,1)S(1)} %get-tuple-element.34.refs_0_.refs_1_, ...), custom_call_target="tpu_custom_call" | custom-call | flops 1000000000 | bytes 2097152 | tf_op jit(solution)/shard_map/other_chips_state/pallas_call | solution.py:216
  22.8 1.4 %collective-permute-start.7 = (bf16[1024,128]{1,0:T(8,128)(2,1)S(1)}, bf16[1024,128]{1,0:T(8,128)(2,1)S(1)}, u32[]{:S(2)}, u32[]{:S(2)}) collective-permute-start(bf16[1024,128]{1,0:T(8,128)(2,1)S(1)} %get-tuple-element.41), channel_id=1, source_target_pairs={{2,0},{3,1},{4,2},{5,3},{6,4},{7,5},{0,6},{1,7},{10,8},{11,9},{12,... | collective-permute-start | bytes 786440 | tf_op jit(solution)/shard_map/ppermute | solution.py:497
  24.2 0.0 collective-permute-done.3.refs_4_.rest_4_
  24.2 0.1 collective-permute-start.8
  24.3 4.6 %collective-permute-done.2.refs_3_.rest_3_ = bf16[784,128]{1,0:T(8,128)(2,1)S(1)} collective-permute-done((bf16[784,128]{1,0:T(8,128)(2,1)S(1)}, bf16[784,128]{1,0:T(8,128)(2,1)S(1)}, u32[]{:S(2)}, u32[]{:S(2)}) %collective-permute-start.2) | collective-permute-done | bytes 200736 | tf_op jit(solution)/shard_map/ppermute | solution.py:497
  28.9 1.4 %collective-permute-start.6 = (bf16[784,128]{1,0:T(8,128)(2,1)S(1)}, bf16[784,128]{1,0:T(8,128)(2,1)S(1)}, u32[]{:S(2)}, u32[]{:S(2)}) collective-permute-start(bf16[784,128]{1,0:T(8,128)(2,1)S(1)} %collective-permute-done.2.refs_3_.rest_3_), channel_id=1, source_target_pairs={{1,0},{0,1},{3,2},{2,3},{5,4},{4,5},{7,6},{6,7},{9,8},{8,9},{11,10... | collective-permute-start | bytes 602120 | tf_op jit(solution)/shard_map/ppermute | solution.py:501
  30.3 0.0 collective-permute-done.refs_1_.rest_1_
  30.3 0.1 collective-permute-start.4
  30.4 4.4 %all_chips_state.1 = (f32[256,16,128]{2,1,0:T(8,128)}, bf16[1024,128]{1,0:T(8,128)(2,1)S(1)}) custom-call(f32[256,16,128]{2,1,0:T(8,128)} %bitcast.42, bf16[1024,128]{1,0:T(8,128)(2,1)} %bitcast.45, bf16[4,16,256]{2,1,0:T(8,128)(2,1)S(1)} %get-tuple-element.34.refs_0_.refs_1_, f32[4,1,256]{2,1,0:T(1,128)S(1)} %get-tuple-element.35.refs_1_.refs_2_, ...), custom_call_target="tpu_custom_call" | custom-call | flops 2000000000 | bytes 4194304 | tf_op jit(solution)/shard_map/all_chips_state/pallas_call | solution.py:263
  34.8 0.0 copy-done
  34.8 0.0 copy-done.2
  34.8 0.0 collective-permute-done.7.rest_9_
  34.8 0.5 collective-permute-start.9
  35.3 0.0 collective-permute-done.8.rest_11_
  35.3 0.1 collective-permute-start.10
  35.4 0.0 collective-permute-done.6.refs_7_.rest_7_
  35.4 0.7 copy-done.5
  36.1 0.4 collective-permute-start.11
  37.2 0.0 collective-permute-done.4.refs_5_.rest_5_
  37.2 0.0 copy-start.8
  37.2 0.7 copy-done.8
  37.9 0.0 all-to-all-done
  37.9 0.0 collective-permute-done.5.refs_6_.rest_6_.rest_14_
  37.9 0.9 %copy-done.1 = bf16[784,128]{1,0:T(8,128)(2,1)S(1)} copy-done((bf16[784,128]{1,0:T(8,128)(2,1)S(1)}, bf16[784,128]{1,0:T(8,128)(2,1)}, u32[]{:S(2)}) %copy-start.1) | copy-done | bytes 200728
  38.8 0.9 %copy-done.3 = bf16[784,128]{1,0:T(8,128)(2,1)S(1)} copy-done((bf16[784,128]{1,0:T(8,128)(2,1)S(1)}, bf16[784,128]{1,0:T(8,128)(2,1)}, u32[]{:S(2)}) %copy-start.3) | copy-done | bytes 200728
  39.7 0.9 %copy-done.6 = bf16[784,128]{1,0:T(8,128)(2,1)S(1)} copy-done((bf16[784,128]{1,0:T(8,128)(2,1)S(1)}, bf16[784,128]{1,0:T(8,128)(2,1)}, u32[]{:S(2)}) %copy-start.6) | copy-done | bytes 200728
  40.7 0.9 %copy-done.9 = bf16[784,128]{1,0:T(8,128)(2,1)S(1)} copy-done((bf16[784,128]{1,0:T(8,128)(2,1)S(1)}, bf16[784,128]{1,0:T(8,128)(2,1)}, u32[]{:S(2)}) %copy-start.9) | copy-done | bytes 200728
  41.6 3.0 %row_side.1 = (bf16[128,128]{1,0:T(8,128)(2,1)S(1)}, f32[128,128]{1,0:T(8,128)S(1)}, f32[128,128]{1,0:T(8,128)S(1)}) custom-call(bf16[2048,128]{1,0:T(8,128)(2,1)S(1)} %bitcast.37, bf16[784,128]{1,0:T(8,128)(2,1)S(1)} %get-tuple-element.24.refs_0_.rest_0_, bf16[784,128]{1,0:T(8,128)(2,1)S(1)} %copy-done.3, ...), custom_call_target="tpu_custom_call" | custom-call | flops 2000000000 | bytes 4194304 | tf_op jit(solution)/shard_map/row_side/pallas_call | solution.py:396
  44.6 0.0 collective-permute-done.9.rest_12_
  44.6 0.0 collective-permute-done.10.rest_13_
  44.6 0.0 collective-permute-done.11.rest_15_
  44.6 0.0 copy-done.4
  44.7 0.0 copy-done.7
  44.7 0.0 copy-start.10
  44.7 0.8 readout.1
  45.5 17.6 %all_to_all.21.part_ref = bf16[16,8,2048]{2,1,0:T(8,128)(2,1)S(1)} all-to-all(bf16[16,8,2048]{2,1,0:T(8,128)(2,1)S(1)} %bitcast.36), channel_id=1, replica_groups=mesh['kv'=16,'tp'=8] {'kv'}, dimensions={0} | all-to-all | bytes 1048576 | tf_op jit(solution)/shard_map/all_to_all | solution.py:559
  63.1 0.3 sum_heads.1
  63.4 15.9 %all_to_all.22 = f32[128,1,128]{2,1,0:T(1,128)S(1)} all-to-all(f32[128,1,128]{2,1,0:T(1,128)S(1)} %bitcast.38), channel_id=1, replica_groups=mesh['kv'=16,'tp'=8] {'kv','tp'}, dimensions={0} | all-to-all | bytes 131072 | tf_op jit(solution)/shard_map/all_to_all | solution.py:560
  79.3 0.0 copy-done.10
  79.3 1.0 %final_rows.1 = bf16[4,16,256]{2,1,0:T(8,128)(2,1)} custom-call(f32[128,128]{1,0:T(8,128)S(1)} %bitcast.39, bf16[1,16]{1,0:T(2,128)(2,1)S(1)} %bitcast.40), custom_call_target="tpu_custom_call" | custom-call | flops 10000000 | bytes 262144 | tf_op jit(solution)/shard_map/final_rows/pallas_call | solution.py:484
  (9 shorter events, 0.0 us)
Async XLA Ops:
  3.5 14.2 %collective-permute-start.1 = (bf16[1808,128]{1,0:T(8,128)(2,1)S(1)}, bf16[1808,128]{1,0:T(8,128)(2,1)S(1)}, u32[]{:S(2)}, u32[]{:S(2)}) collective-permute-start(bf16[1808,128]{1,0:T(8,128)(2,1)S(1)} %get-tuple-element.25), channel_id=1, source_target_pairs={{4,0},{5,1},{6,2},{7,3},{0,4},{1,5},{2,6},{3,7},{12,8},{13,9},{14,... | collective-permute-start | bytes 1388552 | tf_op jit(solution)/shard_map/ppermute | solution.py:497
  7.1 17.1 %collective-permute-start.3 = (bf16[784,128]{1,0:T(8,128)(2,1)S(1)}, bf16[784,128]{1,0:T(8,128)(2,1)S(1)}, u32[]{:S(2)}, u32[]{:S(2)}) collective-permute-start(bf16[784,128]{1,0:T(8,128)(2,1)S(1)} %get-tuple-element.24.refs_0_.rest_0_), channel_id=1, source_target_pairs={{1,0},{0,1},{3,2},{2,3},{5,4},{4,5},{7,6},{6,7},{9,8},{8,9},{11,10... | collective-permute-start | bytes 602120 | tf_op jit(solution)/shard_map/ppermute | solution.py:501
  8.1 29.8 %all-to-all-start = ((bf16[128,16,128]{2,1,0:T(8,128)(2,1)}), bf16[128,16,128]{2,1,0:T(8,128)(2,1)S(1)}, u32[]{:S(2)}, u32[]{:S(2)}) async-start(bf16[128,16,128]{2,1,0:T(8,128)(2,1)} %bitcast.43), calls=%async_computation | async-start | bytes 1048576 | tf_op jit(solution)/shard_map/all_to_all | solution.py:550
  16.3 12.6 %collective-permute-start.2 = (bf16[784,128]{1,0:T(8,128)(2,1)S(1)}, bf16[784,128]{1,0:T(8,128)(2,1)S(1)}, u32[]{:S(2)}, u32[]{:S(2)}) collective-permute-start(bf16[784,128]{1,0:T(8,128)(2,1)S(1)} %get-tuple-element.24.refs_0_.rest_0_), channel_id=1, source_target_pairs={{6,0},{7,1},{0,2},{1,3},{2,4},{3,5},{4,6},{5,7},{14,8},{15,9},{8,1... | collective-permute-start | bytes 602120 | tf_op jit(solution)/shard_map/ppermute | solution.py:497
  17.7 20.1 %collective-permute-start.5 = (bf16[1808,128]{1,0:T(8,128)(2,1)S(1)}, bf16[1808,128]{1,0:T(8,128)(2,1)S(1)}, u32[]{:S(2)}, u32[]{:S(2)}) collective-permute-start(bf16[1808,128]{1,0:T(8,128)(2,1)S(1)} %collective-permute-done.1.refs_2_.rest_2_.rest_10_), channel_id=1, source_target_pairs={{1,0},{0,1},{3,2},{2,3},{5,4},{4,5},{7,6},{6,7},{9,8},{8,9},{11,10... | collective-permute-start | bytes 1388552 | tf_op jit(solution)/shard_map/ppermute | solution.py:501
  19.1 11.2 %collective-permute-start = (bf16[784,128]{1,0:T(8,128)(2,1)S(1)}, bf16[784,128]{1,0:T(8,128)(2,1)S(1)}, u32[]{:S(2)}, u32[]{:S(2)}) collective-permute-start(bf16[784,128]{1,0:T(8,128)(2,1)S(1)} %get-tuple-element.24.refs_0_.rest_0_), channel_id=1, source_target_pairs={{2,0},{3,1},{4,2},{5,3},{6,4},{7,5},{0,6},{1,7},{10,8},{11,9},{12,... | collective-permute-start | bytes 602120 | tf_op jit(solution)/shard_map/ppermute | solution.py:497
  22.8 12.0 %collective-permute-start.7 = (bf16[1024,128]{1,0:T(8,128)(2,1)S(1)}, bf16[1024,128]{1,0:T(8,128)(2,1)S(1)}, u32[]{:S(2)}, u32[]{:S(2)}) collective-permute-start(bf16[1024,128]{1,0:T(8,128)(2,1)S(1)} %get-tuple-element.41), channel_id=1, source_target_pairs={{2,0},{3,1},{4,2},{5,3},{6,4},{7,5},{0,6},{1,7},{10,8},{11,9},{12,... | collective-permute-start | bytes 786440 | tf_op jit(solution)/shard_map/ppermute | solution.py:497
  24.2 11.1 %collective-permute-start.8 = (bf16[1024,128]{1,0:T(8,128)(2,1)S(1)}, bf16[1024,128]{1,0:T(8,128)(2,1)S(1)}, u32[]{:S(2)}, u32[]{:S(2)}) collective-permute-start(bf16[1024,128]{1,0:T(8,128)(2,1)S(1)} %get-tuple-element.42), channel_id=1, source_target_pairs={{6,0},{7,1},{0,2},{1,3},{2,4},{3,5},{4,6},{5,7},{14,8},{15,9},{8,1... | collective-permute-start | bytes 786440 | tf_op jit(solution)/shard_map/ppermute | solution.py:497
  28.9 5.9 %copy-start = (bf16[784,128]{1,0:T(8,128)(2,1)}, bf16[784,128]{1,0:T(8,128)(2,1)S(1)}, u32[]{:S(2)}) copy-start(bf16[784,128]{1,0:T(8,128)(2,1)S(1)} %collective-permute-done.2.refs_3_.rest_3_) | copy-start | bytes 602116
  28.9 6.5 %collective-permute-start.6 = (bf16[784,128]{1,0:T(8,128)(2,1)S(1)}, bf16[784,128]{1,0:T(8,128)(2,1)S(1)}, u32[]{:S(2)}, u32[]{:S(2)}) collective-permute-start(bf16[784,128]{1,0:T(8,128)(2,1)S(1)} %collective-permute-done.2.refs_3_.rest_3_), channel_id=1, source_target_pairs={{1,0},{0,1},{3,2},{2,3},{5,4},{4,5},{7,6},{6,7},{9,8},{8,9},{11,10... | collective-permute-start | bytes 602120 | tf_op jit(solution)/shard_map/ppermute | solution.py:501
  30.3 4.5 %copy-start.2 = (bf16[784,128]{1,0:T(8,128)(2,1)}, bf16[784,128]{1,0:T(8,128)(2,1)S(1)}, u32[]{:S(2)}) copy-start(bf16[784,128]{1,0:T(8,128)(2,1)S(1)} %collective-permute-done.refs_1_.rest_1_) | copy-start | bytes 602116
  30.3 6.9 %collective-permute-start.4 = (bf16[784,128]{1,0:T(8,128)(2,1)S(1)}, bf16[784,128]{1,0:T(8,128)(2,1)S(1)}, u32[]{:S(2)}, u32[]{:S(2)}) collective-permute-start(bf16[784,128]{1,0:T(8,128)(2,1)S(1)} %collective-permute-done.refs_1_.rest_1_), channel_id=1, source_target_pairs={{1,0},{0,1},{3,2},{2,3},{5,4},{4,5},{7,6},{6,7},{9,8},{8,9},{11,10... | collective-permute-start | bytes 602120 | tf_op jit(solution)/shard_map/ppermute | solution.py:501
  34.8 9.8 %collective-permute-start.9 = (bf16[1024,128]{1,0:T(8,128)(2,1)S(1)}, bf16[1024,128]{1,0:T(8,128)(2,1)S(1)}, u32[]{:S(2)}, u32[]{:S(2)}) collective-permute-start(bf16[1024,128]{1,0:T(8,128)(2,1)S(1)} %get-tuple-element.38.rest_8_), channel_id=1, source_target_pairs={{1,0},{0,1},{3,2},{2,3},{5,4},{4,5},{7,6},{6,7},{9,8},{8,9},{11,10... | collective-permute-start | bytes 786440 | tf_op jit(solution)/shard_map/ppermute | solution.py:501
  35.3 9.3 %collective-permute-start.10 = (bf16[1024,128]{1,0:T(8,128)(2,1)S(1)}, bf16[1024,128]{1,0:T(8,128)(2,1)S(1)}, u32[]{:S(2)}, u32[]{:S(2)}) collective-permute-start(bf16[1024,128]{1,0:T(8,128)(2,1)S(1)} %collective-permute-done.7.rest_9_), channel_id=1, source_target_pairs={{1,0},{0,1},{3,2},{2,3},{5,4},{4,5},{7,6},{6,7},{9,8},{8,9},{11,10... | collective-permute-start | bytes 786440 | tf_op jit(solution)/shard_map/ppermute | solution.py:501
  35.4 0.7 copy-start.5
  36.1 8.5 %collective-permute-start.11 = (bf16[1024,128]{1,0:T(8,128)(2,1)S(1)}, bf16[1024,128]{1,0:T(8,128)(2,1)S(1)}, u32[]{:S(2)}, u32[]{:S(2)}) collective-permute-start(bf16[1024,128]{1,0:T(8,128)(2,1)S(1)} %collective-permute-done.8.rest_11_), channel_id=1, source_target_pairs={{1,0},{0,1},{3,2},{2,3},{5,4},{4,5},{7,6},{6,7},{9,8},{8,9},{11,10... | collective-permute-start | bytes 786440 | tf_op jit(solution)/shard_map/ppermute | solution.py:501
  37.2 0.7 copy-start.8
  37.9 0.9 %copy-start.1 = (bf16[784,128]{1,0:T(8,128)(2,1)S(1)}, bf16[784,128]{1,0:T(8,128)(2,1)}, u32[]{:S(2)}) copy-start(bf16[784,128]{1,0:T(8,128)(2,1)} %copy-done) | copy-start | bytes 602116
  38.8 0.9 %copy-start.3 = (bf16[784,128]{1,0:T(8,128)(2,1)S(1)}, bf16[784,128]{1,0:T(8,128)(2,1)}, u32[]{:S(2)}) copy-start(bf16[784,128]{1,0:T(8,128)(2,1)} %copy-done.2) | copy-start | bytes 602116
  39.7 0.9 %copy-start.6 = (bf16[784,128]{1,0:T(8,128)(2,1)S(1)}, bf16[784,128]{1,0:T(8,128)(2,1)}, u32[]{:S(2)}) copy-start(bf16[784,128]{1,0:T(8,128)(2,1)} %copy-done.5) | copy-start | bytes 602116
  40.7 0.9 %copy-start.9 = (bf16[784,128]{1,0:T(8,128)(2,1)S(1)}, bf16[784,128]{1,0:T(8,128)(2,1)}, u32[]{:S(2)}) copy-start(bf16[784,128]{1,0:T(8,128)(2,1)} %copy-done.8) | copy-start | bytes 602116
  41.6 3.1 %copy-start.4 = (bf16[784,128]{1,0:T(8,128)(2,1)S(1)}, bf16[784,128]{1,0:T(8,128)(2,1)}, u32[]{:S(2)}) copy-start(bf16[784,128]{1,0:T(8,128)(2,1)} %copy-done.2) | copy-start | bytes 602116
  41.6 3.1 %copy-start.7 = (bf16[784,128]{1,0:T(8,128)(2,1)S(1)}, bf16[784,128]{1,0:T(8,128)(2,1)}, u32[]{:S(2)}) copy-start(bf16[784,128]{1,0:T(8,128)(2,1)} %copy-done.5) | copy-start | bytes 602116
  44.7 34.6 %copy-start.10 = (bf16[16]{0:T(256)(128)(2,1)S(1)}, bf16[16]{0:T(256)(128)(2,1)}, u32[]{:S(2)}) copy-start(bf16[16]{0:T(256)(128)(2,1)} %param.32) | copy-start | bytes 100
